TPU v7x, 512 devices: a whole 4x8x8 slice. The times are simulated.
512 devices in a mesh: ep: 32 (over z, x), tp: 16 (over y, core).
Axes of the slice: x: 4, y: 8, z: 8, core: 2. Of those that a mesh axis runs over, the one named last changes fastest.
Arguments:
- mixer_group_input: bfloat16 [8192, 1024], P('ep', 'tp'), may hold values from -6 to 6
- log_step_size: float32 [64, 8192], P('tp', 'ep'), may hold values from -16 to 0
- extra_log_decay: float32 [64, 8192], P('tp', 'ep'), may hold values from -0.7 to 0
- negated_eigen_real: float32 [64, 64], P('tp'), may hold values from 0.35 to 0.7
- frequency: float32 [64, 64], P('tp'), may hold values from 0 to 200
- group_input_matrices: bfloat16 [2, 64, 64, 16], P(None, 'tp'), may hold values from -1.5 to 1.5
- group_output_matrices: bfloat16 [2, 64, 16, 64], P(None, 'tp'), may hold values from -0.5 to 0.5
- channel_feedthrough: float32 [1024], P('tp'), may hold values from -3 to 3
- mixer_norm_scale: float32 [1024], replicated, may hold values from 0.1 to 1.9
- mixer_output_weight: bfloat16 [1024, 2048], P(None, 'tp'), may hold values from -0.1875 to 0.1875
- second_micro_input: bfloat16 [4096, 2048], P('ep'), may hold values from -6 to 6
- expert_norm_scale: float32 [2048], replicated, may hold values from 0.1 to 1.9
- routes: int32 [4096, 4], P('ep'), may hold values from 0 to 31, all different within a row; in each aligned block of 128 rows (0 to 127, 128 to 255, ...) at most 32 rows name the same one
- chosen_expert_weight: float32 [4096, 4], P('ep'), may hold values from 0.1 to 1
- expert_gate_weight: bfloat16 [32, 2048, 2048], P('ep', None, 'tp'), may hold values from -0.125 to 0.125
- expert_up_weight: bfloat16 [32, 2048, 2048], P('ep', None, 'tp'), may hold values from -0.125 to 0.125
- expert_down_weight: bfloat16 [32, 2048, 2048], P('ep', None, 'tp'), may hold values from -0.125 to 0.125
- shared_gate_weight: bfloat16 [2048, 2048], P(None, 'tp'), may hold values from -0.125 to 0.125
- shared_up_weight: bfloat16 [2048, 2048], P(None, 'tp'), may hold values from -0.125 to 0.125
- shared_down_weight: bfloat16 [2048, 2048], P(None, 'tp'), may hold values from -0.125 to 0.125
Outputs:
- mixed: bfloat16 [8192, 2048], P('ep', 'tp')
- moe_out: bfloat16 [4096, 2048], P('ep', 'tp')
Inputs may be any that keep to these rules, and one draw needn't show every extreme that they name: `routes`: each row names 4 different experts; in each aligned block of 128 rows no expert is named by more than 32 rows, and in some block one expert is named by exactly 32 rows.
All inputs are finite; a program needn't handle non-finite values.
Results may differ from a plain program's by a relative error of at most 0.0068.
Values may be sent and summed in bfloat16 or wider, within the bound.
No kernel may reach another device: no remote copies, remote signals or barrier semaphores. Data moves between devices by JAX's collectives and lax.ppermute only.
A program may use at most 128 MiB of HBM per device.

v0:
```python
import jax
import jax.numpy as jnp
from jax import lax
from jax.sharding import Mesh
from jax.sharding import PartitionSpec as P

TP = ("tp_0", "tp_1")


eps_norm = 1e-06


def copy_for_each(shard, axis):
    copies = jnp.broadcast_to(shard, (lax.axis_size(axis), *shard.shape))
    return lax.all_to_all(copies, axis, split_axis=0, concat_axis=0, tiled=True)


def gathered_once(shard, axis):
    leaves = jax.tree.leaves(shard)
    order = sorted(range(len(leaves)), key=lambda k: -leaves[k].size)
    width = (1, *leaves[order[0]].shape)[-1]
    lines = [
        jnp.pad(leaves[k].reshape(-1), (0, -leaves[k].size % width)).reshape(-1, width)
        for k in order
    ]
    both, at, found = (copy_for_each(jnp.concatenate(lines), axis), 0, {})
    for k, line in zip(order, lines):
        share = both[:, at : at + len(line)].reshape(len(both), -1)
        found[k] = share[:, : leaves[k].size].reshape(-1, *leaves[k].shape)
        at += len(line)
    numbers = iter(range(len(leaves)))
    return jax.tree.map(lambda _: found[next(numbers)], shard)


def folded_in_pairs(pieces, combine):
    while len(jax.tree.leaves(pieces)[0]) > 1:
        pieces = jax.vmap(combine)(
            *(jax.tree.map(lambda part: part[side::2], pieces) for side in (0, 1))
        )
    return jax.tree.map(lambda part: part[0], pieces)


def prefix_2(shard, axis, combine, identity):
    devices, index = (lax.axis_size(axis), lax.axis_index(axis))
    passed = jnp.arange(devices) < index

    def kept(part, zero, own):
        part = jnp.where(
            passed.reshape(-1, *(1 for _ in own.shape)), part, jnp.asarray(zero, own.dtype)
        )
        return part

    pieces = gathered_once(shard, axis)
    return folded_in_pairs(jax.tree.map(kept, pieces, identity, shard), combine)


def in_order(tiles, dim):
    dims = list(tiles.shape[1:])
    dims[dim] *= tiles.shape[0]
    return jnp.moveaxis(tiles, 0, dim).reshape(dims)


def all_blocks(shard, axes, order):
    tiles = shard[None]
    for k in order:
        tiles = lax.all_gather(tiles, axes[k], axis=0, tiled=True)
    held = [lax.axis_size(axes[k]) for k in reversed(order)]
    tiles = tiles.reshape(*held, *shard.shape)
    turned = sorted(range(len(order)), key=lambda place: order[len(order) - 1 - place])
    return tiles.transpose(*turned, *range(len(order), tiles.ndim)).reshape(-1, *shard.shape)


def whole_of(shard, axes, order, dim):
    return in_order(all_blocks(shard, axes, order), dim)


def side_by_side(arrays, axis, dim, along):
    ends, at = ([], 0)
    for a in arrays[:-1]:
        at += a.shape[along]
        ends.append(at)
    both = jnp.concatenate(arrays, axis=along)
    return tuple(jnp.split(lax.all_gather(both, axis, axis=dim, tiled=True), ends, axis=along))


def combine_steps(earlier, latter):
    return (
        earlier[0] * latter[0] - earlier[1] * latter[1],
        earlier[0] * latter[1] + earlier[1] * latter[0],
        latter[0] * earlier[2] - latter[1] * earlier[3] + latter[2],
        latter[0] * earlier[3] + latter[1] * earlier[2] + latter[3],
    )


def local_states(inputs, step_logs, losses, negated_eigen_real, frequency, group_input_matrices):
    positions = inputs.shape[0]
    group_list, states = negated_eigen_real.shape
    channels = inputs.reshape(positions, group_list, -1)
    step_size = jnp.exp(step_logs).T
    decay_log = -negated_eigen_real[None, :, :] * step_size[:, :, None]
    magnitude = jnp.exp(decay_log + losses.T[:, :, None])
    rotation = frequency[None, :, :] * step_size[:, :, None]
    scaling = jnp.sqrt(-jnp.expm1(2.0 * decay_log))
    driven = jnp.einsum(
        "tgc,rgpc->rtgp", channels, group_input_matrices, preferred_element_type=jnp.float32
    )
    operands = (
        magnitude * jnp.cos(rotation),
        magnitude * jnp.sin(rotation),
        scaling * driven[0],
        scaling * driven[1],
    )
    flat_operands = tuple((item.reshape(positions, group_list * states) for item in operands))
    scanned = lax.associative_scan(combine_steps, flat_operands, axis=0)
    return tuple((item.reshape(positions, group_list, states) for item in scanned))


def readout(state_real_part, state_imaginary, group_output_matrices, inputs, channel_feedthrough):
    positions = state_real_part.shape[0]
    mapped_result = jnp.einsum(
        "fnx,njx->fnj",
        state_real_part,
        group_output_matrices[0].astype(jnp.float32),
        precision=lax.Precision.HIGHEST,
    )
    mapped_result = mapped_result - jnp.einsum(
        "fnx,njx->fnj",
        state_imaginary,
        group_output_matrices[1].astype(jnp.float32),
        precision=lax.Precision.HIGHEST,
    )
    total = mapped_result.reshape(positions, -1) + channel_feedthrough * inputs.astype(jnp.float32)
    return jax.nn.gelu(total).astype(jnp.bfloat16)


def scaled_rows(values, gain):
    widened = values.astype(jnp.float32)
    factor = lax.rsqrt(jnp.mean(widened * widened, axis=-1, keepdims=True) + eps_norm)
    return (widened * factor * gain).astype(jnp.bfloat16)


def slot_table(block_routes, experts, capacity):
    flat_routes = block_routes.reshape(-1)
    onehot = (flat_routes[:, None] == jnp.arange(experts, dtype=jnp.int32)[None, :]).astype(
        jnp.int32
    )
    earlier_count = jnp.sum((jnp.cumsum(onehot, axis=0) - onehot) * onehot, axis=1)
    return flat_routes * capacity + earlier_count


def fill_slots(token_rows, slot_index, slot_count, top_count):
    owner_row = (
        jnp.zeros((slot_count,), jnp.int32)
        .at[slot_index]
        .set(jnp.arange(slot_index.shape[0], dtype=jnp.int32) // top_count)
    )
    occupied = jnp.zeros((slot_count,), jnp.int32).at[slot_index].set(1)
    return jnp.where(occupied[:, None] > 0, token_rows[owner_row], jnp.zeros((), token_rows.dtype))


def on_device(
    mixer_group_input,
    log_step_size,
    extra_log_decay,
    negated_eigen_real,
    frequency,
    group_input_matrices,
    group_output_matrices,
    channel_feedthrough,
    mixer_norm_scale,
    mixer_output_weight,
    second_micro_input,
    expert_norm_scale,
    routes,
    chosen_expert_weight,
    expert_gate_weight,
    expert_up_weight,
    expert_down_weight,
    shared_gate_weight,
    shared_up_weight,
    shared_down_weight,
):
    reach_real, reach_imag, state_real_part, state_imaginary = local_states(
        mixer_group_input,
        log_step_size,
        extra_log_decay,
        negated_eigen_real,
        frequency,
        group_input_matrices,
    )
    block_ends = (reach_real[-1], reach_imag[-1], state_real_part[-1], state_imaginary[-1])
    identity = (
        jnp.ones_like(block_ends[0]),
        jnp.zeros_like(block_ends[1]),
        jnp.zeros_like(block_ends[2]),
        jnp.zeros_like(block_ends[3]),
    )
    prefix = prefix_2(block_ends, "ep", combine_steps, identity)
    state_real_part = state_real_part + reach_real * prefix[2] - reach_imag * prefix[3]
    state_imaginary = state_imaginary + reach_real * prefix[3] + reach_imag * prefix[2]
    ssm_out = readout(
        state_real_part,
        state_imaginary,
        group_output_matrices,
        mixer_group_input,
        channel_feedthrough,
    )
    whole_rows = whole_of(ssm_out, ("tp_0", "tp_1"), (0, 1), 1)
    normed_mix = scaled_rows(whole_rows, mixer_norm_scale)
    mixed = jnp.dot(normed_mix, mixer_output_weight, preferred_element_type=jnp.float32).astype(
        jnp.bfloat16
    )
    token_count, top_count = routes.shape
    model_width = second_micro_input.shape[1]
    experts = lax.axis_size("ep")
    capacity = 2 * token_count * top_count // experts
    slot_count = experts * capacity
    column_count = expert_down_weight.shape[2]
    gate_weight = expert_gate_weight[0]
    up_weight = expert_up_weight[0]
    down_weight = expert_down_weight[0]
    normed_tokens = scaled_rows(second_micro_input, expert_norm_scale)
    slot_index = slot_table(routes, experts, capacity)
    sent = fill_slots(normed_tokens, slot_index, slot_count, top_count).reshape(
        experts, capacity, model_width
    )
    own_columns = lax.dynamic_slice_in_dim(sent, lax.axis_index(TP) * column_count, column_count, 2)
    arrived = lax.all_to_all(own_columns, "ep", split_axis=0, concat_axis=0, tiled=True).reshape(
        slot_count, column_count
    )
    shard_piece = lax.all_gather(arrived, TP, axis=1, tiled=True)
    gate_part = jnp.dot(shard_piece, gate_weight, preferred_element_type=jnp.float32)
    up_part = jnp.dot(shard_piece, up_weight, preferred_element_type=jnp.float32)
    hidden = (jax.nn.silu(gate_part) * up_part).astype(jnp.bfloat16)
    shared_hidden = (
        jax.nn.silu(jnp.dot(normed_tokens, shared_gate_weight, preferred_element_type=jnp.float32))
        * jnp.dot(normed_tokens, shared_up_weight, preferred_element_type=jnp.float32)
    ).astype(jnp.bfloat16)
    shard_pieces = side_by_side((hidden, shared_hidden), TP, 1, 0)
    routed_columns = jnp.dot(shard_pieces[0], down_weight, preferred_element_type=jnp.float32)
    shared_columns = jnp.dot(
        shard_pieces[1], shared_down_weight, preferred_element_type=jnp.float32
    )
    results = routed_columns.astype(jnp.bfloat16).reshape(experts, capacity, column_count)
    returned = lax.all_to_all(results, "ep", split_axis=0, concat_axis=0, tiled=True).reshape(
        slot_count, column_count
    )
    picked = returned[slot_index].reshape(token_count, top_count, column_count).astype(jnp.float32)
    moe_out = (shared_columns + jnp.sum(picked * chosen_expert_weight[:, :, None], axis=1)).astype(
        jnp.bfloat16
    )
    return (mixed, moe_out)


def solution(mesh):
    finer = Mesh(mesh.devices.reshape(mesh.shape["ep"], 8, 2), ("ep", "tp_0", "tp_1"))
    return jax.shard_map(
        on_device,
        mesh=finer,
        in_specs=(
            P("ep", TP),
            P(TP, "ep"),
            P(TP, "ep"),
            P(TP, None),
            P(TP, None),
            P(None, TP, None, None),
            P(None, TP, None, None),
            P(TP),
            P(),
            P(None, TP),
            P("ep", None),
            P(),
            P("ep", None),
            P("ep", None),
            P("ep", None, TP),
            P("ep", None, TP),
            P("ep", None, TP),
            P(None, TP),
            P(None, TP),
            P(None, TP),
        ),
        out_specs=(P("ep", TP), P("ep", TP)),
        check_vma=False,
    )
```

profile of v0, /device:TPU:1, one launch (start us, length us, event | category | flops | bytes accessed | tf_op | source)
XLA Modules:
  0.0 518.2 jit_solution(16124263375213225293)
XLA Ops:
  18.3 6.0 %gather_fusion = bf16[1024,2048]{1,0:T(8,128)(2,1)} fusion(bf16[128,2048]{1,0:T(8,128)(2,1)S(1)} %fusion.10, s32[1024]{0:T(1024)S(1)} %fusion.81), kind=kCustom, calls=%fused_computation | custom fusion | bytes 8392704 | tf_op jit(solution)/shard_map/gather | solution.py:158
  25.5 24.9 %all_to_all.15 = bf16[32,32,128]{2,1,0:T(8,128)(2,1)} all-to-all(bf16[32,32,128]{2,1,0:T(8,128)(2,1)S(1)} %dynamic-slice_select_fusion), channel_id=1, replica_groups=mesh['ep'=32,'tp_0'=8,'tp_1'=2] {'ep'}, dimensions={0} | all-to-all | bytes 524288 | tf_op jit(solution)/shard_map/all_to_all | solution.py:228
  53.8 4.5 slice.643
  58.3 4.5 slice.647
  62.8 4.5 slice.642
  67.3 4.5 slice.649
  71.8 4.5 slice.644
  76.3 4.5 slice.650
  80.8 4.7 slice.646
  85.5 4.5 slice.655
  196.6 5.9 %slice.641 = f32[127,256]{0,1:T(8,128)} slice(f32[256,256]{0,1:T(8,128)} %copy-done.14), slice={[2:256:2], [0:256:1]} | slice | bytes 260096 | tf_op jit(solution)/shard_map/slice | solution.py:114
  202.6 5.9 %slice.752 = f32[127,256]{0,1:T(8,128)} slice(f32[256,256]{0,1:T(8,128)} %copy-done.13), slice={[2:256:2], [0:256:1]} | slice | bytes 260096 | tf_op jit(solution)/shard_map/slice | solution.py:114
  208.5 5.9 %slice.756 = f32[127,256]{0,1:T(8,128)} slice(f32[256,256]{0,1:T(8,128)} %copy-done.12), slice={[2:256:2], [0:256:1]} | slice | bytes 260096 | tf_op jit(solution)/shard_map/slice | solution.py:114
  214.4 6.1 %slice.794 = f32[127,256]{0,1:T(8,128)} slice(f32[256,256]{0,1:T(8,128)} %copy-done.11), slice={[2:256:2], [0:256:1]} | slice | bytes 260096 | tf_op jit(solution)/shard_map/slice | solution.py:114
  374.6 4.8 pad.258
  379.3 5.3 %pad.259 = f32[256,256]{0,1:T(8,128)S(1)} pad(f32[128,256]{0,1:T(8,128)} %add.629, f32[]{:T(128)} %constant.24.clone.1), padding=1_0_1x0_0_0 | pad | bytes 393220 | tf_op jit(solution)/shard_map/pad | solution.py:114
  413.6 4.8 pad.254
  423.2 4.4 pad.256
  427.8 4.5 pad.225
  438.3 4.8 all-to-all-start
  443.4 9.0 %all-to-all-done = f32[32,1,1024]{2,1,0:T(1,128)S(1)} async-done(((f32[32,1,1024]{2,1,0:T(1,128)}), f32[32,1,1024]{2,1,0:T(1,128)S(1)}, u32[]{:S(2)}, u32[]{:S(2)}) %all-to-all-start) | async-done | bytes 131104 | tf_op jit(solution)/shard_map/all_to_all | solution.py:15
  455.1 20.5 %all-gather = bf16[2048,64]{0,1:T(8,128)(2,1)S(1)} all-gather(bf16[256,64]{0,1:T(8,128)(2,1)S(1)} %fusion.55), channel_id=2, replica_groups=mesh['ep'=32,'tp_0'=8,'tp_1'=2] {'tp_0'}, dimensions={0}, use_global_device_ids=true | all-gather | bytes 294912 | tf_op jit(solution)/shard_map/all_gather | solution.py:66
  475.7 10.8 %all_gather.13 = bf16[16,256,64]{1,0,2:T(8,128)(2,1)S(1)} all-gather(bf16[8,256,64]{1,0,2:T(8,128)(2,1)S(1)} %bitcast.204), channel_id=1, replica_groups=mesh['ep'=32,'tp_0'=8,'tp_1'=2] {'tp_1'}, dimensions={0}, use_global_device_ids=true | all-gather | bytes 786432 | tf_op jit(solution)/shard_map/all_gather | solution.py:66
  497.0 10.6 %all-to-all-done.2 = bf16[32,32,128]{2,1,0:T(8,128)(2,1)S(1)} async-done(((bf16[32,32,128]{2,1,0:T(8,128)(2,1)}), bf16[32,32,128]{2,1,0:T(8,128)(2,1)S(1)}, u32[]{:S(2)}, u32[]{:S(2)}) %all-to-all-start.2) | async-done | bytes 262176 | tf_op jit(solution)/shard_map/all_to_all | solution.py:245
  (454 shorter events, 332.1 us)
Async XLA Ops:
  7.2 328.8 %copy-start = (bf16[1,2048,128]{2,1,0:T(8,128)(2,1)S(1)}, bf16[1,2048,128]{2,1,0:T(8,128)(2,1)}, u32[]{:S(2)}) copy-start(bf16[1,2048,128]{2,1,0:T(8,128)(2,1)} %param.34) | copy-start | bytes 1572868
  7.2 328.8 %all-gather.4.cloned.1.call-start = ((), (), s32[]{:S(2)}) async-start(), calls=%async_computation.3 | async-start | bytes 4456448 | tf_op jit(solution)/shard_map/all_gather | solution.py:231
  18.3 32.7 %copy-start.50 = (f32[4,64]{1,0:T(4,128)S(1)}, f32[4,64]{1,0:T(4,128)}, u32[]{:S(2)}) copy-start(f32[4,64]{1,0:T(4,128)} %param.23) | copy-start | bytes 3076
  18.3 32.8 %copy-start.43 = (f32[4,64]{1,0:T(4,128)S(1)}, f32[4,64]{1,0:T(4,128)}, u32[]{:S(2)}) copy-start(f32[4,64]{1,0:T(4,128)} %param.24) | copy-start | bytes 3076
  18.3 32.9 %copy-start.48 = (f32[4,256]{1,0:T(4,128)S(1)}, f32[4,256]{1,0:T(4,128)}, u32[]{:S(2)}) copy-start(f32[4,256]{1,0:T(4,128)} %param.21) | copy-start | bytes 12292
  18.3 32.9 %copy-start.36 = (bf16[256,64]{0,1:T(8,128)(2,1)S(1)}, bf16[256,64]{0,1:T(8,128)(2,1)}, u32[]{:S(2)}) copy-start(bf16[256,64]{0,1:T(8,128)(2,1)} %param.20) | copy-start | bytes 98308
  18.3 32.9 %copy-start.39 = (bf16[2,4,64,16]{2,3,1,0:T(8,128)(2,1)S(1)}, bf16[2,4,64,16]{2,3,1,0:T(8,128)(2,1)}, u32[]{:S(2)}) copy-start(bf16[2,4,64,16]{2,3,1,0:T(8,128)(2,1)} %param.25) | copy-start | bytes 49156
  18.3 34.0 %copy-start.41 = (f32[4,256]{1,0:T(4,128)S(1)}, f32[4,256]{1,0:T(4,128)}, u32[]{:S(2)}) copy-start(f32[4,256]{1,0:T(4,128)} %param.22) | copy-start | bytes 12292
  50.4 437.1 %all-gather.6.cloned.1.call-start = ((), (), s32[]{:S(2)}) async-start(), calls=%async_computation.4 | async-start | bytes 5013504 | tf_op jit(solution)/shard_map/all_gather | solution.py:83
  53.7 31.7 %copy-start.11 = (f32[256,256]{0,1:T(8,128)}, f32[256,256]{0,1:T(8,128)S(1)}, u32[]{:S(2)}) copy-start(f32[256,256]{0,1:T(8,128)S(1)} %get-tuple-element.168) | copy-start | bytes 786436
  53.8 31.7 %copy-start.12 = (f32[256,256]{0,1:T(8,128)}, f32[256,256]{0,1:T(8,128)S(1)}, u32[]{:S(2)}) copy-start(f32[256,256]{0,1:T(8,128)S(1)} %get-tuple-element.169) | copy-start | bytes 786436
  53.8 52.7 %copy-start.13 = (f32[256,256]{0,1:T(8,128)}, f32[256,256]{0,1:T(8,128)S(1)}, u32[]{:S(2)}) copy-start(f32[256,256]{0,1:T(8,128)S(1)} %get-tuple-element.171) | copy-start | bytes 786436
  53.8 60.5 %copy-start.14 = (f32[256,256]{0,1:T(8,128)}, f32[256,256]{0,1:T(8,128)S(1)}, u32[]{:S(2)}) copy-start(f32[256,256]{0,1:T(8,128)S(1)} %get-tuple-element.170) | copy-start | bytes 786436
  228.0 27.1 %copy-start.8 = (f32[2,256]{0,1:T(8,128)S(1)}, f32[2,256]{0,1:T(8,128)}, u32[]{:S(2)}) copy-start(f32[2,256]{0,1:T(8,128)} %copy-done.7) | copy-start | bytes 6148
  250.4 41.1 %copy-start.6 = (f32[8,256]{0,1:T(8,128)S(1)}, f32[8,256]{0,1:T(8,128)}, u32[]{:S(2)}) copy-start(f32[8,256]{0,1:T(8,128)} %copy-done.5) | copy-start | bytes 24580
  257.0 45.8 %copy-start.4 = (f32[8,256]{0,1:T(8,128)S(1)}, f32[8,256]{0,1:T(8,128)}, u32[]{:S(2)}) copy-start(f32[8,256]{0,1:T(8,128)} %copy-done.3) | copy-start | bytes 24580
  292.2 31.0 %copy-start.15 = (f32[8,256]{0,1:T(8,128)S(1)}, f32[8,256]{0,1:T(8,128)}, u32[]{:S(2)}) copy-start(f32[8,256]{0,1:T(8,128)} %pad.236) | copy-start | bytes 24580
  399.9 28.0 %copy-start.31 = (f32[128,256]{0,1:T(8,128)S(1)}, f32[128,256]{0,1:T(8,128)}, u32[]{:S(2)}) copy-start(f32[128,256]{0,1:T(8,128)} %add.626) | copy-start | bytes 393220
  413.5 29.8 %copy-start.49 = (f32[128,4]{0,1:T(4,128)S(1)}, f32[128,4]{0,1:T(4,128)}, u32[]{:S(2)}) copy-start(f32[128,4]{0,1:T(4,128)} %param.33) | copy-start | bytes 6148
  413.5 29.9 %copy-start.46 = (s32[512,1]{0,1:T(1,128)S(1)}, s32[512,1]{0,1:T(1,128)}, u32[]{:S(2)}) copy-start(s32[512,1]{0,1:T(1,128)} %copy-done.45) | copy-start | bytes 6148
  423.2 31.1 %copy-start.38 = (bf16[2,4,16,64]{3,2,1,0:T(8,128)(2,1)S(1)}, bf16[2,4,16,64]{3,2,1,0:T(8,128)(2,1)}, u32[]{:S(2)}) copy-start(bf16[2,4,16,64]{3,2,1,0:T(8,128)(2,1)} %param.26) | copy-start | bytes 49156
  438.3 14.1 %all-to-all-start = ((f32[32,1,1024]{2,1,0:T(1,128)}), f32[32,1,1024]{2,1,0:T(1,128)S(1)}, u32[]{:S(2)}, u32[]{:S(2)}) async-start(f32[32,1,1024]{2,1,0:T(1,128)} %reshape.246), calls=%async_computation | async-start | bytes 262144 | tf_op jit(solution)/shard_map/all_to_all | solution.py:15
  455.1 32.5 %copy-start.52 = (bf16[1,2048,128]{2,1,0:T(8,128)(2,1)S(1)}, bf16[1,2048,128]{2,1,0:T(8,128)(2,1)}, u32[]{:S(2)}) copy-start(bf16[1,2048,128]{2,1,0:T(8,128)(2,1)} %param.36) | copy-start | bytes 1572868
  491.8 15.8 %all-to-all-start.2 = ((bf16[32,32,128]{2,1,0:T(8,128)(2,1)}), bf16[32,32,128]{2,1,0:T(8,128)(2,1)S(1)}, u32[]{:S(2)}, u32[]{:S(2)}) async-start(bf16[32,32,128]{2,1,0:T(8,128)(2,1)} %bitcast.40), calls=%async_computation.2 | async-start | bytes 524288 | tf_op jit(solution)/shard_map/all_to_all | solution.py:245
  (33 other events, 342.4 us)
Sparse Core Ops, SparseCore 0:
  50.6 50.1 all-gather.3
  342.9 52.4 all-gather.5
where the time goes:
time: 525 us; the launch traced here: 518 us
  local copies, waits for them, and re-layouts  336 us (64%)
  other arithmetic  64 us (12%)
  blocking collectives  56.2 us (11%)
  waiting for transfers between devices  19.6 us (4%)
  matrix products  17.2 us (3%)
  between operations  16 us (3%)
  starting transfers between devices  9.3 us (2%)
    slice x81, local copies, waits for them, and re-layouts, local_states(): scanned = lax.associative_scan(combine_steps, flat_operands, axis=0)  162 us
    pad x56, local copies, waits for them, and re-layouts, local_states(): scanned = lax.associative_scan(combine_steps, flat_operands, axis=0)  109 us
    all_gather x2, blocking collectives, all_blocks(): tiles = lax.all_gather(tiles, axes[k], axis=0, tiled=True)  31.3 us
    all_to_all x1, blocking collectives, on_device(): lax.all_to_all(own_columns, 'ep', split_axis=0, concat_axis=0, tiled=True)  24.9 us
    add x30, other arithmetic, local_states(): scanned = lax.associative_scan(combine_steps, flat_operands, axis=0)  20.5 us
    unnamed x129, local copies, waits for them, and re-layouts  20 us
    add x15, other arithmetic, combine_steps(): latter[0] * earlier[3] + latter[1] * earlier[2] + latter[3]  14 us
    all_to_all x1, waiting for transfers between devices, on_device(): lax.all_to_all(results, 'ep', split_axis=0, concat_axis=0, tiled=True)  10.6 us
  transfers between devices with their start and end apart: 4, of which 2 were waited for; matrix products, arithmetic and copies ran while one was open for 74% of the time, Pallas kernels for 0%

commit v1 on v0

v1 whole, which is shorter than its diff:
```python
import jax
import jax.numpy as jnp
from jax import lax
from jax.experimental import pallas as pl
from jax.experimental.pallas import tpu as pltpu
from jax.sharding import Mesh
from jax.sharding import PartitionSpec as P

VM = pltpu.VMEM
F32, BF16 = jnp.float32, jnp.bfloat16
NT = (((1,), (1,)), ((), ()))
EPS = 1e-06
CHUNKS = 8


def iota(shape, dim):
    return lax.broadcasted_iota(jnp.int32, shape, dim)


def vmem(count):
    return [pl.BlockSpec(memory_space=VM)] * count


def sin_cos(x):
    turns = jnp.floor(x * 0.6366197723675814 + 0.5)
    r = x - turns * 1.5703125
    r = r - turns * 4.837512969970703e-4
    r = r - turns * 7.54978995489188e-8
    q = turns.astype(jnp.int32)
    s = r * r
    sin_r = r + r * s * (-1.6666654611e-1 + s * (8.3321608736e-3 - s * 1.9515295891e-4))
    cos_r = 1.0 - 0.5 * s + s * s * (
        4.166664568298827e-2 + s * (-1.388731625493765e-3 + s * 2.443315711809948e-5)
    )
    odd = (q & 1) == 1
    a = jnp.where(odd, cos_r, sin_r)
    b = jnp.where(odd, sin_r, cos_r)
    sin_x = jnp.where((q & 2) == 2, -a, a)
    cos_x = jnp.where(((q + 1) & 2) == 2, -b, b)
    return sin_x, cos_x


def minus_expm1(y):
    small = 1.0 + y * (1.0 / 9.0)
    for n in (8, 7, 6, 5, 4, 3, 2):
        small = 1.0 + y * (1.0 / n) * small
    return jnp.where(y > -0.5, -y * small, 1.0 - jnp.exp(y))


def scan_kernel(x_ref, steps_ref, eig_ref, freq_ref, win_ref, p_re, p_im, h_re, h_im, ends_ref,
                a_re, a_im, d_re, d_im):
    positions, width = x_ref.shape
    groups = steps_ref.shape[1] // 2
    states = eig_ref.shape[1] // groups
    lanes = 128
    per = lanes // states
    channels = width // groups
    spread = (iota((channels, width), 1) % channels == iota((channels, width), 0)).astype(BF16)
    wide = jnp.dot(win_ref[...], spread, preferred_element_type=F32)
    rows = iota(wide.shape, 0) // states % groups
    wide = jnp.where(rows == iota(wide.shape, 1) // channels, wide, 0.0).astype(BF16)
    driven = lax.dot_general(x_ref[...], wide, NT, preferred_element_type=F32)
    half = groups * states
    for tile in range(half // lanes):
        at = slice(tile * lanes, (tile + 1) * lanes)
        place = iota((positions, lanes), 1) // states
        step = jnp.broadcast_to(steps_ref[:, tile * per : tile * per + 1], (positions, lanes))
        loss = jnp.broadcast_to(
            steps_ref[:, groups + tile * per : groups + tile * per + 1], (positions, lanes)
        )
        for k in range(1, per):
            g = tile * per + k
            step = jnp.where(place == k, steps_ref[:, g : g + 1], step)
            loss = jnp.where(place == k, steps_ref[:, groups + g : groups + g + 1], loss)
        decay_log = -eig_ref[:, at] * step
        magnitude = jnp.exp(decay_log + loss)
        sin_x, cos_x = sin_cos(freq_ref[:, at] * step)
        scaling = jnp.sqrt(minus_expm1(2.0 * decay_log))
        a_re[tile] = magnitude * cos_x
        a_im[tile] = magnitude * sin_x
        d_re[tile] = scaling * driven[:, at]
        d_im[tile] = scaling * driven[:, half + tile * lanes : half + (tile + 1) * lanes]
    length = positions // CHUNKS
    ends = []
    for tile in range(half // lanes):
        at = slice(tile * lanes, (tile + 1) * lanes)
        for j in range(length):
            take = pl.ds(j, CHUNKS, stride=length)
            ar, ai = a_re[tile, take, :], a_im[tile, take, :]
            dr, di = d_re[tile, take, :], d_im[tile, take, :]
            if j == 0:
                pr, pi, hr, hi = ar, ai, dr, di
            else:
                pr, pi = pr * ar - pi * ai, pr * ai + pi * ar
                hr, hi = ar * hr - ai * hi + dr, ar * hi + ai * hr + di
            p_re[j, :, at], p_im[j, :, at] = pr, pi
            h_re[j, :, at], h_im[j, :, at] = hr, hi
        er, ei, sr, si = pr[0:1], pi[0:1], hr[0:1], hi[0:1]
        for c in range(1, CHUNKS):
            ar, ai = pr[c : c + 1], pi[c : c + 1]
            er, ei = er * ar - ei * ai, er * ai + ei * ar
            sr, si = ar * sr - ai * si + hr[c : c + 1], ar * si + ai * sr + hi[c : c + 1]
        ends += [er, ei, sr, si]
    packed = jnp.concatenate(ends, axis=0)
    for b in range(ends_ref.shape[0]):
        ends_ref[b] = packed


def run_scan(x, steps, eig, freq, win, blocks):
    positions = x.shape[0]
    half = eig.shape[1]
    piece = jax.ShapeDtypeStruct((positions // CHUNKS, CHUNKS, half), F32)
    return pl.pallas_call(
        scan_kernel,
        out_shape=[piece] * 4 + [jax.ShapeDtypeStruct((blocks, half // 32, 128), F32)],
        in_specs=vmem(5),
        out_specs=vmem(5),
        scratch_shapes=[VM((half // 128, positions, 128), F32)] * 4,
        name="scan",
    )(x, steps, eig, freq, win)


def readout_kernel(where_ref, p_re, p_im, h_re, h_im, ends_ref, x_ref, wout_ref, feed_ref, out_ref,
                   turned):
    length, chunks, half = p_re.shape
    positions, width = x_ref.shape
    states = wout_ref.shape[1]
    channels = wout_ref.shape[0] // 2 // (half // states)
    index = where_ref[0]
    cr = ci = jnp.zeros((1, half), F32)
    for b in range(ends_ref.shape[0] - 1):
        end = ends_ref[b]
        ar, ai, er, ei = (
            jnp.concatenate([end[q : q + 1], end[q + 4 : q + 5]], axis=1) for q in range(4)
        )
        nr = ar * cr - ai * ci + er
        ni = ar * ci + ai * cr + ei
        keep = b < index
        cr, ci = jnp.where(keep, nr, cr), jnp.where(keep, ni, ci)
    carry_r, carry_i = [cr], [ci]
    for c in range(chunks - 1):
        ar, ai = p_re[length - 1, c : c + 1, :], p_im[length - 1, c : c + 1, :]
        cr, ci = (
            ar * cr - ai * ci + h_re[length - 1, c : c + 1, :],
            ar * ci + ai * cr + h_im[length - 1, c : c + 1, :],
        )
        carry_r.append(cr)
        carry_i.append(ci)
    cr = jnp.concatenate(carry_r, axis=0)[None]
    ci = jnp.concatenate(carry_i, axis=0)[None]
    sr = (h_re[...] + p_re[...] * cr - p_im[...] * ci).reshape(positions, half)
    si = (h_im[...] + p_re[...] * ci + p_im[...] * cr).reshape(positions, half)
    spread = (iota((states, half), 1) % states == iota((states, half), 0)).astype(BF16)
    wide = jnp.dot(wout_ref[...], spread, preferred_element_type=F32)
    rows = iota(wide.shape, 0) % width // channels
    wide = jnp.where(rows == iota(wide.shape, 1) // states, wide, 0.0)
    wr, wi = wide[:width].astype(BF16), (-wide[width:]).astype(BF16)
    nothing = jnp.zeros((128 - width, half), BF16)
    wr, wi = (jnp.concatenate([w, nothing], axis=0) for w in (wr, wi))
    total = None
    for state, w in ((sr, wr), (si, wi)):
        high = state.astype(BF16)
        low = (state - high.astype(F32)).astype(BF16)
        for part in (high, low):
            got = lax.dot_general(part, w, NT, preferred_element_type=F32)
            total = got if total is None else total + got
    for j in range(length):
        turned[pl.ds(j, chunks, stride=length), :] = total[j * chunks : (j + 1) * chunks]
    v = turned[:, :width] + feed_ref[...] * x_ref[...].astype(F32)
    v = 0.5 * v * (1.0 + jnp.tanh(0.7978845608028654 * (v + 0.044715 * (v * v * v))))
    both = positions // 2
    out_ref[...] = jnp.concatenate([v[:both], v[both:]], axis=1).astype(BF16)


def run_readout(index, pieces, ends, x, wout, feed):
    positions, width = x.shape
    return pl.pallas_call(
        readout_kernel,
        out_shape=jax.ShapeDtypeStruct((positions // 2, 2 * width), BF16),
        in_specs=[pl.BlockSpec(memory_space=pltpu.SMEM)] + vmem(8),
        out_specs=pl.BlockSpec(memory_space=VM),
        scratch_shapes=[VM((positions, 128), F32)],
        name="readout",
    )(index, *pieces, ends, x, wout, feed)


def mixed_kernel(rows_ref, scale_ref, w_ref, out_ref):
    blocks, both, lanes = rows_ref.shape
    width = lanes // 2
    total = None
    for d in range(blocks):
        v = rows_ref[d].astype(F32)
        total = v * v if total is None else total + v * v
    first = iota((both, lanes), 1) < width
    count = 1.0 / (blocks * width)
    sums = [jnp.sum(jnp.where(m, total, 0.0), axis=1, keepdims=True) for m in (first, ~first)]
    f0, f1 = (lax.rsqrt(s * count + EPS) for s in sums)
    factor = jnp.where(first, f0, f1)
    acc = [jnp.zeros((both, w_ref.shape[1]), F32)] * 2
    for d in range(blocks):
        gain = jnp.concatenate([scale_ref[d : d + 1, :]] * 2, axis=1)
        v = (rows_ref[d].astype(F32) * factor * gain).astype(BF16)
        w = w_ref[d * width : (d + 1) * width, :]
        w2 = jnp.concatenate([w, w], axis=0)
        for k, m in enumerate((first, ~first)):
            part = jnp.where(m, v, jnp.zeros_like(v))
            acc[k] = acc[k] + jnp.dot(part, w2, preferred_element_type=F32)
    out_ref[:both, :] = acc[0].astype(BF16)
    out_ref[both:, :] = acc[1].astype(BF16)


def run_mixed(rows, scale, w):
    blocks, both, lanes = rows.shape
    return pl.pallas_call(
        mixed_kernel,
        out_shape=jax.ShapeDtypeStruct((2 * both, w.shape[1]), BF16),
        in_specs=vmem(3),
        out_specs=pl.BlockSpec(memory_space=VM),
        name="mixed",
    )(rows, scale.reshape(blocks, lanes // 2), w)


def mixer_local(x, log_step, loss, eig, freq, win, blocks):
    steps = jnp.concatenate([jnp.exp(log_step), loss], axis=0).T
    return run_scan(x, steps, eig.reshape(1, -1), freq.reshape(1, -1),
                    win.reshape(-1, win.shape[-1]), blocks)


def expert_table(routes_ref, weights_ref, experts):
    top, tokens = routes_ref.shape
    expert = iota((experts, tokens), 0)
    named = jnp.zeros((experts, tokens), F32)
    gain = jnp.zeros((experts, tokens), F32)
    for k in range(top):
        hit = routes_ref[k : k + 1, :] == expert
        named = jnp.where(hit, 1.0, named)
        if weights_ref is not None:
            gain = jnp.where(hit, weights_ref[k : k + 1, :], gain)
    earlier = (iota((tokens, tokens), 0) < iota((tokens, tokens), 1)).astype(BF16)
    rank = jnp.dot(named.astype(BF16), earlier, preferred_element_type=F32)
    return jnp.where(named > 0.0, rank, -1.0), gain


def dispatch_kernel(where_ref, tokens_ref, gain_ref, routes_ref, normed_ref, sent_ref):
    tokens = tokens_ref.shape[0]
    v = tokens_ref[...].astype(F32)
    factor = lax.rsqrt(jnp.mean(v * v, axis=1, keepdims=True) + EPS)
    normed = (v * factor * gain_ref[...]).astype(BF16)
    normed_ref[...] = normed
    share = 8
    experts = sent_ref.shape[0] // share
    rank, _ = expert_table(routes_ref, None, experts)
    slot = (iota((share, tokens), 0) + where_ref[0] * share).astype(F32)
    chosen = jnp.concatenate(
        [jnp.where(rank[e : e + 1, :] == slot, 1.0, 0.0) for e in range(experts)], axis=0
    ).astype(BF16)
    sent_ref[...] = jnp.dot(chosen, normed, preferred_element_type=F32).astype(BF16)


def run_dispatch(where, tokens, gain, routes, rows):
    return pl.pallas_call(
        dispatch_kernel,
        out_shape=[
            jax.ShapeDtypeStruct(tokens.shape, BF16),
            jax.ShapeDtypeStruct((rows, tokens.shape[1]), BF16),
        ],
        in_specs=[pl.BlockSpec(memory_space=pltpu.SMEM)] + vmem(3),
        out_specs=vmem(2),
        name="dispatch",
    )(where, tokens, gain.reshape(1, -1), routes)


def choice_kernel(routes_ref, weights_ref, high_ref, low_ref):
    tokens = routes_ref.shape[1]
    share, parts = 8, 4
    experts = high_ref.shape[1] // (share * parts)
    rank, gain = expert_table(routes_ref, weights_ref, experts)
    for a in range(parts):
        slot = (iota((share, tokens), 0) + a * share).astype(F32)
        picked = jnp.concatenate(
            [
                jnp.where(rank[e : e + 1, :] == slot, gain[e : e + 1, :], 0.0)
                for e in range(experts)
            ],
            axis=0,
        ).T
        high = picked.astype(BF16)
        at = slice(a * experts * share, (a + 1) * experts * share)
        high_ref[:, at] = high
        low_ref[:, at] = (picked - high.astype(F32)).astype(BF16)


def run_choice(routes, weights, slots):
    return pl.pallas_call(
        choice_kernel,
        out_shape=[jax.ShapeDtypeStruct((routes.shape[1], slots), BF16)] * 2,
        in_specs=vmem(2),
        out_specs=vmem(2),
        name="choice",
    )(routes, weights)


def gated(rows, both):
    got = jnp.dot(rows, both, preferred_element_type=F32)
    half = both.shape[1] // 2
    gate, up = got[:, :half], got[:, half:]
    return (gate / (1.0 + jnp.exp(-gate)) * up).astype(BF16)


def hidden_kernel(rows_ref, *refs):
    *weights, out_ref = refs
    rows = rows_ref[...]
    for q, w in enumerate(weights):
        half = w.shape[1] // 2
        got = gated(rows, w[...])
        for copy in range(out_ref.shape[0]):
            out_ref[copy, :, q * half : (q + 1) * half] = got


def run_hidden(rows, weights, copies):
    half = weights[0].shape[1] // 2
    return pl.pallas_call(
        hidden_kernel,
        out_shape=jax.ShapeDtypeStruct((copies, rows.shape[0], half * len(weights)), BF16),
        in_specs=vmem(1 + len(weights)),
        out_specs=pl.BlockSpec(memory_space=VM),
        name="hidden",
    )(rows, *weights)


def down_kernel(where_ref, *refs):
    hidden, weights, out_ref, whole = refs[0], refs[1:5], refs[5], refs[6]
    sub = where_ref[0]
    lanes = weights[0].shape[1]
    for member in range(hidden.shape[0]):
        for q in range(4):
            at = pl.multiple_of((member * 4 + (sub ^ q)) * lanes, lanes)
            whole[:, pl.ds(at, lanes)] = hidden[member, :, q * lanes : (q + 1) * lanes]
    rows = whole[...]
    for q in (0, 2):
        both = jnp.concatenate([weights[q][...], weights[q + 1][...]], axis=1)
        got = jnp.dot(rows, both, preferred_element_type=F32).astype(BF16)
        out_ref[sub ^ q] = got[:, :lanes]
        out_ref[sub ^ (q + 1)] = got[:, lanes:]


def run_down(where, hidden, weights):
    rows, lanes = hidden.shape[1], weights[0].shape[1]
    return pl.pallas_call(
        down_kernel,
        out_shape=jax.ShapeDtypeStruct((4, rows, lanes), BF16),
        in_specs=[pl.BlockSpec(memory_space=pltpu.SMEM)] + vmem(5),
        out_specs=pl.BlockSpec(memory_space=VM),
        scratch_shapes=[VM((rows, weights[0].shape[0]), BF16)],
        name="down",
    )(where, hidden, *weights)


def shared_kernel(blocks_ref, w_ref, out_ref):
    blocks, tokens, lanes = blocks_ref.shape
    total = jnp.zeros((tokens, w_ref.shape[1]), F32)
    for d in range(blocks):
        total = total + jnp.dot(
            blocks_ref[d], w_ref[d * lanes : (d + 1) * lanes, :], preferred_element_type=F32
        )
    out_ref[...] = total


def run_shared(blocks, w):
    return pl.pallas_call(
        shared_kernel,
        out_shape=jax.ShapeDtypeStruct((blocks.shape[1], w.shape[1]), F32),
        in_specs=vmem(2),
        out_specs=pl.BlockSpec(memory_space=VM),
        name="shared",
    )(blocks, w)


def combine_kernel(shared_ref, back_ref, high_ref, low_ref, out_ref):
    back = back_ref[...]
    total = shared_ref[...]
    for part in (high_ref, low_ref):
        total = total + jnp.dot(part[...], back, preferred_element_type=F32)
    out_ref[...] = total.astype(BF16)


def run_combine(shared, back, high, low):
    return pl.pallas_call(
        combine_kernel,
        out_shape=jax.ShapeDtypeStruct(shared.shape, BF16),
        in_specs=vmem(4),
        out_specs=pl.BlockSpec(memory_space=VM),
        name="combine",
    )(shared, back, high, low)


TP = ("yh", "yl", "co")
SWAP = [(0, 1), (1, 0)]


def exchanged(piece):
    over = lax.ppermute(piece, "yl", SWAP)
    return (piece, lax.ppermute(piece, "co", SWAP), over, lax.ppermute(over, "co", SWAP))


def spread_out(pieces, axes):
    return lax.all_to_all(pieces, axes, split_axis=0, concat_axis=0, tiled=True)


def on_device(
    mixer_group_input,
    log_step_size,
    extra_log_decay,
    negated_eigen_real,
    frequency,
    group_input_matrices,
    group_output_matrices,
    channel_feedthrough,
    mixer_norm_scale,
    mixer_output_weight,
    second_micro_input,
    expert_norm_scale,
    routes,
    chosen_expert_weight,
    expert_gate_weight,
    expert_up_weight,
    expert_down_weight,
    shared_gate_weight,
    shared_up_weight,
    shared_down_weight,
):
    blocks = lax.axis_size("ep")
    tokens, width = second_micro_input.shape
    sub = 2 * lax.axis_index("yl") + lax.axis_index("co")
    where = jnp.stack([sub, lax.axis_index("ep")]).astype(jnp.int32)
    routes = routes.T
    gates = exchanged(jnp.concatenate([expert_gate_weight[0], expert_up_weight[0]], axis=1))
    normed, sent = run_dispatch(where, second_micro_input, expert_norm_scale, routes, blocks * 8)
    arrived = spread_out(sent.reshape(blocks, 8, width), "ep").reshape(blocks * 8, width)
    downs = exchanged(expert_down_weight[0])

    *pieces, ends = mixer_local(
        mixer_group_input,
        log_step_size,
        extra_log_decay,
        negated_eigen_real,
        frequency,
        group_input_matrices,
        blocks,
    )
    ends = spread_out(ends, "ep")
    ssm_out = run_readout(
        where[1:],
        pieces,
        ends,
        mixer_group_input,
        group_output_matrices.reshape(-1, group_output_matrices.shape[-1]),
        channel_feedthrough.reshape(1, -1),
    )
    whole_rows = lax.all_gather(ssm_out, TP, axis=0)
    mixed = run_mixed(whole_rows, mixer_norm_scale, mixer_output_weight)

    shared_gates = jnp.concatenate([shared_gate_weight, shared_up_weight], axis=1)
    shared_hidden = run_hidden(normed, [shared_gates], 1)[0]
    shared = run_shared(lax.all_gather(shared_hidden, TP, axis=0), shared_down_weight)
    high, low = run_choice(routes, chosen_expert_weight.T, blocks * 32)

    hidden = run_hidden(arrived, gates, lax.axis_size("yh"))
    hidden = spread_out(hidden, "yh")
    results = run_down(where, hidden, downs)
    results = results.reshape(4 * blocks, 8, -1)
    back = spread_out(results, ("yl", "co", "ep")).reshape(blocks * 32, -1)
    return (mixed, run_combine(shared, back, high, low))


def solution(mesh):
    finer = Mesh(
        mesh.devices.reshape(mesh.shape["ep"], mesh.shape["tp"] // 4, 2, 2), ("ep", *TP)
    )
    return jax.shard_map(
        on_device,
        mesh=finer,
        in_specs=(
            P("ep", TP),
            P(TP, "ep"),
            P(TP, "ep"),
            P(TP, None),
            P(TP, None),
            P(None, TP, None, None),
            P(None, TP, None, None),
            P(TP),
            P(),
            P(None, TP),
            P("ep", None),
            P(),
            P("ep", None),
            P("ep", None),
            P("ep", None, TP),
            P("ep", None, TP),
            P("ep", None, TP),
            P(None, TP),
            P(None, TP),
            P(None, TP),
        ),
        out_specs=(P("ep", TP), P("ep", TP)),
        check_vma=False,
    )
```

time: 525 us -> 184 us (0.35); the launches traced: 518 us -> 183 us
  local copies, waits for them, and re-layouts: 336 us -> 5.98 us
  other arithmetic: 64 us -> 3.06 us
  starting transfers between devices: 9.3 us -> 59 us
  waiting for transfers between devices: 19.6 us -> 48 us
  Pallas kernels: 0 us -> 28 us
  blocking collectives: 56.2 us -> 38.5 us
  matrix products: 17.2 us -> 0 us
  between operations: 16 us -> 0.89 us
    slice x82 -> x0, local copies, waits for them, and re-layouts: 162 us -> none  [the longest x81 162 us: local_states(): scanned = lax.associative_scan(combine_steps, flat_operands, axis=0)]
    pad x56 -> x0, local copies, waits for them, and re-layouts: 109 us -> none  [local_states(): scanned = lax.associative_scan(combine_steps, flat_operands, axis=0)]
    add x55 -> x0, other arithmetic: 36 us -> none  [the longest x30 20.5 us: local_states(): scanned = lax.associative_scan(combine_steps, flat_operands, axis=0)]
    pallas_call x0 -> x10, Pallas kernels: none -> 28 us  [the longest x2 7.1 us: run_hidden(): pl.pallas_call(hidden_kernel, out_shape=jax.ShapeDtypeStruct((copies, row...]
    ppermute x0 -> x6, starting transfers between devices: none -> 26.9 us  [the longest x2 11.4 us: exchanged(): lax.ppermute(over, 'co', SWAP)]
    ppermute x0 -> x6, waiting for transfers between devices: none -> 25.4 us  [the longest x2 25.4 us: exchanged(): over = lax.ppermute(piece, 'yl', SWAP)]
    all_to_all x1 -> x0, blocking collectives: 24.9 us -> none  [on_device(): lax.all_to_all(own_columns, 'ep', split_axis=0, concat_axis=0, tiled=True)]
    mul x28 -> x0, local copies, waits for them, and re-layouts: 24 us -> none  [the longest x3 2.97 us: combine_steps(): latter[1] * earlier[3]]
  transfers between devices with their start and end apart: 4 -> 10, of which waited for: 2 -> 3; matrix products, arithmetic and copies ran while one was open for 74% -> 3% of each run, Pallas kernels for 0% -> 12%
where the time goes in v1:
time: 184 us; the launch traced here: 183 us
  starting transfers between devices  59 us (32%)
  waiting for transfers between devices  48 us (26%)
  blocking collectives  38.5 us (21%)
  Pallas kernels  28 us (15%)
  local copies, waits for them, and re-layouts  5.98 us (3%)
  other arithmetic  3.06 us (2%)
    all_to_all x4, starting transfers between devices, spread_out(): return lax.all_to_all(pieces, axes, split_axis=0, concat_axis=0, tiled=True)  32.1 us
    ppermute x2, waiting for transfers between devices, exchanged(): over = lax.ppermute(piece, 'yl', SWAP)  25.4 us
    all_to_all x4, waiting for transfers between devices, spread_out(): return lax.all_to_all(pieces, axes, split_axis=0, concat_axis=0, tiled=True)  22.5 us
    all_gather x1, blocking collectives, on_device(): lax.all_gather(shared_hidden, TP, axis=0)  21 us
    all_gather x1, blocking collectives, on_device(): whole_rows = lax.all_gather(ssm_out, TP, axis=0)  17.5 us
    ppermute x2, starting transfers between devices, exchanged(): lax.ppermute(over, 'co', SWAP)  11.4 us
    ppermute x2, starting transfers between devices, exchanged(): lax.ppermute(piece, 'co', SWAP)  8.56 us
    pallas_call x2, Pallas kernels, run_hidden(): pl.pallas_call(hidden_kernel, out_shape=jax.ShapeDtypeStruct((copies, row...  7.1 us
  transfers between devices with their start and end apart: 10, of which 3 were waited for; matrix products, arithmetic and copies ran while one was open for 3% of the time, Pallas kernels for 12%

profile of v1, /device:TPU:1, one launch (start us, length us, event | category | flops | bytes accessed | tf_op | source)
XLA Modules:
  0.0 183.4 jit_solution(6398504642926478525)
XLA Ops:
  2.0 4.0 %collective-permute-start.1 = (bf16[2048,256]{1,0:T(8,128)(2,1)S(1)}, bf16[2048,256]{1,0:T(8,128)(2,1)S(1)}, u32[]{:S(2)}, u32[]{:S(2)}) collective-permute-start(bf16[2048,256]{1,0:T(8,128)(2,1)S(1)} %pad_maximum_fusion.1.refs_0_), channel_id=1, source_target_pairs={{0,2},{2,0},{1,3},{3,1},{4,6},{6,4},{5,7},{7,5},{8,10},{10,8},{9,1... | collective-permute-start | bytes 3145736 | tf_op jit(solution)/shard_map/ppermute | solution.py:402
  6.6 2.7 %dispatch.1 = (bf16[128,2048]{1,0:T(8,128)(2,1)}, bf16[256,2048]{1,0:T(8,128)(2,1)}) custom-call(s32[2]{0:T(128)} %pad_add_fusion.where_ref, bf16[128,2048]{1,0:T(8,128)(2,1)} %tokens_ref.1, f32[1,2048]{1,0:T(1,128)} %bitcast.30, s32[4,128]{1,0:T(4,128)} %bitcast.31), custom_call_target="tpu_custom_call" | custom-call | tf_op jit(solution)/shard_map/dispatch/pallas_call | solution.py:261
  9.3 12.9 %all-to-all-start.1 = ((bf16[32,8,2048]{2,1,0:T(8,128)(2,1)}), bf16[32,8,2048]{2,1,0:T(8,128)(2,1)S(1)}, u32[]{:S(2)}, u32[]{:S(2)}) async-start(bf16[32,8,2048]{2,1,0:T(8,128)(2,1)} %bitcast.21), calls=%async_computation.1 | async-start | bytes 2097152 | tf_op jit(solution)/shard_map/all_to_all | solution.py:407
  22.2 3.1 %collective-permute-start = (bf16[2048,256]{1,0:T(8,128)(2,1)S(1)}, bf16[2048,256]{1,0:T(8,128)(2,1)}, u32[]{:S(2)}, u32[]{:S(2)}) collective-permute-start(bf16[2048,256]{1,0:T(8,128)(2,1)S(1)} %pad_maximum_fusion.1.refs_0_), channel_id=1, source_target_pairs={{0,1},{1,0},{2,3},{3,2},{4,5},{5,4},{6,7},{7,6},{8,9},{9,8},{10,11... | collective-permute-start | bytes 3145736 | tf_op jit(solution)/shard_map/ppermute | solution.py:403
  25.4 6.6 %collective-permute-start.2 = (bf16[2048,256]{1,0:T(8,128)(2,1)S(1)}, bf16[2048,256]{1,0:T(8,128)(2,1)}, u32[]{:S(2)}, u32[]{:S(2)}) collective-permute-start(bf16[2048,256]{1,0:T(8,128)(2,1)S(1)} %collective-permute-done.1.refs_2_), channel_id=1, source_target_pairs={{0,1},{1,0},{2,3},{3,2},{4,5},{5,4},{6,7},{7,6},{8,9},{9,8},{10,11... | collective-permute-start | bytes 3145736 | tf_op jit(solution)/shard_map/ppermute | solution.py:403
  32.0 16.3 %all-to-all-done.1 = bf16[32,8,2048]{2,1,0:T(8,128)(2,1)S(1)} async-done(((bf16[32,8,2048]{2,1,0:T(8,128)(2,1)}), bf16[32,8,2048]{2,1,0:T(8,128)(2,1)S(1)}, u32[]{:S(2)}, u32[]{:S(2)}) %all-to-all-start.1) | async-done | bytes 1048608 | tf_op jit(solution)/shard_map/all_to_all | solution.py:407
  49.3 4.8 %hidden.3 = bf16[4,256,512]{2,1,0:T(8,128)(2,1)} custom-call(bf16[256,2048]{1,0:T(8,128)(2,1)} %bitcast.17, bf16[2048,256]{1,0:T(8,128)(2,1)} %copy-done.1, bf16[2048,256]{1,0:T(8,128)(2,1)} %collective-permute-done.refs_1_, bf16[2048,256]{1,0:T(8,128)(2,1)} %copy-done.4, bf16[2048,256]{1,0:T(8,128)(2,1)} %collective-permute-done.2.refs_3_), custom_call_target="tpu_custom_call" | custom-call | tf_op jit(solution)/shard_map/hidden/pallas_call | solution.py:322
  54.1 6.0 %all-to-all-start.2 = ((bf16[4,256,512]{2,1,0:T(8,128)(2,1)}), bf16[4,256,512]{2,1,0:T(8,128)(2,1)S(1)}, u32[]{:S(2)}, u32[]{:S(2)}) async-start(bf16[4,256,512]{2,1,0:T(8,128)(2,1)} %hidden.3), calls=%async_computation.2 | async-start | bytes 2097152 | tf_op jit(solution)/shard_map/all_to_all | solution.py:407
  60.1 3.0 %collective-permute-start.4 = (bf16[2048,128]{1,0:T(8,128)(2,1)S(1)}, bf16[2048,128]{1,0:T(8,128)(2,1)S(1)}, u32[]{:S(2)}, u32[]{:S(2)}) collective-permute-start(bf16[2048,128]{1,0:T(8,128)(2,1)S(1)} %bitcast.27), channel_id=1, source_target_pairs={{0,2},{2,0},{1,3},{3,1},{4,6},{6,4},{5,7},{7,5},{8,10},{10,8},{9,1... | collective-permute-start | bytes 1572872 | tf_op jit(solution)/shard_map/ppermute | solution.py:402
  63.1 5.4 %collective-permute-start.3 = (bf16[2048,128]{1,0:T(8,128)(2,1)S(1)}, bf16[2048,128]{1,0:T(8,128)(2,1)}, u32[]{:S(2)}, u32[]{:S(2)}) collective-permute-start(bf16[2048,128]{1,0:T(8,128)(2,1)S(1)} %bitcast.28), channel_id=1, source_target_pairs={{0,1},{1,0},{2,3},{3,2},{4,5},{5,4},{6,7},{7,6},{8,9},{9,8},{10,11... | collective-permute-start | bytes 1572872 | tf_op jit(solution)/shard_map/ppermute | solution.py:403
  68.5 25.4 %collective-permute-done.4.refs_3_ = bf16[2048,128]{1,0:T(8,128)(2,1)S(1)} collective-permute-done((bf16[2048,128]{1,0:T(8,128)(2,1)S(1)}, bf16[2048,128]{1,0:T(8,128)(2,1)S(1)}, u32[]{:S(2)}, u32[]{:S(2)}) %collective-permute-start.4) | collective-permute-done | bytes 524320 | tf_op jit(solution)/shard_map/ppermute | solution.py:402
  93.9 4.8 %collective-permute-start.5 = (bf16[2048,128]{1,0:T(8,128)(2,1)S(1)}, bf16[2048,128]{1,0:T(8,128)(2,1)}, u32[]{:S(2)}, u32[]{:S(2)}) collective-permute-start(bf16[2048,128]{1,0:T(8,128)(2,1)S(1)} %collective-permute-done.4.refs_3_), channel_id=1, source_target_pairs={{0,1},{1,0},{2,3},{3,2},{4,5},{5,4},{6,7},{7,6},{8,9},{9,8},{10,11... | collective-permute-start | bytes 1572872 | tf_op jit(solution)/shard_map/ppermute | solution.py:403
  102.3 3.8 %scan.1 = (f32[32,8,256]{2,1,0:T(8,128)}, f32[32,8,256]{2,1,0:T(8,128)}, f32[32,8,256]{2,1,0:T(8,128)}, f32[32,8,256]{2,1,0:T(8,128)}, f32[32,8,128]{2,1,0:T(8,128)}) custom-call(bf16[256,64]{1,0:T(8,128)(2,1)} %copy.29.x_ref, f32[256,8]{1,0:T(8,128)} %bitcast.23, f32[1,256]{1,0:T(1,128)} %reshape.37.eig_ref, f32[1,256]{1,0:T(1,128)} %reshape.38.freq_ref, ...), custom_call_target="tpu_custom_call" | custom-call | tf_op jit(solution)/shard_map/scan/pallas_call | solution.py:113
  106.1 6.3 %all-to-all-start = ((f32[32,8,128]{2,1,0:T(8,128)}), f32[32,8,128]{2,1,0:T(8,128)S(1)}, u32[]{:S(2)}, u32[]{:S(2)}) async-start(f32[32,8,128]{2,1,0:T(8,128)} %get-tuple-element.15), calls=%async_computation | async-start | bytes 262144 | tf_op jit(solution)/shard_map/all_to_all | solution.py:407
  112.5 3.6 %down.1 = bf16[4,256,128]{2,1,0:T(8,128)(2,1)} custom-call(s32[2]{0:T(128)} %pad_add_fusion.where_ref, bf16[4,256,512]{2,1,0:T(8,128)(2,1)} %copy-done, bf16[2048,128]{1,0:T(8,128)(2,1)} %bitcast.26, bf16[2048,128]{1,0:T(8,128)(2,1)} %collective-permute-done.3.refs_2_, bf16[2048,128]{1,0:T(8,128)(2,1)} %copy-done.9, ...), custom_call_target="tpu_custom_call" | custom-call | tf_op jit(solution)/shard_map/down/pallas_call | solution.py:349
  116.1 6.3 %all-to-all-done.ends_ref = f32[32,8,128]{2,1,0:T(8,128)S(1)} async-done(((f32[32,8,128]{2,1,0:T(8,128)}), f32[32,8,128]{2,1,0:T(8,128)S(1)}, u32[]{:S(2)}, u32[]{:S(2)}) %all-to-all-start) | async-done | bytes 131104 | tf_op jit(solution)/shard_map/all_to_all | solution.py:407
  122.4 6.8 %all-to-all-start.3 = ((bf16[128,8,128]{2,1,0:T(8,128)(2,1)}), bf16[128,8,128]{2,1,0:T(8,128)(2,1)S(1)}, u32[]{:S(2)}, u32[]{:S(2)}) async-start(bf16[128,8,128]{2,1,0:T(8,128)(2,1)} %bitcast.19), calls=%async_computation.3 | async-start | bytes 524288 | tf_op jit(solution)/shard_map/all_to_all | solution.py:407
  132.8 2.3 %hidden.2 = bf16[1,128,128]{2,1,0:T(8,128)(2,1)} custom-call(bf16[128,2048]{1,0:T(8,128)(2,1)} %get-tuple-element.16.rows_ref, bf16[2048,256]{1,0:T(8,128)(2,1)} %pad_maximum_fusion.refs_0_), custom_call_target="tpu_custom_call" | custom-call | tf_op jit(solution)/shard_map/hidden/pallas_call | solution.py:322
  135.1 21.0 %all_gather.11.blocks_ref = bf16[16,128,128]{2,1,0:T(8,128)(2,1)} all-gather(bf16[1,128,128]{2,1,0:T(8,128)(2,1)} %hidden.2), channel_id=1, replica_groups=mesh['ep'=32,'yh'=4,'yl'=2,'co'=2] {'yh','yl','co'}, dimensions={0}, use_global_device_ids=true | all-gather | bytes 557056 | tf_op jit(solution)/shard_map/all_gather | solution.py:465
  156.1 2.1 %shared.1.shared_ref = f32[128,128]{1,0:T(8,128)} custom-call(bf16[16,128,128]{2,1,0:T(8,128)(2,1)} %all_gather.11.blocks_ref, bf16[2048,128]{1,0:T(8,128)(2,1)} %w_ref.3), custom_call_target="tpu_custom_call" | custom-call | tf_op jit(solution)/shard_map/shared/pallas_call | solution.py:370
  158.3 2.5 %readout.1 = bf16[128,128]{1,0:T(8,128)(2,1)} custom-call(s32[1]{0:T(128)} %bitcast.where_ref, f32[32,8,256]{2,1,0:T(8,128)} %get-tuple-element.11.p_re, f32[32,8,256]{2,1,0:T(8,128)} %get-tuple-element.12.p_im, f32[32,8,256]{2,1,0:T(8,128)} %get-tuple-element.13.h_re, f32[32,8,256]{2,1,0:T(8,128)} %get-tuple-element.14.h_im, f32[32,8,128]{2,1,0:T(8,128)} %copy-done.5, ...), custom_call_target="tpu_custom_call" | custom-call | tf_op jit(solution)/shard_map/readout/pallas_call | solution.py:177
  160.8 17.5 %all-gather = bf16[2048,128]{1,0:T(8,128)(2,1)} all-gather(bf16[128,128]{1,0:T(8,128)(2,1)} %readout.1), channel_id=2, replica_groups=mesh['ep'=32,'yh'=4,'yl'=2,'co'=2] {'yh','yl','co'}, dimensions={0}, use_global_device_ids=true | all-gather | bytes 557056 | tf_op jit(solution)/shard_map/all_gather | solution.py:460
  178.3 2.3 %mixed.1 = bf16[256,128]{1,0:T(8,128)(2,1)} custom-call(bf16[16,128,128]{2,1,0:T(8,128)(2,1)} %bitcast.18, f32[16,64]{1,0:T(8,128)} %reshape.42.scale_ref, bf16[1024,128]{1,0:T(8,128)(2,1)} %w_ref.2), custom_call_target="tpu_custom_call" | custom-call | tf_op jit(solution)/shard_map/mixed/pallas_call | solution.py:214
  181.3 2.0 %combine.1 = bf16[128,128]{1,0:T(8,128)(2,1)} custom-call(f32[128,128]{1,0:T(8,128)} %shared.1.shared_ref, bf16[1024,128]{1,0:T(8,128)(2,1)} %bitcast.20, bf16[128,1024]{1,0:T(8,128)(2,1)} %get-tuple-element.18.high_ref, bf16[128,1024]{1,0:T(8,128)(2,1)} %get-tuple-element.19.low_ref), custom_call_target="tpu_custom_call" | custom-call | tf_op jit(solution)/shard_map/combine/pallas_call | solution.py:388
  (53 shorter events, 10.9 us)
Async XLA Ops:
  1.9 20.3 %copy-start.1 = (bf16[2048,256]{1,0:T(8,128)(2,1)}, bf16[2048,256]{1,0:T(8,128)(2,1)S(1)}, u32[]{:S(2)}) copy-start(bf16[2048,256]{1,0:T(8,128)(2,1)S(1)} %pad_maximum_fusion.1.refs_0_) | copy-start | bytes 3145732
  2.0 23.4 %collective-permute-start.1 = (bf16[2048,256]{1,0:T(8,128)(2,1)S(1)}, bf16[2048,256]{1,0:T(8,128)(2,1)S(1)}, u32[]{:S(2)}, u32[]{:S(2)}) collective-permute-start(bf16[2048,256]{1,0:T(8,128)(2,1)S(1)} %pad_maximum_fusion.1.refs_0_), channel_id=1, source_target_pairs={{0,2},{2,0},{1,3},{3,1},{4,6},{6,4},{5,7},{7,5},{8,10},{10,8},{9,1... | collective-permute-start | bytes 3145736 | tf_op jit(solution)/shard_map/ppermute | solution.py:402
  9.3 39.0 %all-to-all-start.1 = ((bf16[32,8,2048]{2,1,0:T(8,128)(2,1)}), bf16[32,8,2048]{2,1,0:T(8,128)(2,1)S(1)}, u32[]{:S(2)}, u32[]{:S(2)}) async-start(bf16[32,8,2048]{2,1,0:T(8,128)(2,1)} %bitcast.21), calls=%async_computation.1 | async-start | bytes 2097152 | tf_op jit(solution)/shard_map/all_to_all | solution.py:407
  22.2 9.8 %collective-permute-start = (bf16[2048,256]{1,0:T(8,128)(2,1)S(1)}, bf16[2048,256]{1,0:T(8,128)(2,1)}, u32[]{:S(2)}, u32[]{:S(2)}) collective-permute-start(bf16[2048,256]{1,0:T(8,128)(2,1)S(1)} %pad_maximum_fusion.1.refs_0_), channel_id=1, source_target_pairs={{0,1},{1,0},{2,3},{3,2},{4,5},{5,4},{6,7},{7,6},{8,9},{9,8},{10,11... | collective-permute-start | bytes 3145736 | tf_op jit(solution)/shard_map/ppermute | solution.py:403
  25.4 22.9 %copy-start.4 = (bf16[2048,256]{1,0:T(8,128)(2,1)}, bf16[2048,256]{1,0:T(8,128)(2,1)S(1)}, u32[]{:S(2)}) copy-start(bf16[2048,256]{1,0:T(8,128)(2,1)S(1)} %collective-permute-done.1.refs_2_) | copy-start | bytes 3145732
  25.4 22.9 %collective-permute-start.2 = (bf16[2048,256]{1,0:T(8,128)(2,1)S(1)}, bf16[2048,256]{1,0:T(8,128)(2,1)}, u32[]{:S(2)}, u32[]{:S(2)}) collective-permute-start(bf16[2048,256]{1,0:T(8,128)(2,1)S(1)} %collective-permute-done.1.refs_2_), channel_id=1, source_target_pairs={{0,1},{1,0},{2,3},{3,2},{4,5},{5,4},{6,7},{7,6},{8,9},{9,8},{10,11... | collective-permute-start | bytes 3145736 | tf_op jit(solution)/shard_map/ppermute | solution.py:403
  54.0 6.1 %copy-start.6 = (bf16[1,2048,128]{2,1,0:T(8,128)(2,1)S(1)}, bf16[1,2048,128]{2,1,0:T(8,128)(2,1)}, u32[]{:S(2)}) copy-start(bf16[1,2048,128]{2,1,0:T(8,128)(2,1)} %param.36) | copy-start | bytes 1572868
  54.0 44.7 %copy-start.10 = (bf16[256,64]{0,1:T(8,128)(2,1)S(1)}, bf16[256,64]{0,1:T(8,128)(2,1)}, u32[]{:S(2)}) copy-start(bf16[256,64]{0,1:T(8,128)(2,1)} %param.20) | copy-start | bytes 98308
  54.0 45.4 %copy-start.13 = (f32[4,256]{1,0:T(4,128)S(1)}, f32[4,256]{1,0:T(4,128)}, u32[]{:S(2)}) copy-start(f32[4,256]{1,0:T(4,128)} %param.21) | copy-start | bytes 12292
  54.1 45.4 %copy-start.14 = (f32[4,256]{1,0:T(4,128)S(1)}, f32[4,256]{1,0:T(4,128)}, u32[]{:S(2)}) copy-start(f32[4,256]{1,0:T(4,128)} %param.22) | copy-start | bytes 12292
  54.1 46.2 %copy-start.15 = (f32[4,64]{1,0:T(4,128)S(1)}, f32[4,64]{1,0:T(4,128)}, u32[]{:S(2)}) copy-start(f32[4,64]{1,0:T(4,128)} %param.23) | copy-start | bytes 3076
  54.1 46.8 %copy-start.16 = (f32[4,64]{1,0:T(4,128)S(1)}, f32[4,64]{1,0:T(4,128)}, u32[]{:S(2)}) copy-start(f32[4,64]{1,0:T(4,128)} %param.24) | copy-start | bytes 3076
  54.1 47.5 %copy-start.11 = (bf16[2,4,64,16]{2,3,1,0:T(8,128)(2,1)S(1)}, bf16[2,4,64,16]{2,3,1,0:T(8,128)(2,1)}, u32[]{:S(2)}) copy-start(bf16[2,4,64,16]{2,3,1,0:T(8,128)(2,1)} %param.25) | copy-start | bytes 49156
  54.1 52.0 %all-to-all-start.2 = ((bf16[4,256,512]{2,1,0:T(8,128)(2,1)}), bf16[4,256,512]{2,1,0:T(8,128)(2,1)S(1)}, u32[]{:S(2)}, u32[]{:S(2)}) async-start(bf16[4,256,512]{2,1,0:T(8,128)(2,1)} %hidden.3), calls=%async_computation.2 | async-start | bytes 2097152 | tf_op jit(solution)/shard_map/all_to_all | solution.py:407
  60.1 33.8 %collective-permute-start.4 = (bf16[2048,128]{1,0:T(8,128)(2,1)S(1)}, bf16[2048,128]{1,0:T(8,128)(2,1)S(1)}, u32[]{:S(2)}, u32[]{:S(2)}) collective-permute-start(bf16[2048,128]{1,0:T(8,128)(2,1)S(1)} %bitcast.27), channel_id=1, source_target_pairs={{0,2},{2,0},{1,3},{3,1},{4,6},{6,4},{5,7},{7,5},{8,10},{10,8},{9,1... | collective-permute-start | bytes 1572872 | tf_op jit(solution)/shard_map/ppermute | solution.py:402
  63.1 49.4 %collective-permute-start.3 = (bf16[2048,128]{1,0:T(8,128)(2,1)S(1)}, bf16[2048,128]{1,0:T(8,128)(2,1)}, u32[]{:S(2)}, u32[]{:S(2)}) collective-permute-start(bf16[2048,128]{1,0:T(8,128)(2,1)S(1)} %bitcast.28), channel_id=1, source_target_pairs={{0,1},{1,0},{2,3},{3,2},{4,5},{5,4},{6,7},{7,6},{8,9},{9,8},{10,11... | collective-permute-start | bytes 1572872 | tf_op jit(solution)/shard_map/ppermute | solution.py:403
  93.9 18.6 %copy-start.9 = (bf16[2048,128]{1,0:T(8,128)(2,1)}, bf16[2048,128]{1,0:T(8,128)(2,1)S(1)}, u32[]{:S(2)}) copy-start(bf16[2048,128]{1,0:T(8,128)(2,1)S(1)} %collective-permute-done.4.refs_3_) | copy-start | bytes 1572868
  93.9 18.5 %collective-permute-start.5 = (bf16[2048,128]{1,0:T(8,128)(2,1)S(1)}, bf16[2048,128]{1,0:T(8,128)(2,1)}, u32[]{:S(2)}, u32[]{:S(2)}) collective-permute-start(bf16[2048,128]{1,0:T(8,128)(2,1)S(1)} %collective-permute-done.4.refs_3_), channel_id=1, source_target_pairs={{0,1},{1,0},{2,3},{3,2},{4,5},{5,4},{6,7},{7,6},{8,9},{9,8},{10,11... | collective-permute-start | bytes 1572872 | tf_op jit(solution)/shard_map/ppermute | solution.py:403
  106.1 6.4 %copy-start = (bf16[4,256,512]{2,1,0:T(8,128)(2,1)}, bf16[4,256,512]{2,1,0:T(8,128)(2,1)S(1)}, u32[]{:S(2)}) copy-start(bf16[4,256,512]{2,1,0:T(8,128)(2,1)S(1)} %all-to-all-done.2.refs_0_) | copy-start | bytes 3145732
  106.1 16.3 %all-to-all-start = ((f32[32,8,128]{2,1,0:T(8,128)}), f32[32,8,128]{2,1,0:T(8,128)S(1)}, u32[]{:S(2)}, u32[]{:S(2)}) async-start(f32[32,8,128]{2,1,0:T(8,128)} %get-tuple-element.15), calls=%async_computation | async-start | bytes 262144 | tf_op jit(solution)/shard_map/all_to_all | solution.py:407
  112.4 16.7 %copy-start.7 = (bf16[2048,128]{1,0:T(8,128)(2,1)S(1)}, bf16[2048,128]{1,0:T(8,128)(2,1)}, u32[]{:S(2)}) copy-start(bf16[2048,128]{1,0:T(8,128)(2,1)} %param.38) | copy-start | bytes 1572868
  112.5 16.7 %copy-start.8 = (bf16[2048,128]{1,0:T(8,128)(2,1)S(1)}, bf16[2048,128]{1,0:T(8,128)(2,1)}, u32[]{:S(2)}) copy-start(bf16[2048,128]{1,0:T(8,128)(2,1)} %param.37) | copy-start | bytes 1572868
  122.4 7.9 %copy-start.5 = (f32[32,8,128]{2,1,0:T(8,128)}, f32[32,8,128]{2,1,0:T(8,128)S(1)}, u32[]{:S(2)}) copy-start(f32[32,8,128]{2,1,0:T(8,128)S(1)} %all-to-all-done.ends_ref) | copy-start | bytes 393220
  122.4 58.3 %all-to-all-start.3 = ((bf16[128,8,128]{2,1,0:T(8,128)(2,1)}), bf16[128,8,128]{2,1,0:T(8,128)(2,1)S(1)}, u32[]{:S(2)}, u32[]{:S(2)}) async-start(bf16[128,8,128]{2,1,0:T(8,128)(2,1)} %bitcast.19), calls=%async_computation.3 | async-start | bytes 524288 | tf_op jit(solution)/shard_map/all_to_all | solution.py:407
  (3 other events, 2.8 us)

commit v2 on v1

--- a/solution.py
+++ b/solution.py
@@ -5,6 +5,7 @@
 from jax.experimental.pallas import tpu as pltpu
 from jax.sharding import Mesh
 from jax.sharding import PartitionSpec as P
+
 
 VM = pltpu.VMEM
 F32, BF16 = jnp.float32, jnp.bfloat16
@@ -47,39 +48,56 @@
     return jnp.where(y > -0.5, -y * small, 1.0 - jnp.exp(y))
 
 
-def scan_kernel(x_ref, steps_ref, eig_ref, freq_ref, win_ref, p_re, p_im, h_re, h_im, ends_ref,
-                a_re, a_im, d_re, d_im):
-    positions, width = x_ref.shape
-    groups = steps_ref.shape[1] // 2
-    states = eig_ref.shape[1] // groups
+def flat(ref):
+    return jnp.concatenate([ref[g : g + 1, :] for g in range(ref.shape[0])], axis=1)
+
+
+def block_diagonal(ref, groups):
+    rows, states = ref.shape
+    width = rows // 2
+    half = groups * states
+    repeat = (iota((states, half), 1) % states == iota((states, half), 0)).astype(BF16)
+    wide = jnp.dot(ref[...], repeat, preferred_element_type=F32)
+    group = iota(wide.shape, 0) % width // (width // groups)
+    wide = jnp.where(group == iota(wide.shape, 1) // states, wide, 0.0)
+    return wide[:width], wide[width:]
+
+
+def scan_part(x_ref, log_ref, loss_ref, eig_ref, freq_ref, win_ref, feed_ref,
+              p_re, p_im, h_re, h_im, through_ref, a_re, a_im, d_re, d_im):
+    _, positions = x_ref.shape
+    groups, states = eig_ref.shape
     lanes = 128
     per = lanes // states
-    channels = width // groups
-    spread = (iota((channels, width), 1) % channels == iota((channels, width), 0)).astype(BF16)
-    wide = jnp.dot(win_ref[...], spread, preferred_element_type=F32)
-    rows = iota(wide.shape, 0) // states % groups
-    wide = jnp.where(rows == iota(wide.shape, 1) // channels, wide, 0.0).astype(BF16)
-    driven = lax.dot_general(x_ref[...], wide, NT, preferred_element_type=F32)
+    x = x_ref[...].astype(F32).T
+    through_ref[...] = x * feed_ref[...]
+    steps = jnp.concatenate([jnp.exp(log_ref[...]), loss_ref[...]], axis=0).T
+    eig, freq = flat(eig_ref), flat(freq_ref)
+    x = x.astype(BF16)
+    driven = [
+        jnp.dot(x, w.astype(BF16), preferred_element_type=F32)
+        for w in block_diagonal(win_ref, groups)
+    ]
     half = groups * states
     for tile in range(half // lanes):
         at = slice(tile * lanes, (tile + 1) * lanes)
         place = iota((positions, lanes), 1) // states
-        step = jnp.broadcast_to(steps_ref[:, tile * per : tile * per + 1], (positions, lanes))
+        step = jnp.broadcast_to(steps[:, tile * per : tile * per + 1], (positions, lanes))
         loss = jnp.broadcast_to(
-            steps_ref[:, groups + tile * per : groups + tile * per + 1], (positions, lanes)
+            steps[:, groups + tile * per : groups + tile * per + 1], (positions, lanes)
         )
         for k in range(1, per):
             g = tile * per + k
-            step = jnp.where(place == k, steps_ref[:, g : g + 1], step)
-            loss = jnp.where(place == k, steps_ref[:, groups + g : groups + g + 1], loss)
-        decay_log = -eig_ref[:, at] * step
+            step = jnp.where(place == k, steps[:, g : g + 1], step)
+            loss = jnp.where(place == k, steps[:, groups + g : groups + g + 1], loss)
+        decay_log = -eig[:, at] * step
         magnitude = jnp.exp(decay_log + loss)
-        sin_x, cos_x = sin_cos(freq_ref[:, at] * step)
+        sin_x, cos_x = sin_cos(freq[:, at] * step)
         scaling = jnp.sqrt(minus_expm1(2.0 * decay_log))
         a_re[tile] = magnitude * cos_x
         a_im[tile] = magnitude * sin_x
-        d_re[tile] = scaling * driven[:, at]
-        d_im[tile] = scaling * driven[:, half + tile * lanes : half + (tile + 1) * lanes]
+        d_re[tile] = scaling * driven[0][:, at]
+        d_im[tile] = scaling * driven[1][:, at]
     length = positions // CHUNKS
     ends = []
     for tile in range(half // lanes):
@@ -101,35 +119,19 @@
             er, ei = er * ar - ei * ai, er * ai + ei * ar
             sr, si = ar * sr - ai * si + hr[c : c + 1], ar * si + ai * sr + hi[c : c + 1]
         ends += [er, ei, sr, si]
-    packed = jnp.concatenate(ends, axis=0)
-    for b in range(ends_ref.shape[0]):
-        ends_ref[b] = packed
-
-
-def run_scan(x, steps, eig, freq, win, blocks):
-    positions = x.shape[0]
-    half = eig.shape[1]
-    piece = jax.ShapeDtypeStruct((positions // CHUNKS, CHUNKS, half), F32)
-    return pl.pallas_call(
-        scan_kernel,
-        out_shape=[piece] * 4 + [jax.ShapeDtypeStruct((blocks, half // 32, 128), F32)],
-        in_specs=vmem(5),
-        out_specs=vmem(5),
-        scratch_shapes=[VM((half // 128, positions, 128), F32)] * 4,
-        name="scan",
-    )(x, steps, eig, freq, win)
-
-
-def readout_kernel(where_ref, p_re, p_im, h_re, h_im, ends_ref, x_ref, wout_ref, feed_ref, out_ref,
-                   turned):
+    ends = jnp.concatenate(ends, axis=0)
+    high = ends.astype(BF16)
+    return jnp.concatenate([high, (ends - high.astype(F32)).astype(BF16)], axis=1)
+
+
+def readout_kernel(p_re, p_im, h_re, h_im, ends_ref, through_ref, wout_ref, out_ref, turned):
     length, chunks, half = p_re.shape
-    positions, width = x_ref.shape
-    states = wout_ref.shape[1]
-    channels = wout_ref.shape[0] // 2 // (half // states)
-    index = where_ref[0]
+    positions, width = through_ref.shape
+    index = lax.axis_index("ep")
     cr = ci = jnp.zeros((1, half), F32)
     for b in range(ends_ref.shape[0] - 1):
-        end = ends_ref[b]
+        end = ends_ref[b].astype(F32)
+        end = end[:, :128] + end[:, 128:]
         ar, ai, er, ei = (
             jnp.concatenate([end[q : q + 1], end[q + 4 : q + 5]], axis=1) for q in range(4)
         )
@@ -150,11 +152,8 @@
     ci = jnp.concatenate(carry_i, axis=0)[None]
     sr = (h_re[...] + p_re[...] * cr - p_im[...] * ci).reshape(positions, half)
     si = (h_im[...] + p_re[...] * ci + p_im[...] * cr).reshape(positions, half)
-    spread = (iota((states, half), 1) % states == iota((states, half), 0)).astype(BF16)
-    wide = jnp.dot(wout_ref[...], spread, preferred_element_type=F32)
-    rows = iota(wide.shape, 0) % width // channels
-    wide = jnp.where(rows == iota(wide.shape, 1) // states, wide, 0.0)
-    wr, wi = wide[:width].astype(BF16), (-wide[width:]).astype(BF16)
+    wr, wi = block_diagonal(wout_ref, half // wout_ref.shape[1])
+    wr, wi = wr.astype(BF16), (-wi).astype(BF16)
     nothing = jnp.zeros((128 - width, half), BF16)
     wr, wi = (jnp.concatenate([w, nothing], axis=0) for w in (wr, wi))
     total = None
@@ -166,22 +165,22 @@
             total = got if total is None else total + got
     for j in range(length):
         turned[pl.ds(j, chunks, stride=length), :] = total[j * chunks : (j + 1) * chunks]
-    v = turned[:, :width] + feed_ref[...] * x_ref[...].astype(F32)
+    v = turned[:, :width] + through_ref[...]
     v = 0.5 * v * (1.0 + jnp.tanh(0.7978845608028654 * (v + 0.044715 * (v * v * v))))
     both = positions // 2
     out_ref[...] = jnp.concatenate([v[:both], v[both:]], axis=1).astype(BF16)
 
 
-def run_readout(index, pieces, ends, x, wout, feed):
-    positions, width = x.shape
+def run_readout(pieces, ends, through, wout):
+    positions, width = through.shape
     return pl.pallas_call(
         readout_kernel,
         out_shape=jax.ShapeDtypeStruct((positions // 2, 2 * width), BF16),
-        in_specs=[pl.BlockSpec(memory_space=pltpu.SMEM)] + vmem(8),
+        in_specs=vmem(7),
         out_specs=pl.BlockSpec(memory_space=VM),
         scratch_shapes=[VM((positions, 128), F32)],
         name="readout",
-    )(index, *pieces, ends, x, wout, feed)
+    )(*pieces, ends, through, wout)
 
 
 def mixed_kernel(rows_ref, scale_ref, w_ref, out_ref):
@@ -220,12 +219,6 @@
     )(rows, scale.reshape(blocks, lanes // 2), w)
 
 
-def mixer_local(x, log_step, loss, eig, freq, win, blocks):
-    steps = jnp.concatenate([jnp.exp(log_step), loss], axis=0).T
-    return run_scan(x, steps, eig.reshape(1, -1), freq.reshape(1, -1),
-                    win.reshape(-1, win.shape[-1]), blocks)
-
-
 def expert_table(routes_ref, weights_ref, experts):
     top, tokens = routes_ref.shape
     expert = iota((experts, tokens), 0)
@@ -241,33 +234,47 @@
     return jnp.where(named > 0.0, rank, -1.0), gain
 
 
-def dispatch_kernel(where_ref, tokens_ref, gain_ref, routes_ref, normed_ref, sent_ref):
-    tokens = tokens_ref.shape[0]
+def own_sub():
+    return 2 * lax.axis_index("yl") + lax.axis_index("co")
+
+
+def first_kernel(tokens_ref, gain_ref, routes_ref, *refs):
+    scan_in, (normed_ref, sent_ref), scan_out = refs[:7], refs[7:9], refs[9:]
+    ends = scan_part(*scan_in, *scan_out)
+    tokens, width = tokens_ref.shape
     v = tokens_ref[...].astype(F32)
     factor = lax.rsqrt(jnp.mean(v * v, axis=1, keepdims=True) + EPS)
     normed = (v * factor * gain_ref[...]).astype(BF16)
     normed_ref[...] = normed
-    share = 8
+    share = ends.shape[0]
     experts = sent_ref.shape[0] // share
     rank, _ = expert_table(routes_ref, None, experts)
-    slot = (iota((share, tokens), 0) + where_ref[0] * share).astype(F32)
+    slot = (iota((share, tokens), 0) + own_sub() * share).astype(F32)
     chosen = jnp.concatenate(
         [jnp.where(rank[e : e + 1, :] == slot, 1.0, 0.0) for e in range(experts)], axis=0
     ).astype(BF16)
-    sent_ref[...] = jnp.dot(chosen, normed, preferred_element_type=F32).astype(BF16)
-
-
-def run_dispatch(where, tokens, gain, routes, rows):
-    return pl.pallas_call(
-        dispatch_kernel,
+    sent_ref[:, :width] = jnp.dot(chosen, normed, preferred_element_type=F32).astype(BF16)
+    for e in range(experts):
+        sent_ref[e * share : (e + 1) * share, width:] = ends
+
+
+def run_first(tokens, gain, routes, blocks, x, log_step, loss, eig, freq, win, feed):
+    width, positions = x.shape
+    half = eig.size
+    piece = jax.ShapeDtypeStruct((positions // CHUNKS, CHUNKS, half), F32)
+    return pl.pallas_call(
+        first_kernel,
         out_shape=[
             jax.ShapeDtypeStruct(tokens.shape, BF16),
-            jax.ShapeDtypeStruct((rows, tokens.shape[1]), BF16),
-        ],
-        in_specs=[pl.BlockSpec(memory_space=pltpu.SMEM)] + vmem(3),
-        out_specs=vmem(2),
-        name="dispatch",
-    )(where, tokens, gain.reshape(1, -1), routes)
+            jax.ShapeDtypeStruct((blocks * half // 32, tokens.shape[1] + 256), BF16),
+        ]
+        + [piece] * 4
+        + [jax.ShapeDtypeStruct((positions, width), F32)],
+        in_specs=vmem(10),
+        out_specs=vmem(7),
+        scratch_shapes=[VM((half // 128, positions, 128), F32)] * 4,
+        name="first",
+    )(tokens, gain.reshape(1, -1), routes, x, log_step, loss, eig, freq, win, feed)
 
 
 def choice_kernel(routes_ref, weights_ref, high_ref, low_ref):
@@ -300,21 +307,36 @@
     )(routes, weights)
 
 
-def gated(rows, both):
-    got = jnp.dot(rows, both, preferred_element_type=F32)
-    half = both.shape[1] // 2
+def gated(got):
+    half = got.shape[1] // 2
     gate, up = got[:, :half], got[:, half:]
     return (gate / (1.0 + jnp.exp(-gate)) * up).astype(BF16)
 
 
 def hidden_kernel(rows_ref, *refs):
     *weights, out_ref = refs
-    rows = rows_ref[...]
+    rows = rows_ref[:, : weights[0].shape[0]]
     for q, w in enumerate(weights):
         half = w.shape[1] // 2
-        got = gated(rows, w[...])
+        got = gated(jnp.dot(rows, w[...], preferred_element_type=F32))
         for copy in range(out_ref.shape[0]):
             out_ref[copy, :, q * half : (q + 1) * half] = got
+
+
+def shared_hidden_kernel(rows_ref, gate_ref, up_ref, out_ref):
+    both = jnp.concatenate([gate_ref[...], up_ref[...]], axis=1)
+    got = gated(jnp.dot(rows_ref[...], both, preferred_element_type=F32))
+    out_ref[...] = got
+
+
+def run_shared_hidden(rows, gate, up):
+    return pl.pallas_call(
+        shared_hidden_kernel,
+        out_shape=jax.ShapeDtypeStruct((rows.shape[0], gate.shape[1]), BF16),
+        in_specs=vmem(3),
+        out_specs=pl.BlockSpec(memory_space=VM),
+        name="shared_hidden",
+    )(rows, gate, up)
 
 
 def run_hidden(rows, weights, copies):
@@ -328,9 +350,9 @@
     )(rows, *weights)
 
 
-def down_kernel(where_ref, *refs):
+def down_kernel(*refs):
     hidden, weights, out_ref, whole = refs[0], refs[1:5], refs[5], refs[6]
-    sub = where_ref[0]
+    sub = own_sub()
     lanes = weights[0].shape[1]
     for member in range(hidden.shape[0]):
         for q in range(4):
@@ -344,16 +366,16 @@
         out_ref[sub ^ (q + 1)] = got[:, lanes:]
 
 
-def run_down(where, hidden, weights):
+def run_down(hidden, weights):
     rows, lanes = hidden.shape[1], weights[0].shape[1]
     return pl.pallas_call(
         down_kernel,
         out_shape=jax.ShapeDtypeStruct((4, rows, lanes), BF16),
-        in_specs=[pl.BlockSpec(memory_space=pltpu.SMEM)] + vmem(5),
+        in_specs=vmem(5),
         out_specs=pl.BlockSpec(memory_space=VM),
         scratch_shapes=[VM((rows, weights[0].shape[0]), BF16)],
         name="down",
-    )(where, hidden, *weights)
+    )(hidden, *weights)
 
 
 def shared_kernel(blocks_ref, w_ref, out_ref):
@@ -400,7 +422,9 @@
 
 def exchanged(piece):
     over = lax.ppermute(piece, "yl", SWAP)
-    return (piece, lax.ppermute(piece, "co", SWAP), over, lax.ppermute(over, "co", SWAP))
+    core = lax.ppermute(piece, "co", SWAP)
+    both = lax.ppermute(over, "co", SWAP)
+    return (piece, core, over, both)
 
 
 def spread_out(pieces, axes):
@@ -430,45 +454,43 @@
     shared_down_weight,
 ):
     blocks = lax.axis_size("ep")
-    tokens, width = second_micro_input.shape
-    sub = 2 * lax.axis_index("yl") + lax.axis_index("co")
-    where = jnp.stack([sub, lax.axis_index("ep")]).astype(jnp.int32)
+    width = second_micro_input.shape[1]
     routes = routes.T
-    gates = exchanged(jnp.concatenate([expert_gate_weight[0], expert_up_weight[0]], axis=1))
-    normed, sent = run_dispatch(where, second_micro_input, expert_norm_scale, routes, blocks * 8)
-    arrived = spread_out(sent.reshape(blocks, 8, width), "ep").reshape(blocks * 8, width)
-    downs = exchanged(expert_down_weight[0])
-
-    *pieces, ends = mixer_local(
-        mixer_group_input,
+    normed, sent, *pieces, through = run_first(
+        second_micro_input,
+        expert_norm_scale,
+        routes,
+        blocks,
+        mixer_group_input.T,
         log_step_size,
         extra_log_decay,
         negated_eigen_real,
         frequency,
-        group_input_matrices,
-        blocks,
+        group_input_matrices.swapaxes(2, 3).reshape(-1, frequency.shape[1]),
+        channel_feedthrough.reshape(1, -1),
     )
-    ends = spread_out(ends, "ep")
+    arrived = spread_out(sent.reshape(blocks, 8, -1), "ep")
+    both = jnp.concatenate([expert_gate_weight[0], expert_up_weight[0]], axis=1)
+    gates = exchanged(both)
+    downs = exchanged(expert_down_weight[0])
+
+    shared_hidden = run_shared_hidden(normed, shared_gate_weight, shared_up_weight)
+    shared_rows = lax.all_gather(shared_hidden, TP, axis=0)
+    shared = run_shared(shared_rows, shared_down_weight)
+
     ssm_out = run_readout(
-        where[1:],
         pieces,
-        ends,
-        mixer_group_input,
-        group_output_matrices.reshape(-1, group_output_matrices.shape[-1]),
-        channel_feedthrough.reshape(1, -1),
+        arrived[:, :, width:],
+        through,
+        group_output_matrices.reshape(-1, frequency.shape[1]),
     )
     whole_rows = lax.all_gather(ssm_out, TP, axis=0)
     mixed = run_mixed(whole_rows, mixer_norm_scale, mixer_output_weight)
-
-    shared_gates = jnp.concatenate([shared_gate_weight, shared_up_weight], axis=1)
-    shared_hidden = run_hidden(normed, [shared_gates], 1)[0]
-    shared = run_shared(lax.all_gather(shared_hidden, TP, axis=0), shared_down_weight)
     high, low = run_choice(routes, chosen_expert_weight.T, blocks * 32)
 
-    hidden = run_hidden(arrived, gates, lax.axis_size("yh"))
+    hidden = run_hidden(arrived.reshape(blocks * 8, -1), gates, lax.axis_size("yh"))
     hidden = spread_out(hidden, "yh")
-    results = run_down(where, hidden, downs)
-    results = results.reshape(4 * blocks, 8, -1)
+    results = run_down(hidden, downs).reshape(4 * blocks, 8, -1)
     back = spread_out(results, ("yl", "co", "ep")).reshape(blocks * 32, -1)
     return (mixed, run_combine(shared, back, high, low))
 

time: 184 us -> 176 us (0.957)
  starting transfers between devices: 59 us -> 51 us
  waiting for transfers between devices: 48 us -> 51.7 us
  other arithmetic: 3.06 us -> 0.12 us
    ppermute x2, waiting for transfers between devices: 25.4 us -> 48.8 us  [exchanged(): over = lax.ppermute(piece, 'yl', SWAP)]
    all_to_all x4 -> x3, waiting for transfers between devices: 22.5 us -> 0.01 us  [spread_out(): return lax.all_to_all(pieces, axes, split_axis=0, concat_axis=0, tiled=True)]
    ppermute x4, starting transfers between devices: 19.9 us -> 12.8 us  [the longest x2 6.84 us: exchanged(): both = lax.ppermute(over, 'co', SWAP)]
    ppermute x4, waiting for transfers between devices: 0.01 us -> 2.9 us  [the longest x2 2.9 us: exchanged(): both = lax.ppermute(over, 'co', SWAP)]
    pallas_call x2 -> x1, Pallas kernels: 7.1 us -> 4.8 us  [run_hidden(): pl.pallas_call(hidden_kernel, out_shape=jax.ShapeDtypeStruct((copies, row...]
    concatenate x3 -> x1, other arithmetic: 2.41 us -> 0.12 us  [on_device(): both = jnp.concatenate([expert_gate_weight[0], expert_up_weight[0]], axis=1)]
    unnamed x36 -> x26, local copies, waits for them, and re-layouts: 3.24 us -> 4.51 us
    all_to_all x4 -> x3, starting transfers between devices: 32.1 us -> 32.6 us  [spread_out(): return lax.all_to_all(pieces, axes, split_axis=0, concat_axis=0, tiled=True)]
  transfers between devices with their start and end apart: 10 -> 9, of which waited for: 3 -> 4; matrix products, arithmetic and copies ran while one was open for 3% -> 1% of each run, Pallas kernels for 12% -> 6%
where the time goes in v2:
time: 176 us
  waiting for transfers between devices  51.7 us (29%)
  starting transfers between devices  51 us (29%)
  blocking collectives  39.1 us (22%)
  Pallas kernels  26.2 us (15%)
  local copies, waits for them, and re-layouts  6.74 us (4%)
    ppermute x2, waiting for transfers between devices, exchanged(): over = lax.ppermute(piece, 'yl', SWAP)  48.8 us
    all_to_all x3, starting transfers between devices, spread_out(): return lax.all_to_all(pieces, axes, split_axis=0, concat_axis=0, tiled=True)  32.6 us
    all_gather x1, blocking collectives, on_device(): shared_rows = lax.all_gather(shared_hidden, TP, axis=0)  21.6 us
    all_gather x1, blocking collectives, on_device(): whole_rows = lax.all_gather(ssm_out, TP, axis=0)  17.5 us
    ppermute x2, starting transfers between devices, exchanged(): both = lax.ppermute(over, 'co', SWAP)  6.84 us
    ppermute x2, starting transfers between devices, exchanged(): core = lax.ppermute(piece, 'co', SWAP)  5.99 us
    ppermute x2, starting transfers between devices, exchanged(): over = lax.ppermute(piece, 'yl', SWAP)  5.63 us
    pallas_call x1, Pallas kernels, run_hidden(): pl.pallas_call(hidden_kernel, out_shape=jax.ShapeDtypeStruct((copies, row...  4.8 us
  transfers between devices with their start and end apart: 9, of which 4 were waited for; matrix products, arithmetic and copies ran while one was open for 1% of the time, Pallas kernels for 6%

profile of v2, /device:TPU:1, one launch (start us, length us, event | category | flops | bytes accessed | tf_op | source)
XLA Modules:
  0.0 175.7 jit_solution(13754384048218010918)
XLA Ops:
  0.6 4.8 %first.1 = (bf16[128,2048]{1,0:T(8,128)(2,1)}, bf16[256,2304]{1,0:T(8,128)(2,1)}, f32[32,8,256]{2,1,0:T(8,128)}, f32[32,8,256]{2,1,0:T(8,128)}, f32[32,8,256]{2,...) custom-call(bf16[128,2048]{1,0:T(8,128)(2,1)} %tokens_ref.1, f32[1,2048]{1,0:T(1,128)} %bitcast.32, ...), custom_call_target="tpu_custom_call" | custom-call | tf_op jit(solution)/shard_map/first/pallas_call | solution.py:265
  5.4 13.8 %all-to-all-start = ((bf16[32,8,2304]{2,1,0:T(8,128)(2,1)}), bf16[32,8,2304]{2,1,0:T(8,128)(2,1)S(1)}, u32[]{:S(2)}, u32[]{:S(2)}) async-start(bf16[32,8,2304]{2,1,0:T(8,128)(2,1)} %bitcast.21), calls=%async_computation | async-start | bytes 2359296 | tf_op jit(solution)/shard_map/all_to_all | solution.py:431
  19.4 3.2 %collective-permute-start.1 = (bf16[2048,256]{1,0:T(8,128)(2,1)S(1)}, bf16[2048,256]{1,0:T(8,128)(2,1)S(1)}, u32[]{:S(2)}, u32[]{:S(2)}) collective-permute-start(bf16[2048,256]{1,0:T(8,128)(2,1)S(1)} %pad_maximum_fusion.refs_0_), channel_id=1, source_target_pairs={{0,2},{2,0},{1,3},{3,1},{4,6},{6,4},{5,7},{7,5},{8,10},{10,8},{9,1... | collective-permute-start | bytes 3145736 | tf_op jit(solution)/shard_map/ppermute | solution.py:424
  22.6 3.2 %collective-permute-start = (bf16[2048,256]{1,0:T(8,128)(2,1)S(1)}, bf16[2048,256]{1,0:T(8,128)(2,1)S(1)}, u32[]{:S(2)}, u32[]{:S(2)}) collective-permute-start(bf16[2048,256]{1,0:T(8,128)(2,1)S(1)} %pad_maximum_fusion.refs_0_), channel_id=1, source_target_pairs={{0,1},{1,0},{2,3},{3,2},{4,5},{5,4},{6,7},{7,6},{8,9},{9,8},{10,11... | collective-permute-start | bytes 3145736 | tf_op jit(solution)/shard_map/ppermute | solution.py:425
  25.8 19.3 %collective-permute-done.1.refs_2_ = bf16[2048,256]{1,0:T(8,128)(2,1)S(1)} collective-permute-done((bf16[2048,256]{1,0:T(8,128)(2,1)S(1)}, bf16[2048,256]{1,0:T(8,128)(2,1)S(1)}, u32[]{:S(2)}, u32[]{:S(2)}) %collective-permute-start.1) | collective-permute-done | bytes 1048608 | tf_op jit(solution)/shard_map/ppermute | solution.py:424
  45.1 3.7 %collective-permute-start.2 = (bf16[2048,256]{1,0:T(8,128)(2,1)S(1)}, bf16[2048,256]{1,0:T(8,128)(2,1)}, u32[]{:S(2)}, u32[]{:S(2)}) collective-permute-start(bf16[2048,256]{1,0:T(8,128)(2,1)S(1)} %collective-permute-done.1.refs_2_), channel_id=1, source_target_pairs={{0,1},{1,0},{2,3},{3,2},{4,5},{5,4},{6,7},{7,6},{8,9},{9,8},{10,11... | collective-permute-start | bytes 3145736 | tf_op jit(solution)/shard_map/ppermute | solution.py:426
  52.2 4.8 %hidden.1 = bf16[4,256,512]{2,1,0:T(8,128)(2,1)} custom-call(bf16[256,2304]{1,0:T(8,128)(2,1)} %bitcast.18, bf16[2048,256]{1,0:T(8,128)(2,1)} %copy-done.1, bf16[2048,256]{1,0:T(8,128)(2,1)} %copy-done.4, bf16[2048,256]{1,0:T(8,128)(2,1)} %copy-done.3, bf16[2048,256]{1,0:T(8,128)(2,1)} %collective-permute-done.2.refs_3_), custom_call_target="tpu_custom_call" | custom-call | tf_op jit(solution)/shard_map/hidden/pallas_call | solution.py:344
  57.0 6.9 %all-to-all-start.1 = ((bf16[4,256,512]{2,1,0:T(8,128)(2,1)}), bf16[4,256,512]{2,1,0:T(8,128)(2,1)S(1)}, u32[]{:S(2)}, u32[]{:S(2)}) async-start(bf16[4,256,512]{2,1,0:T(8,128)(2,1)} %hidden.1), calls=%async_computation.1 | async-start | bytes 2097152 | tf_op jit(solution)/shard_map/all_to_all | solution.py:431
  64.0 2.4 %collective-permute-start.4 = (bf16[2048,128]{1,0:T(8,128)(2,1)S(1)}, bf16[2048,128]{1,0:T(8,128)(2,1)S(1)}, u32[]{:S(2)}, u32[]{:S(2)}) collective-permute-start(bf16[2048,128]{1,0:T(8,128)(2,1)S(1)} %bitcast.27), channel_id=1, source_target_pairs={{0,2},{2,0},{1,3},{3,1},{4,6},{6,4},{5,7},{7,5},{8,10},{10,8},{9,1... | collective-permute-start | bytes 1572872 | tf_op jit(solution)/shard_map/ppermute | solution.py:424
  66.4 2.8 %collective-permute-start.3 = (bf16[2048,128]{1,0:T(8,128)(2,1)S(1)}, bf16[2048,128]{1,0:T(8,128)(2,1)S(1)}, u32[]{:S(2)}, u32[]{:S(2)}) collective-permute-start(bf16[2048,128]{1,0:T(8,128)(2,1)S(1)} %bitcast.28), channel_id=1, source_target_pairs={{0,1},{1,0},{2,3},{3,2},{4,5},{5,4},{6,7},{7,6},{8,9},{9,8},{10,11... | collective-permute-start | bytes 1572872 | tf_op jit(solution)/shard_map/ppermute | solution.py:425
  69.3 29.5 %collective-permute-done.4.refs_3_ = bf16[2048,128]{1,0:T(8,128)(2,1)S(1)} collective-permute-done((bf16[2048,128]{1,0:T(8,128)(2,1)S(1)}, bf16[2048,128]{1,0:T(8,128)(2,1)S(1)}, u32[]{:S(2)}, u32[]{:S(2)}) %collective-permute-start.4) | collective-permute-done | bytes 524320 | tf_op jit(solution)/shard_map/ppermute | solution.py:424
  98.8 3.1 %collective-permute-start.5 = (bf16[2048,128]{1,0:T(8,128)(2,1)S(1)}, bf16[2048,128]{1,0:T(8,128)(2,1)S(1)}, u32[]{:S(2)}, u32[]{:S(2)}) collective-permute-start(bf16[2048,128]{1,0:T(8,128)(2,1)S(1)} %collective-permute-done.4.refs_3_), channel_id=1, source_target_pairs={{0,1},{1,0},{2,3},{3,2},{4,5},{5,4},{6,7},{7,6},{8,9},{9,8},{10,11... | collective-permute-start | bytes 1572872 | tf_op jit(solution)/shard_map/ppermute | solution.py:426
  101.9 1.5 collective-permute-done.5.refs_4_
  105.2 3.5 %down.1 = bf16[4,256,128]{2,1,0:T(8,128)(2,1)} custom-call(bf16[4,256,512]{2,1,0:T(8,128)(2,1)} %copy-done.2, bf16[2048,128]{1,0:T(8,128)(2,1)} %bitcast.26, bf16[2048,128]{1,0:T(8,128)(2,1)} %copy-done.10, bf16[2048,128]{1,0:T(8,128)(2,1)} %copy-done.9, bf16[2048,128]{1,0:T(8,128)(2,1)} %copy-done.11), custom_call_target="tpu_custom_call" | custom-call | tf_op jit(solution)/shard_map/down/pallas_call | solution.py:371
  108.7 11.8 %all-to-all-start.2 = ((bf16[128,8,128]{2,1,0:T(8,128)(2,1)}), bf16[128,8,128]{2,1,0:T(8,128)(2,1)S(1)}, u32[]{:S(2)}, u32[]{:S(2)}) async-start(bf16[128,8,128]{2,1,0:T(8,128)(2,1)} %bitcast.23), calls=%async_computation.2 | async-start | bytes 524288 | tf_op jit(solution)/shard_map/all_to_all | solution.py:431
  121.2 1.8 %choice.1 = (bf16[128,1024]{1,0:T(8,128)(2,1)}, bf16[128,1024]{1,0:T(8,128)(2,1)}) custom-call(s32[4,128]{1,0:T(4,128)} %bitcast.34, f32[4,128]{1,0:T(4,128)} %bitcast.35), custom_call_target="tpu_custom_call" | custom-call | tf_op jit(solution)/shard_map/choice/pallas_call | solution.py:301
  123.0 2.3 %shared_hidden.1 = bf16[128,128]{1,0:T(8,128)(2,1)} custom-call(bf16[128,2048]{1,0:T(8,128)(2,1)} %get-tuple-element.17.rows_ref, bf16[2048,128]{1,0:T(8,128)(2,1)} %gate_ref.1, bf16[2048,128]{1,0:T(8,128)(2,1)} %up_ref.1), custom_call_target="tpu_custom_call" | custom-call | tf_op jit(solution)/shard_map/shared_hidden/pallas_call | solution.py:333
  125.3 21.6 %all-gather.1 = bf16[2048,128]{1,0:T(8,128)(2,1)} all-gather(bf16[128,128]{1,0:T(8,128)(2,1)} %shared_hidden.1), channel_id=3, replica_groups=mesh['ep'=32,'yh'=4,'yl'=2,'co'=2] {'yh','yl','co'}, dimensions={0}, use_global_device_ids=true | all-gather | bytes 557056 | tf_op jit(solution)/shard_map/all_gather | solution.py:478
  146.8 2.1 %shared.1.shared_ref = f32[128,128]{1,0:T(8,128)} custom-call(bf16[16,128,128]{2,1,0:T(8,128)(2,1)} %bitcast.20, bf16[2048,128]{1,0:T(8,128)(2,1)} %w_ref.3), custom_call_target="tpu_custom_call" | custom-call | tf_op jit(solution)/shard_map/shared/pallas_call | solution.py:392
  149.0 1.6 slice.4.ends_ref
  150.5 2.5 %readout.1 = bf16[128,128]{1,0:T(8,128)(2,1)} custom-call(f32[32,8,256]{2,1,0:T(8,128)} %get-tuple-element.11.p_re, f32[32,8,256]{2,1,0:T(8,128)} %get-tuple-element.12.p_im, f32[32,8,256]{2,1,0:T(8,128)} %get-tuple-element.13.h_re, f32[32,8,256]{2,1,0:T(8,128)} %get-tuple-element.14.h_im, bf16[32,8,256]{2,1,0:T(8,128)(2,1)} %slice.4.ends_ref, ...), custom_call_target="tpu_custom_call" | custom-call | tf_op jit(solution)/shard_map/readout/pallas_call | solution.py:176
  153.0 17.5 %all-gather = bf16[2048,128]{1,0:T(8,128)(2,1)} all-gather(bf16[128,128]{1,0:T(8,128)(2,1)} %readout.1), channel_id=2, replica_groups=mesh['ep'=32,'yh'=4,'yl'=2,'co'=2] {'yh','yl','co'}, dimensions={0}, use_global_device_ids=true | all-gather | bytes 557056 | tf_op jit(solution)/shard_map/all_gather | solution.py:487
  170.6 2.3 %mixed.1 = bf16[256,128]{1,0:T(8,128)(2,1)} custom-call(bf16[16,128,128]{2,1,0:T(8,128)(2,1)} %bitcast.19, f32[16,64]{1,0:T(8,128)} %reshape.36.scale_ref, bf16[1024,128]{1,0:T(8,128)(2,1)} %w_ref.2), custom_call_target="tpu_custom_call" | custom-call | tf_op jit(solution)/shard_map/mixed/pallas_call | solution.py:213
  173.6 2.0 %combine.1 = bf16[128,128]{1,0:T(8,128)(2,1)} custom-call(f32[128,128]{1,0:T(8,128)} %shared.1.shared_ref, bf16[1024,128]{1,0:T(8,128)(2,1)} %bitcast.22, bf16[128,1024]{1,0:T(8,128)(2,1)} %get-tuple-element.18.high_ref, bf16[128,1024]{1,0:T(8,128)(2,1)} %get-tuple-element.19.low_ref), custom_call_target="tpu_custom_call" | custom-call | tf_op jit(solution)/shard_map/combine/pallas_call | solution.py:410
  (34 shorter events, 6.7 us)
Async XLA Ops:
  5.4 13.9 %copy-start.6 = (bf16[1,2048,128]{2,1,0:T(8,128)(2,1)S(1)}, bf16[1,2048,128]{2,1,0:T(8,128)(2,1)}, u32[]{:S(2)}) copy-start(bf16[1,2048,128]{2,1,0:T(8,128)(2,1)} %param.35) | copy-start | bytes 1572868
  5.4 13.9 %copy-start.7 = (bf16[1,2048,128]{2,1,0:T(8,128)(2,1)S(1)}, bf16[1,2048,128]{2,1,0:T(8,128)(2,1)}, u32[]{:S(2)}) copy-start(bf16[1,2048,128]{2,1,0:T(8,128)(2,1)} %param.34) | copy-start | bytes 1572868
  5.4 45.8 %all-to-all-start = ((bf16[32,8,2304]{2,1,0:T(8,128)(2,1)}), bf16[32,8,2304]{2,1,0:T(8,128)(2,1)S(1)}, u32[]{:S(2)}, u32[]{:S(2)}) async-start(bf16[32,8,2304]{2,1,0:T(8,128)(2,1)} %bitcast.21), calls=%async_computation | async-start | bytes 2359296 | tf_op jit(solution)/shard_map/all_to_all | solution.py:431
  19.4 31.8 %copy-start.1 = (bf16[2048,256]{1,0:T(8,128)(2,1)}, bf16[2048,256]{1,0:T(8,128)(2,1)S(1)}, u32[]{:S(2)}) copy-start(bf16[2048,256]{1,0:T(8,128)(2,1)S(1)} %pad_maximum_fusion.refs_0_) | copy-start | bytes 3145732
  19.4 25.6 %collective-permute-start.1 = (bf16[2048,256]{1,0:T(8,128)(2,1)S(1)}, bf16[2048,256]{1,0:T(8,128)(2,1)S(1)}, u32[]{:S(2)}, u32[]{:S(2)}) collective-permute-start(bf16[2048,256]{1,0:T(8,128)(2,1)S(1)} %pad_maximum_fusion.refs_0_), channel_id=1, source_target_pairs={{0,2},{2,0},{1,3},{3,1},{4,6},{6,4},{5,7},{7,5},{8,10},{10,8},{9,1... | collective-permute-start | bytes 3145736 | tf_op jit(solution)/shard_map/ppermute | solution.py:424
  22.6 26.2 %collective-permute-start = (bf16[2048,256]{1,0:T(8,128)(2,1)S(1)}, bf16[2048,256]{1,0:T(8,128)(2,1)S(1)}, u32[]{:S(2)}, u32[]{:S(2)}) collective-permute-start(bf16[2048,256]{1,0:T(8,128)(2,1)S(1)} %pad_maximum_fusion.refs_0_), channel_id=1, source_target_pairs={{0,1},{1,0},{2,3},{3,2},{4,5},{5,4},{6,7},{7,6},{8,9},{9,8},{10,11... | collective-permute-start | bytes 3145736 | tf_op jit(solution)/shard_map/ppermute | solution.py:425
  45.1 6.1 %copy-start.3 = (bf16[2048,256]{1,0:T(8,128)(2,1)}, bf16[2048,256]{1,0:T(8,128)(2,1)S(1)}, u32[]{:S(2)}) copy-start(bf16[2048,256]{1,0:T(8,128)(2,1)S(1)} %collective-permute-done.1.refs_2_) | copy-start | bytes 3145732
  45.1 6.1 %collective-permute-start.2 = (bf16[2048,256]{1,0:T(8,128)(2,1)S(1)}, bf16[2048,256]{1,0:T(8,128)(2,1)}, u32[]{:S(2)}, u32[]{:S(2)}) collective-permute-start(bf16[2048,256]{1,0:T(8,128)(2,1)S(1)} %collective-permute-done.1.refs_2_), channel_id=1, source_target_pairs={{0,1},{1,0},{2,3},{3,2},{4,5},{5,4},{6,7},{7,6},{8,9},{9,8},{10,11... | collective-permute-start | bytes 3145736 | tf_op jit(solution)/shard_map/ppermute | solution.py:426
  48.8 1.0 copy-start.4
  51.2 1.1 copy-start
  57.0 7.0 %copy-start.8 = (bf16[1,2048,128]{2,1,0:T(8,128)(2,1)S(1)}, bf16[1,2048,128]{2,1,0:T(8,128)(2,1)}, u32[]{:S(2)}) copy-start(bf16[1,2048,128]{2,1,0:T(8,128)(2,1)} %param.36) | copy-start | bytes 1572868
  57.0 46.4 %all-to-all-start.1 = ((bf16[4,256,512]{2,1,0:T(8,128)(2,1)}), bf16[4,256,512]{2,1,0:T(8,128)(2,1)S(1)}, u32[]{:S(2)}, u32[]{:S(2)}) async-start(bf16[4,256,512]{2,1,0:T(8,128)(2,1)} %hidden.1), calls=%async_computation.1 | async-start | bytes 2097152 | tf_op jit(solution)/shard_map/all_to_all | solution.py:431
  64.0 56.5 %copy-start.12 = (f32[1024]{0:T(1024)S(1)}, f32[1024]{0:T(1024)}, u32[]{:S(2)}) copy-start(f32[1024]{0:T(1024)} %param.28) | copy-start | bytes 12292
  64.0 34.8 %collective-permute-start.4 = (bf16[2048,128]{1,0:T(8,128)(2,1)S(1)}, bf16[2048,128]{1,0:T(8,128)(2,1)S(1)}, u32[]{:S(2)}, u32[]{:S(2)}) collective-permute-start(bf16[2048,128]{1,0:T(8,128)(2,1)S(1)} %bitcast.27), channel_id=1, source_target_pairs={{0,2},{2,0},{1,3},{3,1},{4,6},{6,4},{5,7},{7,5},{8,10},{10,8},{9,1... | collective-permute-start | bytes 1572872 | tf_op jit(solution)/shard_map/ppermute | solution.py:424
  66.4 35.5 %collective-permute-start.3 = (bf16[2048,128]{1,0:T(8,128)(2,1)S(1)}, bf16[2048,128]{1,0:T(8,128)(2,1)S(1)}, u32[]{:S(2)}, u32[]{:S(2)}) collective-permute-start(bf16[2048,128]{1,0:T(8,128)(2,1)S(1)} %bitcast.28), channel_id=1, source_target_pairs={{0,1},{1,0},{2,3},{3,2},{4,5},{5,4},{6,7},{7,6},{8,9},{9,8},{10,11... | collective-permute-start | bytes 1572872 | tf_op jit(solution)/shard_map/ppermute | solution.py:425
  98.8 4.7 %copy-start.9 = (bf16[2048,128]{1,0:T(8,128)(2,1)}, bf16[2048,128]{1,0:T(8,128)(2,1)S(1)}, u32[]{:S(2)}) copy-start(bf16[2048,128]{1,0:T(8,128)(2,1)S(1)} %collective-permute-done.4.refs_3_) | copy-start | bytes 1572868
  98.8 4.6 %collective-permute-start.5 = (bf16[2048,128]{1,0:T(8,128)(2,1)S(1)}, bf16[2048,128]{1,0:T(8,128)(2,1)S(1)}, u32[]{:S(2)}, u32[]{:S(2)}) collective-permute-start(bf16[2048,128]{1,0:T(8,128)(2,1)S(1)} %collective-permute-done.4.refs_3_), channel_id=1, source_target_pairs={{0,1},{1,0},{2,3},{3,2},{4,5},{5,4},{6,7},{7,6},{8,9},{9,8},{10,11... | collective-permute-start | bytes 1572872 | tf_op jit(solution)/shard_map/ppermute | solution.py:426
  101.9 1.5 copy-start.10
  103.4 0.8 copy-start.11
  104.2 1.0 copy-start.2
  108.7 64.2 %all-to-all-start.2 = ((bf16[128,8,128]{2,1,0:T(8,128)(2,1)}), bf16[128,8,128]{2,1,0:T(8,128)(2,1)S(1)}, u32[]{:S(2)}, u32[]{:S(2)}) async-start(bf16[128,8,128]{2,1,0:T(8,128)(2,1)} %bitcast.23), calls=%async_computation.2 | async-start | bytes 524288 | tf_op jit(solution)/shard_map/all_to_all | solution.py:431
  172.9 0.7 copy-start.5

commit v3 on v2

--- a/solution.py
+++ b/solution.py
@@ -124,13 +124,13 @@
     return jnp.concatenate([high, (ends - high.astype(F32)).astype(BF16)], axis=1)
 
 
-def readout_kernel(p_re, p_im, h_re, h_im, ends_ref, through_ref, wout_ref, out_ref, turned):
+def readout_part(p_re, p_im, h_re, h_im, ends_ref, through_ref, wout_ref, turned):
     length, chunks, half = p_re.shape
     positions, width = through_ref.shape
     index = lax.axis_index("ep")
     cr = ci = jnp.zeros((1, half), F32)
     for b in range(ends_ref.shape[0] - 1):
-        end = ends_ref[b].astype(F32)
+        end = ends_ref[b, :, ends_ref.shape[2] - 256 :].astype(F32)
         end = end[:, :128] + end[:, 128:]
         ar, ai, er, ei = (
             jnp.concatenate([end[q : q + 1], end[q + 4 : q + 5]], axis=1) for q in range(4)
@@ -168,55 +168,71 @@
     v = turned[:, :width] + through_ref[...]
     v = 0.5 * v * (1.0 + jnp.tanh(0.7978845608028654 * (v + 0.044715 * (v * v * v))))
     both = positions // 2
-    out_ref[...] = jnp.concatenate([v[:both], v[both:]], axis=1).astype(BF16)
-
-
-def run_readout(pieces, ends, through, wout):
-    positions, width = through.shape
-    return pl.pallas_call(
-        readout_kernel,
-        out_shape=jax.ShapeDtypeStruct((positions // 2, 2 * width), BF16),
-        in_specs=vmem(7),
-        out_specs=pl.BlockSpec(memory_space=VM),
-        scratch_shapes=[VM((positions, 128), F32)],
-        name="readout",
-    )(*pieces, ends, through, wout)
-
-
-def mixed_kernel(rows_ref, scale_ref, w_ref, out_ref):
-    blocks, both, lanes = rows_ref.shape
+    return jnp.concatenate([v[:both], v[both:]], axis=1).astype(BF16)
+
+
+def block_of(ref, member, part):
+    rows = ref.shape[1] // 2
+    lanes = 128
+    return jnp.concatenate(
+        [
+            ref[member, part * rows : (part + 1) * rows, i * lanes : (i + 1) * lanes]
+            for i in range(ref.shape[2] // lanes)
+        ],
+        axis=0,
+    )
+
+
+def third_kernel(*refs):
+    pieces, (scale_ref, w_ref, down_ref, mixed_ref, shared_ref) = refs[:4], refs[4:]
+    sub = own_sub()
+    members = pieces[0].shape[0]
+    places = [(m, q) for m in range(members) for q in range(4)]
+    blocks = [block_of(pieces[q], m, 0) for m, q in places]
+    both, lanes = blocks[0].shape
     width = lanes // 2
     total = None
-    for d in range(blocks):
-        v = rows_ref[d].astype(F32)
+    for v in blocks:
+        v = v.astype(F32)
         total = v * v if total is None else total + v * v
     first = iota((both, lanes), 1) < width
-    count = 1.0 / (blocks * width)
+    count = 1.0 / (len(places) * width)
     sums = [jnp.sum(jnp.where(m, total, 0.0), axis=1, keepdims=True) for m in (first, ~first)]
     f0, f1 = (lax.rsqrt(s * count + EPS) for s in sums)
     factor = jnp.where(first, f0, f1)
     acc = [jnp.zeros((both, w_ref.shape[1]), F32)] * 2
-    for d in range(blocks):
-        gain = jnp.concatenate([scale_ref[d : d + 1, :]] * 2, axis=1)
-        v = (rows_ref[d].astype(F32) * factor * gain).astype(BF16)
-        w = w_ref[d * width : (d + 1) * width, :]
+    shared = jnp.zeros(shared_ref.shape, F32)
+    for (m, q), block in zip(places, blocks):
+        d = m * 4 + (sub ^ q)
+        gain = jnp.concatenate([scale_ref[pl.ds(d, 1), :]] * 2, axis=1)
+        v = (block.astype(F32) * factor * gain).astype(BF16)
+        w = w_ref[pl.ds(pl.multiple_of(d * width, width), width), :]
         w2 = jnp.concatenate([w, w], axis=0)
-        for k, m in enumerate((first, ~first)):
-            part = jnp.where(m, v, jnp.zeros_like(v))
+        for k, half in enumerate((first, ~first)):
+            part = jnp.where(half, v, jnp.zeros_like(v))
             acc[k] = acc[k] + jnp.dot(part, w2, preferred_element_type=F32)
-    out_ref[:both, :] = acc[0].astype(BF16)
-    out_ref[both:, :] = acc[1].astype(BF16)
-
-
-def run_mixed(rows, scale, w):
-    blocks, both, lanes = rows.shape
-    return pl.pallas_call(
-        mixed_kernel,
-        out_shape=jax.ShapeDtypeStruct((2 * both, w.shape[1]), BF16),
-        in_specs=vmem(3),
-        out_specs=pl.BlockSpec(memory_space=VM),
-        name="mixed",
-    )(rows, scale.reshape(blocks, lanes // 2), w)
+        shared = shared + jnp.dot(
+            block_of(pieces[q], m, 1),
+            down_ref[pl.ds(pl.multiple_of(d * lanes, lanes), lanes), :],
+            preferred_element_type=F32,
+        )
+    mixed_ref[:both, :] = acc[0].astype(BF16)
+    mixed_ref[both:, :] = acc[1].astype(BF16)
+    shared_ref[...] = shared
+
+
+def run_third(pieces, scale, w, down, positions, tokens):
+    lanes = w.shape[1]
+    return pl.pallas_call(
+        third_kernel,
+        out_shape=[
+            jax.ShapeDtypeStruct((positions, lanes), BF16),
+            jax.ShapeDtypeStruct((tokens, lanes), F32),
+        ],
+        in_specs=vmem(7),
+        out_specs=vmem(2),
+        name="third",
+    )(*pieces, scale.reshape(pieces[0].shape[0] * 4, -1), w, down)
 
 
 def expert_table(routes_ref, weights_ref, experts):
@@ -313,14 +329,41 @@
     return (gate / (1.0 + jnp.exp(-gate)) * up).astype(BF16)
 
 
-def hidden_kernel(rows_ref, *refs):
-    *weights, out_ref = refs
-    rows = rows_ref[:, : weights[0].shape[0]]
-    for q, w in enumerate(weights):
-        half = w.shape[1] // 2
-        got = gated(jnp.dot(rows, w[...], preferred_element_type=F32))
-        for copy in range(out_ref.shape[0]):
-            out_ref[copy, :, q * half : (q + 1) * half] = got
+def second_kernel(arrived_ref, extra_ref, *refs):
+    gates, ups, readout_in, (out_ref, turned) = refs[:4], refs[4:8], refs[8:14], refs[14:]
+    mix = readout_part(*readout_in[:4], arrived_ref, *readout_in[4:], turned)
+    blocks, share, _ = arrived_ref.shape
+    rows = arrived_ref[:, :, : gates[0].shape[0]].reshape(blocks * share, -1)
+    copies, _, wide = out_ref.shape
+    lanes = mix.shape[1]
+    for q, (gate, up) in enumerate(zip(gates, ups)):
+        both = jnp.concatenate([gate[...], up[...]], axis=1)
+        got = gated(jnp.dot(rows, both, preferred_element_type=F32))
+        for copy in range(copies):
+            out_ref[copy, : blocks * share, q * lanes : (q + 1) * lanes] = got
+    at = blocks * share
+    for item in (mix, extra_ref[...]):
+        part = item.shape[0] * lanes // wide
+        for i in range(wide // lanes):
+            for copy in range(copies):
+                out_ref[copy, at : at + part, i * lanes : (i + 1) * lanes] = item[
+                    i * part : (i + 1) * part
+                ]
+        at += part
+
+
+def run_second(arrived, extra, gates, ups, pieces, through, wout, copies):
+    blocks, share, _ = arrived.shape
+    wide = 4 * gates[0].shape[1]
+    rows = blocks * share + (through.size + extra.size) // wide
+    return pl.pallas_call(
+        second_kernel,
+        out_shape=jax.ShapeDtypeStruct((copies, rows, wide), BF16),
+        in_specs=vmem(16),
+        out_specs=pl.BlockSpec(memory_space=VM),
+        scratch_shapes=[VM((through.shape[0], 128), F32)],
+        name="second",
+    )(arrived, extra, *gates, *ups, *pieces, through, wout)
 
 
 def shared_hidden_kernel(rows_ref, gate_ref, up_ref, out_ref):
@@ -337,17 +380,6 @@
         out_specs=pl.BlockSpec(memory_space=VM),
         name="shared_hidden",
     )(rows, gate, up)
-
-
-def run_hidden(rows, weights, copies):
-    half = weights[0].shape[1] // 2
-    return pl.pallas_call(
-        hidden_kernel,
-        out_shape=jax.ShapeDtypeStruct((copies, rows.shape[0], half * len(weights)), BF16),
-        in_specs=vmem(1 + len(weights)),
-        out_specs=pl.BlockSpec(memory_space=VM),
-        name="hidden",
-    )(rows, *weights)
 
 
 def down_kernel(*refs):
@@ -357,7 +389,7 @@
     for member in range(hidden.shape[0]):
         for q in range(4):
             at = pl.multiple_of((member * 4 + (sub ^ q)) * lanes, lanes)
-            whole[:, pl.ds(at, lanes)] = hidden[member, :, q * lanes : (q + 1) * lanes]
+            whole[:, pl.ds(at, lanes)] = hidden[member, : whole.shape[0], q * lanes : (q + 1) * lanes]
     rows = whole[...]
     for q in (0, 2):
         both = jnp.concatenate([weights[q][...], weights[q + 1][...]], axis=1)
@@ -366,8 +398,8 @@
         out_ref[sub ^ (q + 1)] = got[:, lanes:]
 
 
-def run_down(hidden, weights):
-    rows, lanes = hidden.shape[1], weights[0].shape[1]
+def run_down(hidden, weights, rows):
+    lanes = weights[0].shape[1]
     return pl.pallas_call(
         down_kernel,
         out_shape=jax.ShapeDtypeStruct((4, rows, lanes), BF16),
@@ -376,26 +408,6 @@
         scratch_shapes=[VM((rows, weights[0].shape[0]), BF16)],
         name="down",
     )(hidden, *weights)
-
-
-def shared_kernel(blocks_ref, w_ref, out_ref):
-    blocks, tokens, lanes = blocks_ref.shape
-    total = jnp.zeros((tokens, w_ref.shape[1]), F32)
-    for d in range(blocks):
-        total = total + jnp.dot(
-            blocks_ref[d], w_ref[d * lanes : (d + 1) * lanes, :], preferred_element_type=F32
-        )
-    out_ref[...] = total
-
-
-def run_shared(blocks, w):
-    return pl.pallas_call(
-        shared_kernel,
-        out_shape=jax.ShapeDtypeStruct((blocks.shape[1], w.shape[1]), F32),
-        in_specs=vmem(2),
-        out_specs=pl.BlockSpec(memory_space=VM),
-        name="shared",
-    )(blocks, w)
 
 
 def combine_kernel(shared_ref, back_ref, high_ref, low_ref, out_ref):
@@ -454,7 +466,6 @@
     shared_down_weight,
 ):
     blocks = lax.axis_size("ep")
-    width = second_micro_input.shape[1]
     routes = routes.T
     normed, sent, *pieces, through = run_first(
         second_micro_input,
@@ -470,28 +481,38 @@
         channel_feedthrough.reshape(1, -1),
     )
     arrived = spread_out(sent.reshape(blocks, 8, -1), "ep")
-    both = jnp.concatenate([expert_gate_weight[0], expert_up_weight[0]], axis=1)
-    gates = exchanged(both)
+    gates = exchanged(expert_gate_weight[0])
+    ups = exchanged(expert_up_weight[0])
     downs = exchanged(expert_down_weight[0])
-
     shared_hidden = run_shared_hidden(normed, shared_gate_weight, shared_up_weight)
-    shared_rows = lax.all_gather(shared_hidden, TP, axis=0)
-    shared = run_shared(shared_rows, shared_down_weight)
-
-    ssm_out = run_readout(
+    high, low = run_choice(routes, chosen_expert_weight.T, blocks * 32)
+
+    hidden = run_second(
+        arrived,
+        shared_hidden,
+        gates,
+        ups,
         pieces,
-        arrived[:, :, width:],
         through,
         group_output_matrices.reshape(-1, frequency.shape[1]),
-    )
-    whole_rows = lax.all_gather(ssm_out, TP, axis=0)
-    mixed = run_mixed(whole_rows, mixer_norm_scale, mixer_output_weight)
-    high, low = run_choice(routes, chosen_expert_weight.T, blocks * 32)
-
-    hidden = run_hidden(arrived.reshape(blocks * 8, -1), gates, lax.axis_size("yh"))
+        lax.axis_size("yh"),
+    )
     hidden = spread_out(hidden, "yh")
-    results = run_down(hidden, downs).reshape(4 * blocks, 8, -1)
+    results = run_down(hidden, downs, blocks * 8).reshape(4 * blocks, 8, -1)
     back = spread_out(results, ("yl", "co", "ep")).reshape(blocks * 32, -1)
+
+    own = hidden[:, blocks * 8 :]
+    core = lax.ppermute(own, "co", SWAP)
+    over = lax.ppermute(own, "yl", SWAP)
+    both = lax.ppermute(core, "yl", SWAP)
+    mixed, shared = run_third(
+        (own, core, over, both),
+        mixer_norm_scale,
+        mixer_output_weight,
+        shared_down_weight,
+        through.shape[0],
+        routes.shape[1],
+    )
     return (mixed, run_combine(shared, back, high, low))
 
 

time: 176 us -> 149 us (0.85)
  blocking collectives: 39.1 us -> 0 us
  starting transfers between devices: 51 us -> 67.5 us
  Pallas kernels: 26.2 us -> 23 us
  local copies, waits for them, and re-layouts: 6.74 us -> 3.89 us
    all_gather x2 -> x0, blocking collectives: 39.1 us -> none  [the longest x1 21.6 us: on_device(): shared_rows = lax.all_gather(shared_hidden, TP, axis=0)]
    ppermute x0 -> x3, starting transfers between devices: none -> 7.67 us  [the longest x1 3.7 us: on_device(): over = lax.ppermute(own, 'yl', SWAP)]
    ppermute x0 -> x3, waiting for transfers between devices: none -> 7.56 us  [the longest x1 5.61 us: on_device(): both = lax.ppermute(core, 'yl', SWAP)]
    ppermute x2 -> x3, starting transfers between devices: 6.84 us -> 11.7 us  [exchanged(): both = lax.ppermute(over, 'co', SWAP)]
    pallas_call x4 -> x2, Pallas kernels: 11.8 us -> 8.42 us  [the longest x1 5.59 us: run_second(): pl.pallas_call(second_kernel, out_shape=jax.ShapeDtypeStruct((copies, row...]
    ppermute x2 -> x3, waiting for transfers between devices: 48.8 us -> 45.7 us  [exchanged(): over = lax.ppermute(piece, 'yl', SWAP)]
    ppermute x2 -> x3, waiting for transfers between devices: 2.9 us -> 0.01 us  [exchanged(): both = lax.ppermute(over, 'co', SWAP)]
    ppermute x2 -> x3, starting transfers between devices: 5.63 us -> 7.58 us  [exchanged(): over = lax.ppermute(piece, 'yl', SWAP)]
  transfers between devices with their start and end apart: 9 -> 15, of which waited for: 4 -> 5; matrix products, arithmetic and copies ran while one was open for 1% -> 0% of each run, Pallas kernels for 6% -> 7%
where the time goes in v3:
time: 149 us
  starting transfers between devices  67.5 us (45%)
  waiting for transfers between devices  53.3 us (36%)
  Pallas kernels  23 us (15%)
  local copies, waits for them, and re-layouts  3.89 us (3%)
    ppermute x3, waiting for transfers between devices, exchanged(): over = lax.ppermute(piece, 'yl', SWAP)  45.7 us
    all_to_all x3, starting transfers between devices, spread_out(): return lax.all_to_all(pieces, axes, split_axis=0, concat_axis=0, tiled=True)  32.7 us
    ppermute x3, starting transfers between devices, exchanged(): both = lax.ppermute(over, 'co', SWAP)  11.7 us
    ppermute x3, starting transfers between devices, exchanged(): core = lax.ppermute(piece, 'co', SWAP)  7.87 us
    ppermute x3, starting transfers between devices, exchanged(): over = lax.ppermute(piece, 'yl', SWAP)  7.58 us
    ppermute x1, waiting for transfers between devices, on_device(): both = lax.ppermute(core, 'yl', SWAP)  5.61 us
    pallas_call x1, Pallas kernels, run_second(): pl.pallas_call(second_kernel, out_shape=jax.ShapeDtypeStruct((copies, row...  5.59 us
    pallas_call x1, Pallas kernels, run_first(): pl.pallas_call(first_kernel, out_shape=[jax.ShapeDtypeStruct(tokens.shape...  4.77 us
  transfers between devices with their start and end apart: 15, of which 5 were waited for; matrix products, arithmetic and copies ran while one was open for 0% of the time, Pallas kernels for 7%

profile of v3, /device:TPU:1, one launch (start us, length us, event | category | flops | bytes accessed | tf_op | source)
XLA Modules:
  0.0 148.6 jit_solution(6570554659848241746)
XLA Ops:
  0.6 4.8 %first.1 = (bf16[128,2048]{1,0:T(8,128)(2,1)}, bf16[256,2304]{1,0:T(8,128)(2,1)}, f32[32,8,256]{2,1,0:T(8,128)}, f32[32,8,256]{2,1,0:T(8,128)}, f32[32,8,256]{2,...) custom-call(bf16[128,2048]{1,0:T(8,128)(2,1)} %tokens_ref.1, f32[1,2048]{1,0:T(1,128)} %bitcast.30, ...), custom_call_target="tpu_custom_call" | custom-call | tf_op jit(solution)/shard_map/first/pallas_call | solution.py:281
  5.4 13.8 %all-to-all-start = ((bf16[32,8,2304]{2,1,0:T(8,128)(2,1)}), bf16[32,8,2304]{2,1,0:T(8,128)(2,1)S(1)}, u32[]{:S(2)}, u32[]{:S(2)}) async-start(bf16[32,8,2304]{2,1,0:T(8,128)(2,1)} %bitcast.15), calls=%async_computation | async-start | bytes 2359296 | tf_op jit(solution)/shard_map/all_to_all | solution.py:443
  19.3 3.2 %collective-permute-start.1 = (bf16[2048,128]{1,0:T(8,128)(2,1)S(1)}, bf16[2048,128]{1,0:T(8,128)(2,1)S(1)}, u32[]{:S(2)}, u32[]{:S(2)}) collective-permute-start(bf16[2048,128]{1,0:T(8,128)(2,1)S(1)} %bitcast.22), channel_id=1, source_target_pairs={{0,2},{2,0},{1,3},{3,1},{4,6},{6,4},{5,7},{7,5},{8,10},{10,8},{9,1... | collective-permute-start | bytes 1572872 | tf_op jit(solution)/shard_map/ppermute | solution.py:436
  22.5 2.1 %collective-permute-start.4 = (bf16[2048,128]{1,0:T(8,128)(2,1)S(1)}, bf16[2048,128]{1,0:T(8,128)(2,1)S(1)}, u32[]{:S(2)}, u32[]{:S(2)}) collective-permute-start(bf16[2048,128]{1,0:T(8,128)(2,1)S(1)} %bitcast.25), channel_id=1, source_target_pairs={{0,2},{2,0},{1,3},{3,1},{4,6},{6,4},{5,7},{7,5},{8,10},{10,8},{9,1... | collective-permute-start | bytes 1572872 | tf_op jit(solution)/shard_map/ppermute | solution.py:436
  24.6 3.4 %collective-permute-start = (bf16[2048,128]{1,0:T(8,128)(2,1)S(1)}, bf16[2048,128]{1,0:T(8,128)(2,1)}, u32[]{:S(2)}, u32[]{:S(2)}) collective-permute-start(bf16[2048,128]{1,0:T(8,128)(2,1)S(1)} %bitcast.23), channel_id=1, source_target_pairs={{0,1},{1,0},{2,3},{3,2},{4,5},{5,4},{6,7},{7,6},{8,9},{9,8},{10,11... | collective-permute-start | bytes 1572872 | tf_op jit(solution)/shard_map/ppermute | solution.py:437
  30.0 3.7 %collective-permute-done.1.refs_2_ = bf16[2048,128]{1,0:T(8,128)(2,1)S(1)} collective-permute-done((bf16[2048,128]{1,0:T(8,128)(2,1)S(1)}, bf16[2048,128]{1,0:T(8,128)(2,1)S(1)}, u32[]{:S(2)}, u32[]{:S(2)}) %collective-permute-start.1) | collective-permute-done | bytes 524320 | tf_op jit(solution)/shard_map/ppermute | solution.py:436
  33.7 5.1 %collective-permute-start.2 = (bf16[2048,128]{1,0:T(8,128)(2,1)S(1)}, bf16[2048,128]{1,0:T(8,128)(2,1)}, u32[]{:S(2)}, u32[]{:S(2)}) collective-permute-start(bf16[2048,128]{1,0:T(8,128)(2,1)S(1)} %collective-permute-done.1.refs_2_), channel_id=1, source_target_pairs={{0,1},{1,0},{2,3},{3,2},{4,5},{5,4},{6,7},{7,6},{8,9},{9,8},{10,11... | collective-permute-start | bytes 1572872 | tf_op jit(solution)/shard_map/ppermute | solution.py:438
  38.8 6.1 %collective-permute-done.4.refs_6_ = bf16[2048,128]{1,0:T(8,128)(2,1)S(1)} collective-permute-done((bf16[2048,128]{1,0:T(8,128)(2,1)S(1)}, bf16[2048,128]{1,0:T(8,128)(2,1)S(1)}, u32[]{:S(2)}, u32[]{:S(2)}) %collective-permute-start.4) | collective-permute-done | bytes 524320 | tf_op jit(solution)/shard_map/ppermute | solution.py:436
  44.9 3.7 %collective-permute-start.5 = (bf16[2048,128]{1,0:T(8,128)(2,1)S(1)}, bf16[2048,128]{1,0:T(8,128)(2,1)}, u32[]{:S(2)}, u32[]{:S(2)}) collective-permute-start(bf16[2048,128]{1,0:T(8,128)(2,1)S(1)} %collective-permute-done.4.refs_6_), channel_id=1, source_target_pairs={{0,1},{1,0},{2,3},{3,2},{4,5},{5,4},{6,7},{7,6},{8,9},{9,8},{10,11... | collective-permute-start | bytes 1572872 | tf_op jit(solution)/shard_map/ppermute | solution.py:438
  48.6 2.3 %shared_hidden.1.extra_ref = bf16[128,128]{1,0:T(8,128)(2,1)} custom-call(bf16[128,2048]{1,0:T(8,128)(2,1)} %get-tuple-element.14.rows_ref, bf16[2048,128]{1,0:T(8,128)(2,1)} %gate_ref.1, bf16[2048,128]{1,0:T(8,128)(2,1)} %up_ref.1), custom_call_target="tpu_custom_call" | custom-call | tf_op jit(solution)/shard_map/shared_hidden/pallas_call | solution.py:376
  52.0 5.6 %second.1 = bf16[4,320,512]{2,1,0:T(8,128)(2,1)} custom-call(bf16[32,8,2304]{2,1,0:T(8,128)(2,1)} %copy-done.1, bf16[128,128]{1,0:T(8,128)(2,1)} %shared_hidden.1.extra_ref, bf16[2048,128]{1,0:T(8,128)(2,1)} %bitcast.21, bf16[2048,128]{1,0:T(8,128)(2,1)} %collective-permute-done.refs_1_, bf16[2048,128]{1,0:T(8,128)(2,1)} %copy-done.9, ...), custom_call_target="tpu_custom_call" | custom-call | tf_op jit(solution)/shard_map/second/pallas_call | solution.py:359
  57.6 6.9 %all-to-all-start.1 = ((bf16[4,320,512]{2,1,0:T(8,128)(2,1)}), bf16[4,320,512]{2,1,0:T(8,128)(2,1)S(1)}, u32[]{:S(2)}, u32[]{:S(2)}) async-start(bf16[4,320,512]{2,1,0:T(8,128)(2,1)} %second.1), calls=%async_computation.1 | async-start | bytes 2621440 | tf_op jit(solution)/shard_map/all_to_all | solution.py:443
  64.6 2.3 %collective-permute-start.10 = (bf16[2048,128]{1,0:T(8,128)(2,1)S(1)}, bf16[2048,128]{1,0:T(8,128)(2,1)S(1)}, u32[]{:S(2)}, u32[]{:S(2)}) collective-permute-start(bf16[2048,128]{1,0:T(8,128)(2,1)S(1)} %bitcast.19), channel_id=1, source_target_pairs={{0,2},{2,0},{1,3},{3,1},{4,6},{6,4},{5,7},{7,5},{8,10},{10,8},{9,1... | collective-permute-start | bytes 1572872 | tf_op jit(solution)/shard_map/ppermute | solution.py:436
  66.9 2.5 %collective-permute-start.9 = (bf16[2048,128]{1,0:T(8,128)(2,1)S(1)}, bf16[2048,128]{1,0:T(8,128)(2,1)S(1)}, u32[]{:S(2)}, u32[]{:S(2)}) collective-permute-start(bf16[2048,128]{1,0:T(8,128)(2,1)S(1)} %bitcast.20), channel_id=1, source_target_pairs={{0,1},{1,0},{2,3},{3,2},{4,5},{5,4},{6,7},{7,6},{8,9},{9,8},{10,11... | collective-permute-start | bytes 1572872 | tf_op jit(solution)/shard_map/ppermute | solution.py:437
  69.4 35.9 %collective-permute-done.10.refs_3_ = bf16[2048,128]{1,0:T(8,128)(2,1)S(1)} collective-permute-done((bf16[2048,128]{1,0:T(8,128)(2,1)S(1)}, bf16[2048,128]{1,0:T(8,128)(2,1)S(1)}, u32[]{:S(2)}, u32[]{:S(2)}) %collective-permute-start.10) | collective-permute-done | bytes 524320 | tf_op jit(solution)/shard_map/ppermute | solution.py:436
  105.3 2.8 %collective-permute-start.11 = (bf16[2048,128]{1,0:T(8,128)(2,1)S(1)}, bf16[2048,128]{1,0:T(8,128)(2,1)}, u32[]{:S(2)}, u32[]{:S(2)}) collective-permute-start(bf16[2048,128]{1,0:T(8,128)(2,1)S(1)} %collective-permute-done.10.refs_3_), channel_id=1, source_target_pairs={{0,1},{1,0},{2,3},{3,2},{4,5},{5,4},{6,7},{7,6},{8,9},{9,8},{10,11... | collective-permute-start | bytes 1572872 | tf_op jit(solution)/shard_map/ppermute | solution.py:438
  108.1 2.1 %collective-permute-start.6 = (bf16[4,64,512]{2,1,0:T(8,128)(2,1)S(1)}, bf16[4,64,512]{2,1,0:T(8,128)(2,1)S(1)}, u32[]{:S(2)}, u32[]{:S(2)}) collective-permute-start(bf16[4,64,512]{2,1,0:T(8,128)(2,1)S(1)} %slice.4.refs_0_), channel_id=1, source_target_pairs={{0,1},{1,0},{2,3},{3,2},{4,5},{5,4},{6,7},{7,6},{8,9},{9,8},{10,11... | collective-permute-start | bytes 786440 | tf_op jit(solution)/shard_map/ppermute | solution.py:505
  111.0 3.6 %down.1 = bf16[4,256,128]{2,1,0:T(8,128)(2,1)} custom-call(bf16[4,320,512]{2,1,0:T(8,128)(2,1)} %copy-done, bf16[2048,128]{1,0:T(8,128)(2,1)} %bitcast.18, bf16[2048,128]{1,0:T(8,128)(2,1)} %copy-done.6, bf16[2048,128]{1,0:T(8,128)(2,1)} %copy-done.5, bf16[2048,128]{1,0:T(8,128)(2,1)} %collective-permute-done.11.refs_4_), custom_call_target="tpu_custom_call" | custom-call | tf_op jit(solution)/shard_map/down/pallas_call | solution.py:403
  114.6 12.0 %all-to-all-start.2 = ((bf16[128,8,128]{2,1,0:T(8,128)(2,1)}), bf16[128,8,128]{2,1,0:T(8,128)(2,1)S(1)}, u32[]{:S(2)}, u32[]{:S(2)}) async-start(bf16[128,8,128]{2,1,0:T(8,128)(2,1)} %bitcast.16), calls=%async_computation.2 | async-start | bytes 524288 | tf_op jit(solution)/shard_map/all_to_all | solution.py:443
  126.6 3.7 %collective-permute-start.7 = (bf16[4,64,512]{2,1,0:T(8,128)(2,1)S(1)}, bf16[4,64,512]{2,1,0:T(8,128)(2,1)S(1)}, u32[]{:S(2)}, u32[]{:S(2)}) collective-permute-start(bf16[4,64,512]{2,1,0:T(8,128)(2,1)S(1)} %slice.4.refs_0_), channel_id=1, source_target_pairs={{0,2},{2,0},{1,3},{3,1},{4,6},{6,4},{5,7},{7,5},{8,10},{10,8},{9,1... | collective-permute-start | bytes 786440 | tf_op jit(solution)/shard_map/ppermute | solution.py:506
  134.7 1.9 %collective-permute-done.7.refs_2_ = bf16[4,64,512]{2,1,0:T(8,128)(2,1)S(1)} collective-permute-done((bf16[4,64,512]{2,1,0:T(8,128)(2,1)S(1)}, bf16[4,64,512]{2,1,0:T(8,128)(2,1)S(1)}, u32[]{:S(2)}, u32[]{:S(2)}) %collective-permute-start.7) | collective-permute-done | bytes 262176 | tf_op jit(solution)/shard_map/ppermute | solution.py:506
  136.7 5.6 %collective-permute-done.8.refs_3_ = bf16[4,64,512]{2,1,0:T(8,128)(2,1)S(1)} collective-permute-done((bf16[4,64,512]{2,1,0:T(8,128)(2,1)S(1)}, bf16[4,64,512]{2,1,0:T(8,128)(2,1)S(1)}, u32[]{:S(2)}, u32[]{:S(2)}) %collective-permute-start.8) | collective-permute-done | bytes 262176 | tf_op jit(solution)/shard_map/ppermute | solution.py:507
  143.0 2.8 %third.1 = (bf16[256,128]{1,0:T(8,128)(2,1)}, f32[128,128]{1,0:T(8,128)}) custom-call(bf16[4,64,512]{2,1,0:T(8,128)(2,1)} %copy-done.2, bf16[4,64,512]{2,1,0:T(8,128)(2,1)} %copy-done.11, bf16[4,64,512]{2,1,0:T(8,128)(2,1)} %copy-done.12, bf16[4,64,512]{2,1,0:T(8,128)(2,1)} %copy-done.13, f32[16,64]{1,0:T(8,128)} %reshape.33.refs_4_, ...), custom_call_target="tpu_custom_call" | custom-call | tf_op jit(solution)/shard_map/third/pallas_call | solution.py:226
  146.5 2.0 %combine.1 = bf16[128,128]{1,0:T(8,128)(2,1)} custom-call(f32[128,128]{1,0:T(8,128)} %get-tuple-element.21.shared_ref, bf16[1024,128]{1,0:T(8,128)(2,1)} %bitcast.17, bf16[128,1024]{1,0:T(8,128)(2,1)} %get-tuple-element.22.high_ref, bf16[128,1024]{1,0:T(8,128)(2,1)} %get-tuple-element.23.low_ref), custom_call_target="tpu_custom_call" | custom-call | tf_op jit(solution)/shard_map/combine/pallas_call | solution.py:422
  (45 shorter events, 9.6 us)
Async XLA Ops:
  5.4 13.9 %copy-start.7 = (bf16[1,2048,128]{2,1,0:T(8,128)(2,1)S(1)}, bf16[1,2048,128]{2,1,0:T(8,128)(2,1)}, u32[]{:S(2)}) copy-start(bf16[1,2048,128]{2,1,0:T(8,128)(2,1)} %param.34) | copy-start | bytes 1572868
  5.4 17.1 %copy-start.8 = (bf16[1,2048,128]{2,1,0:T(8,128)(2,1)S(1)}, bf16[1,2048,128]{2,1,0:T(8,128)(2,1)}, u32[]{:S(2)}) copy-start(bf16[1,2048,128]{2,1,0:T(8,128)(2,1)} %param.35) | copy-start | bytes 1572868
  5.4 45.6 %all-to-all-start = ((bf16[32,8,2304]{2,1,0:T(8,128)(2,1)}), bf16[32,8,2304]{2,1,0:T(8,128)(2,1)S(1)}, u32[]{:S(2)}, u32[]{:S(2)}) async-start(bf16[32,8,2304]{2,1,0:T(8,128)(2,1)} %bitcast.15), calls=%async_computation | async-start | bytes 2359296 | tf_op jit(solution)/shard_map/all_to_all | solution.py:443
  19.3 14.4 %collective-permute-start.1 = (bf16[2048,128]{1,0:T(8,128)(2,1)S(1)}, bf16[2048,128]{1,0:T(8,128)(2,1)S(1)}, u32[]{:S(2)}, u32[]{:S(2)}) collective-permute-start(bf16[2048,128]{1,0:T(8,128)(2,1)S(1)} %bitcast.22), channel_id=1, source_target_pairs={{0,2},{2,0},{1,3},{3,1},{4,6},{6,4},{5,7},{7,5},{8,10},{10,8},{9,1... | collective-permute-start | bytes 1572872 | tf_op jit(solution)/shard_map/ppermute | solution.py:436
  22.5 22.4 %collective-permute-start.4 = (bf16[2048,128]{1,0:T(8,128)(2,1)S(1)}, bf16[2048,128]{1,0:T(8,128)(2,1)S(1)}, u32[]{:S(2)}, u32[]{:S(2)}) collective-permute-start(bf16[2048,128]{1,0:T(8,128)(2,1)S(1)} %bitcast.25), channel_id=1, source_target_pairs={{0,2},{2,0},{1,3},{3,1},{4,6},{6,4},{5,7},{7,5},{8,10},{10,8},{9,1... | collective-permute-start | bytes 1572872 | tf_op jit(solution)/shard_map/ppermute | solution.py:436
  24.6 26.4 %collective-permute-start = (bf16[2048,128]{1,0:T(8,128)(2,1)S(1)}, bf16[2048,128]{1,0:T(8,128)(2,1)}, u32[]{:S(2)}, u32[]{:S(2)}) collective-permute-start(bf16[2048,128]{1,0:T(8,128)(2,1)S(1)} %bitcast.23), channel_id=1, source_target_pairs={{0,1},{1,0},{2,3},{3,2},{4,5},{5,4},{6,7},{7,6},{8,9},{9,8},{10,11... | collective-permute-start | bytes 1572872 | tf_op jit(solution)/shard_map/ppermute | solution.py:437
  28.0 22.9 %collective-permute-start.3 = (bf16[2048,128]{1,0:T(8,128)(2,1)S(1)}, bf16[2048,128]{1,0:T(8,128)(2,1)}, u32[]{:S(2)}, u32[]{:S(2)}) collective-permute-start(bf16[2048,128]{1,0:T(8,128)(2,1)S(1)} %bitcast.26), channel_id=1, source_target_pairs={{0,1},{1,0},{2,3},{3,2},{4,5},{5,4},{6,7},{7,6},{8,9},{9,8},{10,11... | collective-permute-start | bytes 1572872 | tf_op jit(solution)/shard_map/ppermute | solution.py:437
  33.7 17.3 %copy-start.9 = (bf16[2048,128]{1,0:T(8,128)(2,1)}, bf16[2048,128]{1,0:T(8,128)(2,1)S(1)}, u32[]{:S(2)}) copy-start(bf16[2048,128]{1,0:T(8,128)(2,1)S(1)} %collective-permute-done.1.refs_2_) | copy-start | bytes 1572868
  33.7 17.3 %collective-permute-start.2 = (bf16[2048,128]{1,0:T(8,128)(2,1)S(1)}, bf16[2048,128]{1,0:T(8,128)(2,1)}, u32[]{:S(2)}, u32[]{:S(2)}) collective-permute-start(bf16[2048,128]{1,0:T(8,128)(2,1)S(1)} %collective-permute-done.1.refs_2_), channel_id=1, source_target_pairs={{0,1},{1,0},{2,3},{3,2},{4,5},{5,4},{6,7},{7,6},{8,9},{9,8},{10,11... | collective-permute-start | bytes 1572872 | tf_op jit(solution)/shard_map/ppermute | solution.py:438
  44.9 6.1 %copy-start.10 = (bf16[2048,128]{1,0:T(8,128)(2,1)}, bf16[2048,128]{1,0:T(8,128)(2,1)S(1)}, u32[]{:S(2)}) copy-start(bf16[2048,128]{1,0:T(8,128)(2,1)S(1)} %collective-permute-done.4.refs_6_) | copy-start | bytes 1572868
  44.9 6.0 %collective-permute-start.5 = (bf16[2048,128]{1,0:T(8,128)(2,1)S(1)}, bf16[2048,128]{1,0:T(8,128)(2,1)}, u32[]{:S(2)}, u32[]{:S(2)}) collective-permute-start(bf16[2048,128]{1,0:T(8,128)(2,1)S(1)} %collective-permute-done.4.refs_6_), channel_id=1, source_target_pairs={{0,1},{1,0},{2,3},{3,2},{4,5},{5,4},{6,7},{7,6},{8,9},{9,8},{10,11... | collective-permute-start | bytes 1572872 | tf_op jit(solution)/shard_map/ppermute | solution.py:438
  57.6 6.9 %copy-start.4 = (bf16[1,2048,128]{2,1,0:T(8,128)(2,1)S(1)}, bf16[1,2048,128]{2,1,0:T(8,128)(2,1)}, u32[]{:S(2)}) copy-start(bf16[1,2048,128]{2,1,0:T(8,128)(2,1)} %param.36) | copy-start | bytes 1572868
  57.6 50.5 %all-to-all-start.1 = ((bf16[4,320,512]{2,1,0:T(8,128)(2,1)}), bf16[4,320,512]{2,1,0:T(8,128)(2,1)S(1)}, u32[]{:S(2)}, u32[]{:S(2)}) async-start(bf16[4,320,512]{2,1,0:T(8,128)(2,1)} %second.1), calls=%async_computation.1 | async-start | bytes 2621440 | tf_op jit(solution)/shard_map/all_to_all | solution.py:443
  64.6 40.7 %collective-permute-start.10 = (bf16[2048,128]{1,0:T(8,128)(2,1)S(1)}, bf16[2048,128]{1,0:T(8,128)(2,1)S(1)}, u32[]{:S(2)}, u32[]{:S(2)}) collective-permute-start(bf16[2048,128]{1,0:T(8,128)(2,1)S(1)} %bitcast.19), channel_id=1, source_target_pairs={{0,2},{2,0},{1,3},{3,1},{4,6},{6,4},{5,7},{7,5},{8,10},{10,8},{9,1... | collective-permute-start | bytes 1572872 | tf_op jit(solution)/shard_map/ppermute | solution.py:436
  66.9 43.4 %collective-permute-start.9 = (bf16[2048,128]{1,0:T(8,128)(2,1)S(1)}, bf16[2048,128]{1,0:T(8,128)(2,1)S(1)}, u32[]{:S(2)}, u32[]{:S(2)}) collective-permute-start(bf16[2048,128]{1,0:T(8,128)(2,1)S(1)} %bitcast.20), channel_id=1, source_target_pairs={{0,1},{1,0},{2,3},{3,2},{4,5},{5,4},{6,7},{7,6},{8,9},{9,8},{10,11... | collective-permute-start | bytes 1572872 | tf_op jit(solution)/shard_map/ppermute | solution.py:437
  105.3 5.0 %collective-permute-start.11 = (bf16[2048,128]{1,0:T(8,128)(2,1)S(1)}, bf16[2048,128]{1,0:T(8,128)(2,1)}, u32[]{:S(2)}, u32[]{:S(2)}) collective-permute-start(bf16[2048,128]{1,0:T(8,128)(2,1)S(1)} %collective-permute-done.10.refs_3_), channel_id=1, source_target_pairs={{0,1},{1,0},{2,3},{3,2},{4,5},{5,4},{6,7},{7,6},{8,9},{9,8},{10,11... | collective-permute-start | bytes 1572872 | tf_op jit(solution)/shard_map/ppermute | solution.py:438
  108.1 18.5 %copy-start.2 = (bf16[4,64,512]{2,1,0:T(8,128)(2,1)}, bf16[4,64,512]{2,1,0:T(8,128)(2,1)S(1)}, u32[]{:S(2)}) copy-start(bf16[4,64,512]{2,1,0:T(8,128)(2,1)S(1)} %slice.4.refs_0_) | copy-start | bytes 786436
  108.1 24.1 %copy-start.14 = (f32[1024]{0:T(1024)S(1)}, f32[1024]{0:T(1024)}, u32[]{:S(2)}) copy-start(f32[1024]{0:T(1024)} %param.28) | copy-start | bytes 12292
  108.1 22.2 %collective-permute-start.6 = (bf16[4,64,512]{2,1,0:T(8,128)(2,1)S(1)}, bf16[4,64,512]{2,1,0:T(8,128)(2,1)S(1)}, u32[]{:S(2)}, u32[]{:S(2)}) collective-permute-start(bf16[4,64,512]{2,1,0:T(8,128)(2,1)S(1)} %slice.4.refs_0_), channel_id=1, source_target_pairs={{0,1},{1,0},{2,3},{3,2},{4,5},{5,4},{6,7},{7,6},{8,9},{9,8},{10,11... | collective-permute-start | bytes 786440 | tf_op jit(solution)/shard_map/ppermute | solution.py:505
  114.6 31.2 %all-to-all-start.2 = ((bf16[128,8,128]{2,1,0:T(8,128)(2,1)}), bf16[128,8,128]{2,1,0:T(8,128)(2,1)S(1)}, u32[]{:S(2)}, u32[]{:S(2)}) async-start(bf16[128,8,128]{2,1,0:T(8,128)(2,1)} %bitcast.16), calls=%async_computation.2 | async-start | bytes 524288 | tf_op jit(solution)/shard_map/all_to_all | solution.py:443
  126.6 10.1 %collective-permute-start.7 = (bf16[4,64,512]{2,1,0:T(8,128)(2,1)S(1)}, bf16[4,64,512]{2,1,0:T(8,128)(2,1)S(1)}, u32[]{:S(2)}, u32[]{:S(2)}) collective-permute-start(bf16[4,64,512]{2,1,0:T(8,128)(2,1)S(1)} %slice.4.refs_0_), channel_id=1, source_target_pairs={{0,2},{2,0},{1,3},{3,1},{4,6},{6,4},{5,7},{7,5},{8,10},{10,8},{9,1... | collective-permute-start | bytes 786440 | tf_op jit(solution)/shard_map/ppermute | solution.py:506
  130.3 12.0 %copy-start.11 = (bf16[4,64,512]{2,1,0:T(8,128)(2,1)}, bf16[4,64,512]{2,1,0:T(8,128)(2,1)S(1)}, u32[]{:S(2)}) copy-start(bf16[4,64,512]{2,1,0:T(8,128)(2,1)S(1)} %collective-permute-done.6.refs_1_) | copy-start | bytes 786436
  130.3 12.0 %collective-permute-start.8 = (bf16[4,64,512]{2,1,0:T(8,128)(2,1)S(1)}, bf16[4,64,512]{2,1,0:T(8,128)(2,1)S(1)}, u32[]{:S(2)}, u32[]{:S(2)}) collective-permute-start(bf16[4,64,512]{2,1,0:T(8,128)(2,1)S(1)} %collective-permute-done.6.refs_1_), channel_id=1, source_target_pairs={{0,2},{2,0},{1,3},{3,1},{4,6},{6,4},{5,7},{7,5},{8,10},{10,8},{9,1... | collective-permute-start | bytes 786440 | tf_op jit(solution)/shard_map/ppermute | solution.py:507
  136.7 5.6 %copy-start.12 = (bf16[4,64,512]{2,1,0:T(8,128)(2,1)}, bf16[4,64,512]{2,1,0:T(8,128)(2,1)S(1)}, u32[]{:S(2)}) copy-start(bf16[4,64,512]{2,1,0:T(8,128)(2,1)S(1)} %collective-permute-done.7.refs_2_) | copy-start | bytes 786436
  (6 other events, 10.4 us)

commit v4 on v3

--- a/solution.py
+++ b/solution.py
@@ -20,6 +20,10 @@
 
 def vmem(count):
     return [pl.BlockSpec(memory_space=VM)] * count
+
+
+def held(*arrays):
+    return [pltpu.with_memory_space_constraint(a, VM) for a in arrays]
 
 
 def sin_cos(x):
@@ -184,7 +188,10 @@
 
 
 def third_kernel(*refs):
-    pieces, (scale_ref, w_ref, down_ref, mixed_ref, shared_ref) = refs[:4], refs[4:]
+    pieces, (scale_ref, w_ref, down_ref, mixed_ref, shared_ref, gains) = refs[:4], refs[4:]
+    for d in range(gains.shape[0]):
+        part = scale_ref[:, d * gains.shape[1] : (d + 1) * gains.shape[1]]
+        gains[d : d + 1, :] = part
     sub = own_sub()
     members = pieces[0].shape[0]
     places = [(m, q) for m in range(members) for q in range(4)]
@@ -204,7 +211,7 @@
     shared = jnp.zeros(shared_ref.shape, F32)
     for (m, q), block in zip(places, blocks):
         d = m * 4 + (sub ^ q)
-        gain = jnp.concatenate([scale_ref[pl.ds(d, 1), :]] * 2, axis=1)
+        gain = jnp.concatenate([gains[pl.ds(d, 1), :]] * 2, axis=1)
         v = (block.astype(F32) * factor * gain).astype(BF16)
         w = w_ref[pl.ds(pl.multiple_of(d * width, width), width), :]
         w2 = jnp.concatenate([w, w], axis=0)
@@ -231,8 +238,9 @@
         ],
         in_specs=vmem(7),
         out_specs=vmem(2),
+        scratch_shapes=[VM((pieces[0].shape[0] * 4, scale.size // pieces[0].shape[0] // 4), F32)],
         name="third",
-    )(*pieces, scale.reshape(pieces[0].shape[0] * 4, -1), w, down)
+    )(pieces[0], *held(*pieces[1:]), scale.reshape(1, -1), w, down)
 
 
 def expert_table(routes_ref, weights_ref, experts):
@@ -363,7 +371,7 @@
         out_specs=pl.BlockSpec(memory_space=VM),
         scratch_shapes=[VM((through.shape[0], 128), F32)],
         name="second",
-    )(arrived, extra, *gates, *ups, *pieces, through, wout)
+    )(*held(arrived), extra, *gates, *ups, *pieces, through, wout)
 
 
 def shared_hidden_kernel(rows_ref, gate_ref, up_ref, out_ref):
@@ -383,7 +391,8 @@
 
 
 def down_kernel(*refs):
-    hidden, weights, out_ref, whole = refs[0], refs[1:5], refs[5], refs[6]
+    hidden, weights, (out_ref, rest_ref, whole) = refs[0], refs[1:5], refs[5:]
+    rest_ref[...] = hidden[:, whole.shape[0] :, :]
     sub = own_sub()
     lanes = weights[0].shape[1]
     for member in range(hidden.shape[0]):
@@ -402,12 +411,17 @@
     lanes = weights[0].shape[1]
     return pl.pallas_call(
         down_kernel,
-        out_shape=jax.ShapeDtypeStruct((4, rows, lanes), BF16),
+        out_shape=[
+            jax.ShapeDtypeStruct((4, rows, lanes), BF16),
+            jax.ShapeDtypeStruct(
+                (hidden.shape[0], hidden.shape[1] - rows, hidden.shape[2]), BF16
+            ),
+        ],
         in_specs=vmem(5),
-        out_specs=pl.BlockSpec(memory_space=VM),
+        out_specs=vmem(2),
         scratch_shapes=[VM((rows, weights[0].shape[0]), BF16)],
         name="down",
-    )(hidden, *weights)
+    )(*held(hidden), *weights)
 
 
 def combine_kernel(shared_ref, back_ref, high_ref, low_ref, out_ref):
@@ -425,7 +439,7 @@
         in_specs=vmem(4),
         out_specs=pl.BlockSpec(memory_space=VM),
         name="combine",
-    )(shared, back, high, low)
+    )(shared, *held(back), high, low)
 
 
 TP = ("yh", "yl", "co")
@@ -498,13 +512,13 @@
         lax.axis_size("yh"),
     )
     hidden = spread_out(hidden, "yh")
-    results = run_down(hidden, downs, blocks * 8).reshape(4 * blocks, 8, -1)
+    results, own = run_down(hidden, downs, blocks * 8)
+    results = results.reshape(4 * blocks, 8, -1)
     back = spread_out(results, ("yl", "co", "ep")).reshape(blocks * 32, -1)
 
-    own = hidden[:, blocks * 8 :]
     core = lax.ppermute(own, "co", SWAP)
     over = lax.ppermute(own, "yl", SWAP)
-    both = lax.ppermute(core, "yl", SWAP)
+    both = lax.ppermute(over, "co", SWAP)
     mixed, shared = run_third(
         (own, core, over, both),
         mixer_norm_scale,

time: 149 us -> 143 us (0.960)
  local copies, waits for them, and re-layouts: 3.89 us -> 0.82 us
  waiting for transfers between devices: 53.3 us -> 51.4 us
    ppermute x1, waiting for transfers between devices: 5.61 us -> 0.01 us  [on_device(): both = lax.ppermute(over, 'co', SWAP)]
    all_to_all x3, waiting for transfers between devices: 0.01 us -> 4.17 us  [spread_out(): return lax.all_to_all(pieces, axes, split_axis=0, concat_axis=0, tiled=True)]
    unnamed x30 -> x16, local copies, waits for them, and re-layouts: 3.21 us -> 0.82 us
    ppermute x1, waiting for transfers between devices: 1.94 us -> 0.01 us  [on_device(): over = lax.ppermute(own, 'yl', SWAP)]
    ppermute x3, waiting for transfers between devices: 0.01 us -> 1.5 us  [exchanged(): both = lax.ppermute(over, 'co', SWAP)]
  transfers between devices with their start and end apart: 15 -> 15, of which waited for: 5 -> 5; matrix products, arithmetic and copies ran while one was open for 0% -> 0% of each run, Pallas kernels for 7% -> 5%
where the time goes in v4:
time: 143 us; the launch traced here: 142 us
  starting transfers between devices  66.8 us (47%)
  waiting for transfers between devices  51.4 us (36%)
  Pallas kernels  21.9 us (15%)
    ppermute x3, waiting for transfers between devices, exchanged(): over = lax.ppermute(piece, 'yl', SWAP)  45.8 us
    all_to_all x3, starting transfers between devices, spread_out(): return lax.all_to_all(pieces, axes, split_axis=0, concat_axis=0, tiled=True)  32 us
    ppermute x3, starting transfers between devices, exchanged(): both = lax.ppermute(over, 'co', SWAP)  11.6 us
    ppermute x3, starting transfers between devices, exchanged(): core = lax.ppermute(piece, 'co', SWAP)  7.84 us
    ppermute x3, starting transfers between devices, exchanged(): over = lax.ppermute(piece, 'yl', SWAP)  7.58 us
    pallas_call x1, Pallas kernels, run_second(): pl.pallas_call(second_kernel, out_shape=jax.ShapeDtypeStruct((copies, row...  5.26 us
    pallas_call x1, Pallas kernels, run_first(): pl.pallas_call(first_kernel, out_shape=[jax.ShapeDtypeStruct(tokens.shape...  4.7 us
    all_to_all x3, waiting for transfers between devices, spread_out(): return lax.all_to_all(pieces, axes, split_axis=0, concat_axis=0, tiled=True)  4.17 us
  transfers between devices with their start and end apart: 15, of which 5 were waited for; matrix products, arithmetic and copies ran while one was open for 0% of the time, Pallas kernels for 5%

profile of v4, /device:TPU:1, one launch (start us, length us, event | category | flops | bytes accessed | tf_op | source)
XLA Modules:
  0.0 141.8 jit_solution(14873233399107245946)
XLA Ops:
  0.6 4.7 %first.1 = (bf16[128,2048]{1,0:T(8,128)(2,1)}, bf16[256,2304]{1,0:T(8,128)(2,1)}, f32[32,8,256]{2,1,0:T(8,128)}, f32[32,8,256]{2,1,0:T(8,128)}, f32[32,8,256]{2,...) custom-call(bf16[128,2048]{1,0:T(8,128)(2,1)} %tokens_ref.1, f32[1,2048]{1,0:T(1,128)} %bitcast.31, ...), custom_call_target="tpu_custom_call" | custom-call | tf_op jit(solution)/shard_map/first/pallas_call | solution.py:289
  5.4 13.8 %all-to-all-start = ((bf16[32,8,2304]{2,1,0:T(8,128)(2,1)}), bf16[32,8,2304]{2,1,0:T(8,128)(2,1)S(1)}, u32[]{:S(2)}, u32[]{:S(2)}) async-start(bf16[32,8,2304]{2,1,0:T(8,128)(2,1)} %bitcast.17), calls=%async_computation | async-start | bytes 2359296 | tf_op jit(solution)/shard_map/all_to_all | solution.py:457
  19.2 3.2 %collective-permute-start.1 = (bf16[2048,128]{1,0:T(8,128)(2,1)S(1)}, bf16[2048,128]{1,0:T(8,128)(2,1)S(1)}, u32[]{:S(2)}, u32[]{:S(2)}) collective-permute-start(bf16[2048,128]{1,0:T(8,128)(2,1)S(1)} %bitcast.22), channel_id=1, source_target_pairs={{0,2},{2,0},{1,3},{3,1},{4,6},{6,4},{5,7},{7,5},{8,10},{10,8},{9,1... | collective-permute-start | bytes 1572872 | tf_op jit(solution)/shard_map/ppermute | solution.py:450
  22.4 2.1 %collective-permute-start.4 = (bf16[2048,128]{1,0:T(8,128)(2,1)S(1)}, bf16[2048,128]{1,0:T(8,128)(2,1)S(1)}, u32[]{:S(2)}, u32[]{:S(2)}) collective-permute-start(bf16[2048,128]{1,0:T(8,128)(2,1)S(1)} %bitcast.25), channel_id=1, source_target_pairs={{0,2},{2,0},{1,3},{3,1},{4,6},{6,4},{5,7},{7,5},{8,10},{10,8},{9,1... | collective-permute-start | bytes 1572872 | tf_op jit(solution)/shard_map/ppermute | solution.py:450
  24.5 3.4 %collective-permute-start = (bf16[2048,128]{1,0:T(8,128)(2,1)S(1)}, bf16[2048,128]{1,0:T(8,128)(2,1)}, u32[]{:S(2)}, u32[]{:S(2)}) collective-permute-start(bf16[2048,128]{1,0:T(8,128)(2,1)S(1)} %bitcast.23), channel_id=1, source_target_pairs={{0,1},{1,0},{2,3},{3,2},{4,5},{5,4},{6,7},{7,6},{8,9},{9,8},{10,11... | collective-permute-start | bytes 1572872 | tf_op jit(solution)/shard_map/ppermute | solution.py:451
  28.0 1.9 %collective-permute-start.3 = (bf16[2048,128]{1,0:T(8,128)(2,1)S(1)}, bf16[2048,128]{1,0:T(8,128)(2,1)}, u32[]{:S(2)}, u32[]{:S(2)}) collective-permute-start(bf16[2048,128]{1,0:T(8,128)(2,1)S(1)} %bitcast.26), channel_id=1, source_target_pairs={{0,1},{1,0},{2,3},{3,2},{4,5},{5,4},{6,7},{7,6},{8,9},{9,8},{10,11... | collective-permute-start | bytes 1572872 | tf_op jit(solution)/shard_map/ppermute | solution.py:451
  29.9 3.7 %collective-permute-done.1.refs_2_ = bf16[2048,128]{1,0:T(8,128)(2,1)S(1)} collective-permute-done((bf16[2048,128]{1,0:T(8,128)(2,1)S(1)}, bf16[2048,128]{1,0:T(8,128)(2,1)S(1)}, u32[]{:S(2)}, u32[]{:S(2)}) %collective-permute-start.1) | collective-permute-done | bytes 524320 | tf_op jit(solution)/shard_map/ppermute | solution.py:450
  33.6 5.1 %collective-permute-start.2 = (bf16[2048,128]{1,0:T(8,128)(2,1)S(1)}, bf16[2048,128]{1,0:T(8,128)(2,1)}, u32[]{:S(2)}, u32[]{:S(2)}) collective-permute-start(bf16[2048,128]{1,0:T(8,128)(2,1)S(1)} %collective-permute-done.1.refs_2_), channel_id=1, source_target_pairs={{0,1},{1,0},{2,3},{3,2},{4,5},{5,4},{6,7},{7,6},{8,9},{9,8},{10,11... | collective-permute-start | bytes 1572872 | tf_op jit(solution)/shard_map/ppermute | solution.py:452
  38.8 6.1 %collective-permute-done.4.refs_6_ = bf16[2048,128]{1,0:T(8,128)(2,1)S(1)} collective-permute-done((bf16[2048,128]{1,0:T(8,128)(2,1)S(1)}, bf16[2048,128]{1,0:T(8,128)(2,1)S(1)}, u32[]{:S(2)}, u32[]{:S(2)}) %collective-permute-start.4) | collective-permute-done | bytes 524320 | tf_op jit(solution)/shard_map/ppermute | solution.py:450
  44.9 3.7 %collective-permute-start.5 = (bf16[2048,128]{1,0:T(8,128)(2,1)S(1)}, bf16[2048,128]{1,0:T(8,128)(2,1)}, u32[]{:S(2)}, u32[]{:S(2)}) collective-permute-start(bf16[2048,128]{1,0:T(8,128)(2,1)S(1)} %collective-permute-done.4.refs_6_), channel_id=1, source_target_pairs={{0,1},{1,0},{2,3},{3,2},{4,5},{5,4},{6,7},{7,6},{8,9},{9,8},{10,11... | collective-permute-start | bytes 1572872 | tf_op jit(solution)/shard_map/ppermute | solution.py:452
  48.6 2.3 %shared_hidden.1.extra_ref = bf16[128,128]{1,0:T(8,128)(2,1)} custom-call(bf16[128,2048]{1,0:T(8,128)(2,1)} %get-tuple-element.16.rows_ref, bf16[2048,128]{1,0:T(8,128)(2,1)} %gate_ref.1, bf16[2048,128]{1,0:T(8,128)(2,1)} %up_ref.1), custom_call_target="tpu_custom_call" | custom-call | tf_op jit(solution)/shard_map/shared_hidden/pallas_call | solution.py:384
  50.9 5.3 %second.1 = bf16[4,320,512]{2,1,0:T(8,128)(2,1)} custom-call(bf16[32,8,2304]{2,1,0:T(8,128)(2,1)S(1)} %all-to-all-done.arrived_ref, bf16[128,128]{1,0:T(8,128)(2,1)} %shared_hidden.1.extra_ref, bf16[2048,128]{1,0:T(8,128)(2,1)} %bitcast.21, bf16[2048,128]{1,0:T(8,128)(2,1)} %collective-permute-done.refs_1_, bf16[2048,128]{1,0:T(8,128)(2,1)} %copy-done.6, ...), custom_call_target="tpu_custom_call" | custom-call | tf_op jit(solution)/shard_map/second/pallas_call | solution.py:367
  56.2 7.0 %all-to-all-start.1 = ((bf16[4,320,512]{2,1,0:T(8,128)(2,1)}), bf16[4,320,512]{2,1,0:T(8,128)(2,1)S(1)}, u32[]{:S(2)}, u32[]{:S(2)}) async-start(bf16[4,320,512]{2,1,0:T(8,128)(2,1)} %second.1), calls=%async_computation.1 | async-start | bytes 2621440 | tf_op jit(solution)/shard_map/all_to_all | solution.py:457
  63.2 2.3 %collective-permute-start.7 = (bf16[2048,128]{1,0:T(8,128)(2,1)S(1)}, bf16[2048,128]{1,0:T(8,128)(2,1)S(1)}, u32[]{:S(2)}, u32[]{:S(2)}) collective-permute-start(bf16[2048,128]{1,0:T(8,128)(2,1)S(1)} %bitcast.19), channel_id=1, source_target_pairs={{0,2},{2,0},{1,3},{3,1},{4,6},{6,4},{5,7},{7,5},{8,10},{10,8},{9,1... | collective-permute-start | bytes 1572872 | tf_op jit(solution)/shard_map/ppermute | solution.py:450
  65.5 2.5 %collective-permute-start.6 = (bf16[2048,128]{1,0:T(8,128)(2,1)S(1)}, bf16[2048,128]{1,0:T(8,128)(2,1)S(1)}, u32[]{:S(2)}, u32[]{:S(2)}) collective-permute-start(bf16[2048,128]{1,0:T(8,128)(2,1)S(1)} %bitcast.20), channel_id=1, source_target_pairs={{0,1},{1,0},{2,3},{3,2},{4,5},{5,4},{6,7},{7,6},{8,9},{9,8},{10,11... | collective-permute-start | bytes 1572872 | tf_op jit(solution)/shard_map/ppermute | solution.py:451
  67.9 35.9 %collective-permute-done.7.refs_3_ = bf16[2048,128]{1,0:T(8,128)(2,1)S(1)} collective-permute-done((bf16[2048,128]{1,0:T(8,128)(2,1)S(1)}, bf16[2048,128]{1,0:T(8,128)(2,1)S(1)}, u32[]{:S(2)}, u32[]{:S(2)}) %collective-permute-start.7) | collective-permute-done | bytes 524320 | tf_op jit(solution)/shard_map/ppermute | solution.py:450
  103.9 2.8 %collective-permute-start.8 = (bf16[2048,128]{1,0:T(8,128)(2,1)S(1)}, bf16[2048,128]{1,0:T(8,128)(2,1)S(1)}, u32[]{:S(2)}, u32[]{:S(2)}) collective-permute-start(bf16[2048,128]{1,0:T(8,128)(2,1)S(1)} %collective-permute-done.7.refs_3_), channel_id=1, source_target_pairs={{0,1},{1,0},{2,3},{3,2},{4,5},{5,4},{6,7},{7,6},{8,9},{9,8},{10,11... | collective-permute-start | bytes 1572872 | tf_op jit(solution)/shard_map/ppermute | solution.py:452
  109.0 3.2 %down.1 = (bf16[4,256,128]{2,1,0:T(8,128)(2,1)}, bf16[4,64,512]{2,1,0:T(8,128)(2,1)}) custom-call(bf16[4,320,512]{2,1,0:T(8,128)(2,1)S(1)} %all-to-all-done.1.refs_0_, bf16[2048,128]{1,0:T(8,128)(2,1)} %bitcast.18, bf16[2048,128]{1,0:T(8,128)(2,1)} %copy-done.2, bf16[2048,128]{1,0:T(8,128)(2,1)} %copy-done.1, bf16[2048,128]{1,0:T(8,128)(2,1)} %copy-done.3), custom_call_target="tpu_custom_call" | custom-call | tf_op jit(solution)/shard_map/down/pallas_call | solution.py:412
  112.2 3.1 %collective-permute-start.10 = (bf16[4,64,512]{2,1,0:T(8,128)(2,1)}, bf16[4,64,512]{2,1,0:T(8,128)(2,1)S(1)}, u32[]{:S(2)}, u32[]{:S(2)}) collective-permute-start(bf16[4,64,512]{2,1,0:T(8,128)(2,1)} %get-tuple-element.22.refs_0_), channel_id=1, source_target_pairs={{0,2},{2,0},{1,3},{3,1},{4,6},{6,4},{5,7},{7,5},{8,10},{10,8},{9,1... | collective-permute-start | bytes 786440 | tf_op jit(solution)/shard_map/ppermute | solution.py:520
  115.4 11.2 %all-to-all-start.2 = ((bf16[128,8,128]{2,1,0:T(8,128)(2,1)}), bf16[128,8,128]{2,1,0:T(8,128)(2,1)S(1)}, u32[]{:S(2)}, u32[]{:S(2)}) async-start(bf16[128,8,128]{2,1,0:T(8,128)(2,1)} %bitcast.27), calls=%async_computation.2 | async-start | bytes 524288 | tf_op jit(solution)/shard_map/all_to_all | solution.py:457
  126.6 2.7 %collective-permute-start.9 = (bf16[4,64,512]{2,1,0:T(8,128)(2,1)}, bf16[4,64,512]{2,1,0:T(8,128)(2,1)S(1)}, u32[]{:S(2)}, u32[]{:S(2)}) collective-permute-start(bf16[4,64,512]{2,1,0:T(8,128)(2,1)} %get-tuple-element.22.refs_0_), channel_id=1, source_target_pairs={{0,1},{1,0},{2,3},{3,2},{4,5},{5,4},{6,7},{7,6},{8,9},{9,8},{10,11... | collective-permute-start | bytes 786440 | tf_op jit(solution)/shard_map/ppermute | solution.py:519
  133.1 2.6 %third.1 = (bf16[256,128]{1,0:T(8,128)(2,1)}, f32[128,128]{1,0:T(8,128)}) custom-call(bf16[4,64,512]{2,1,0:T(8,128)(2,1)} %get-tuple-element.22.refs_0_, bf16[4,64,512]{2,1,0:T(8,128)(2,1)S(1)} %collective-permute-done.9.refs_1_, bf16[4,64,512]{2,1,0:T(8,128)(2,1)S(1)} %collective-permute-done.10.refs_2_, ...), custom_call_target="tpu_custom_call" | custom-call | tf_op jit(solution)/shard_map/third/pallas_call | solution.py:233
  135.7 4.2 %all-to-all-done.2 = bf16[128,8,128]{2,1,0:T(8,128)(2,1)S(1)} async-done(((bf16[128,8,128]{2,1,0:T(8,128)(2,1)}), bf16[128,8,128]{2,1,0:T(8,128)(2,1)S(1)}, u32[]{:S(2)}, u32[]{:S(2)}) %all-to-all-start.2) | async-done | bytes 262176 | tf_op jit(solution)/shard_map/all_to_all | solution.py:457
  139.9 2.0 %combine.1 = bf16[128,128]{1,0:T(8,128)(2,1)} custom-call(f32[128,128]{1,0:T(8,128)} %get-tuple-element.24.shared_ref, bf16[1024,128]{1,0:T(8,128)(2,1)S(1)} %bitcast.16, bf16[128,1024]{1,0:T(8,128)(2,1)} %get-tuple-element.26.high_ref, bf16[128,1024]{1,0:T(8,128)(2,1)} %get-tuple-element.27.low_ref), custom_call_target="tpu_custom_call" | custom-call | tf_op jit(solution)/shard_map/combine/pallas_call | solution.py:436
  (29 shorter events, 6.1 us)
Async XLA Ops:
  5.3 13.9 %copy-start.4 = (bf16[1,2048,128]{2,1,0:T(8,128)(2,1)S(1)}, bf16[1,2048,128]{2,1,0:T(8,128)(2,1)}, u32[]{:S(2)}) copy-start(bf16[1,2048,128]{2,1,0:T(8,128)(2,1)} %param.34) | copy-start | bytes 1572868
  5.3 17.1 %copy-start.5 = (bf16[1,2048,128]{2,1,0:T(8,128)(2,1)S(1)}, bf16[1,2048,128]{2,1,0:T(8,128)(2,1)}, u32[]{:S(2)}) copy-start(bf16[1,2048,128]{2,1,0:T(8,128)(2,1)} %param.35) | copy-start | bytes 1572868
  5.4 45.6 %all-to-all-start = ((bf16[32,8,2304]{2,1,0:T(8,128)(2,1)}), bf16[32,8,2304]{2,1,0:T(8,128)(2,1)S(1)}, u32[]{:S(2)}, u32[]{:S(2)}) async-start(bf16[32,8,2304]{2,1,0:T(8,128)(2,1)} %bitcast.17), calls=%async_computation | async-start | bytes 2359296 | tf_op jit(solution)/shard_map/all_to_all | solution.py:457
  19.2 14.4 %collective-permute-start.1 = (bf16[2048,128]{1,0:T(8,128)(2,1)S(1)}, bf16[2048,128]{1,0:T(8,128)(2,1)S(1)}, u32[]{:S(2)}, u32[]{:S(2)}) collective-permute-start(bf16[2048,128]{1,0:T(8,128)(2,1)S(1)} %bitcast.22), channel_id=1, source_target_pairs={{0,2},{2,0},{1,3},{3,1},{4,6},{6,4},{5,7},{7,5},{8,10},{10,8},{9,1... | collective-permute-start | bytes 1572872 | tf_op jit(solution)/shard_map/ppermute | solution.py:450
  22.4 22.4 %collective-permute-start.4 = (bf16[2048,128]{1,0:T(8,128)(2,1)S(1)}, bf16[2048,128]{1,0:T(8,128)(2,1)S(1)}, u32[]{:S(2)}, u32[]{:S(2)}) collective-permute-start(bf16[2048,128]{1,0:T(8,128)(2,1)S(1)} %bitcast.25), channel_id=1, source_target_pairs={{0,2},{2,0},{1,3},{3,1},{4,6},{6,4},{5,7},{7,5},{8,10},{10,8},{9,1... | collective-permute-start | bytes 1572872 | tf_op jit(solution)/shard_map/ppermute | solution.py:450
  24.5 26.4 %collective-permute-start = (bf16[2048,128]{1,0:T(8,128)(2,1)S(1)}, bf16[2048,128]{1,0:T(8,128)(2,1)}, u32[]{:S(2)}, u32[]{:S(2)}) collective-permute-start(bf16[2048,128]{1,0:T(8,128)(2,1)S(1)} %bitcast.23), channel_id=1, source_target_pairs={{0,1},{1,0},{2,3},{3,2},{4,5},{5,4},{6,7},{7,6},{8,9},{9,8},{10,11... | collective-permute-start | bytes 1572872 | tf_op jit(solution)/shard_map/ppermute | solution.py:451
  28.0 22.9 %collective-permute-start.3 = (bf16[2048,128]{1,0:T(8,128)(2,1)S(1)}, bf16[2048,128]{1,0:T(8,128)(2,1)}, u32[]{:S(2)}, u32[]{:S(2)}) collective-permute-start(bf16[2048,128]{1,0:T(8,128)(2,1)S(1)} %bitcast.26), channel_id=1, source_target_pairs={{0,1},{1,0},{2,3},{3,2},{4,5},{5,4},{6,7},{7,6},{8,9},{9,8},{10,11... | collective-permute-start | bytes 1572872 | tf_op jit(solution)/shard_map/ppermute | solution.py:451
  33.6 17.3 %copy-start.6 = (bf16[2048,128]{1,0:T(8,128)(2,1)}, bf16[2048,128]{1,0:T(8,128)(2,1)S(1)}, u32[]{:S(2)}) copy-start(bf16[2048,128]{1,0:T(8,128)(2,1)S(1)} %collective-permute-done.1.refs_2_) | copy-start | bytes 1572868
  33.6 17.3 %collective-permute-start.2 = (bf16[2048,128]{1,0:T(8,128)(2,1)S(1)}, bf16[2048,128]{1,0:T(8,128)(2,1)}, u32[]{:S(2)}, u32[]{:S(2)}) collective-permute-start(bf16[2048,128]{1,0:T(8,128)(2,1)S(1)} %collective-permute-done.1.refs_2_), channel_id=1, source_target_pairs={{0,1},{1,0},{2,3},{3,2},{4,5},{5,4},{6,7},{7,6},{8,9},{9,8},{10,11... | collective-permute-start | bytes 1572872 | tf_op jit(solution)/shard_map/ppermute | solution.py:452
  44.9 6.1 %copy-start.7 = (bf16[2048,128]{1,0:T(8,128)(2,1)}, bf16[2048,128]{1,0:T(8,128)(2,1)S(1)}, u32[]{:S(2)}) copy-start(bf16[2048,128]{1,0:T(8,128)(2,1)S(1)} %collective-permute-done.4.refs_6_) | copy-start | bytes 1572868
  44.9 6.0 %collective-permute-start.5 = (bf16[2048,128]{1,0:T(8,128)(2,1)S(1)}, bf16[2048,128]{1,0:T(8,128)(2,1)}, u32[]{:S(2)}, u32[]{:S(2)}) collective-permute-start(bf16[2048,128]{1,0:T(8,128)(2,1)S(1)} %collective-permute-done.4.refs_6_), channel_id=1, source_target_pairs={{0,1},{1,0},{2,3},{3,2},{4,5},{5,4},{6,7},{7,6},{8,9},{9,8},{10,11... | collective-permute-start | bytes 1572872 | tf_op jit(solution)/shard_map/ppermute | solution.py:452
  56.2 7.0 %copy-start = (bf16[1,2048,128]{2,1,0:T(8,128)(2,1)S(1)}, bf16[1,2048,128]{2,1,0:T(8,128)(2,1)}, u32[]{:S(2)}) copy-start(bf16[1,2048,128]{2,1,0:T(8,128)(2,1)} %param.36) | copy-start | bytes 1572868
  56.2 52.0 %all-to-all-start.1 = ((bf16[4,320,512]{2,1,0:T(8,128)(2,1)}), bf16[4,320,512]{2,1,0:T(8,128)(2,1)S(1)}, u32[]{:S(2)}, u32[]{:S(2)}) async-start(bf16[4,320,512]{2,1,0:T(8,128)(2,1)} %second.1), calls=%async_computation.1 | async-start | bytes 2621440 | tf_op jit(solution)/shard_map/all_to_all | solution.py:457
  63.2 40.7 %collective-permute-start.7 = (bf16[2048,128]{1,0:T(8,128)(2,1)S(1)}, bf16[2048,128]{1,0:T(8,128)(2,1)S(1)}, u32[]{:S(2)}, u32[]{:S(2)}) collective-permute-start(bf16[2048,128]{1,0:T(8,128)(2,1)S(1)} %bitcast.19), channel_id=1, source_target_pairs={{0,2},{2,0},{1,3},{3,1},{4,6},{6,4},{5,7},{7,5},{8,10},{10,8},{9,1... | collective-permute-start | bytes 1572872 | tf_op jit(solution)/shard_map/ppermute | solution.py:450
  65.5 41.2 %collective-permute-start.6 = (bf16[2048,128]{1,0:T(8,128)(2,1)S(1)}, bf16[2048,128]{1,0:T(8,128)(2,1)S(1)}, u32[]{:S(2)}, u32[]{:S(2)}) collective-permute-start(bf16[2048,128]{1,0:T(8,128)(2,1)S(1)} %bitcast.20), channel_id=1, source_target_pairs={{0,1},{1,0},{2,3},{3,2},{4,5},{5,4},{6,7},{7,6},{8,9},{9,8},{10,11... | collective-permute-start | bytes 1572872 | tf_op jit(solution)/shard_map/ppermute | solution.py:451
  103.9 4.3 %copy-start.1 = (bf16[2048,128]{1,0:T(8,128)(2,1)}, bf16[2048,128]{1,0:T(8,128)(2,1)S(1)}, u32[]{:S(2)}) copy-start(bf16[2048,128]{1,0:T(8,128)(2,1)S(1)} %collective-permute-done.7.refs_3_) | copy-start | bytes 1572868
  103.9 4.3 %collective-permute-start.8 = (bf16[2048,128]{1,0:T(8,128)(2,1)S(1)}, bf16[2048,128]{1,0:T(8,128)(2,1)S(1)}, u32[]{:S(2)}, u32[]{:S(2)}) collective-permute-start(bf16[2048,128]{1,0:T(8,128)(2,1)S(1)} %collective-permute-done.7.refs_3_), channel_id=1, source_target_pairs={{0,1},{1,0},{2,3},{3,2},{4,5},{5,4},{6,7},{7,6},{8,9},{9,8},{10,11... | collective-permute-start | bytes 1572872 | tf_op jit(solution)/shard_map/ppermute | solution.py:452
  106.7 1.5 %copy-start.2 = (bf16[2048,128]{1,0:T(8,128)(2,1)}, bf16[2048,128]{1,0:T(8,128)(2,1)S(1)}, u32[]{:S(2)}) copy-start(bf16[2048,128]{1,0:T(8,128)(2,1)S(1)} %collective-permute-done.6.refs_2_) | copy-start | bytes 1572868
  108.2 0.8 copy-start.3
  112.2 17.0 %collective-permute-start.10 = (bf16[4,64,512]{2,1,0:T(8,128)(2,1)}, bf16[4,64,512]{2,1,0:T(8,128)(2,1)S(1)}, u32[]{:S(2)}, u32[]{:S(2)}) collective-permute-start(bf16[4,64,512]{2,1,0:T(8,128)(2,1)} %get-tuple-element.22.refs_0_), channel_id=1, source_target_pairs={{0,2},{2,0},{1,3},{3,1},{4,6},{6,4},{5,7},{7,5},{8,10},{10,8},{9,1... | collective-permute-start | bytes 786440 | tf_op jit(solution)/shard_map/ppermute | solution.py:520
  115.4 24.5 %all-to-all-start.2 = ((bf16[128,8,128]{2,1,0:T(8,128)(2,1)}), bf16[128,8,128]{2,1,0:T(8,128)(2,1)S(1)}, u32[]{:S(2)}, u32[]{:S(2)}) async-start(bf16[128,8,128]{2,1,0:T(8,128)(2,1)} %bitcast.27), calls=%async_computation.2 | async-start | bytes 524288 | tf_op jit(solution)/shard_map/all_to_all | solution.py:457
  126.6 6.5 %collective-permute-start.9 = (bf16[4,64,512]{2,1,0:T(8,128)(2,1)}, bf16[4,64,512]{2,1,0:T(8,128)(2,1)S(1)}, u32[]{:S(2)}, u32[]{:S(2)}) collective-permute-start(bf16[4,64,512]{2,1,0:T(8,128)(2,1)} %get-tuple-element.22.refs_0_), channel_id=1, source_target_pairs={{0,1},{1,0},{2,3},{3,2},{4,5},{5,4},{6,7},{7,6},{8,9},{9,8},{10,11... | collective-permute-start | bytes 786440 | tf_op jit(solution)/shard_map/ppermute | solution.py:519
  129.3 3.8 %collective-permute-start.11 = (bf16[4,64,512]{2,1,0:T(8,128)(2,1)S(1)}, bf16[4,64,512]{2,1,0:T(8,128)(2,1)S(1)}, u32[]{:S(2)}, u32[]{:S(2)}) collective-permute-start(bf16[4,64,512]{2,1,0:T(8,128)(2,1)S(1)} %collective-permute-done.10.refs_2_), channel_id=1, source_target_pairs={{0,1},{1,0},{2,3},{3,2},{4,5},{5,4},{6,7},{7,6},{8,9},{9,8},{10,11... | collective-permute-start | bytes 786440 | tf_op jit(solution)/shard_map/ppermute | solution.py:521

commit v5 on v4

--- a/solution.py
+++ b/solution.py
@@ -210,7 +210,7 @@
     acc = [jnp.zeros((both, w_ref.shape[1]), F32)] * 2
     shared = jnp.zeros(shared_ref.shape, F32)
     for (m, q), block in zip(places, blocks):
-        d = m * 4 + (sub ^ q)
+        d = m * 4 + (sub ^ q ^ flipped(m))
         gain = jnp.concatenate([gains[pl.ds(d, 1), :]] * 2, axis=1)
         v = (block.astype(F32) * factor * gain).astype(BF16)
         w = w_ref[pl.ds(pl.multiple_of(d * width, width), width), :]
@@ -258,8 +258,16 @@
     return jnp.where(named > 0.0, rank, -1.0), gain
 
 
+def own_place():
+    return 2 * lax.axis_index("yl") + lax.axis_index("co")
+
+
+def flipped(quad):
+    return quad // 2 * 2
+
+
 def own_sub():
-    return 2 * lax.axis_index("yl") + lax.axis_index("co")
+    return own_place() ^ flipped(lax.axis_index("yh"))
 
 
 def first_kernel(tokens_ref, gain_ref, routes_ref, *refs):
@@ -307,7 +315,8 @@
     experts = high_ref.shape[1] // (share * parts)
     rank, gain = expert_table(routes_ref, weights_ref, experts)
     for a in range(parts):
-        slot = (iota((share, tokens), 0) + a * share).astype(F32)
+        held_by = a ^ flipped(lax.axis_index("yh"))
+        slot = (iota((share, tokens), 0) + held_by * share).astype(F32)
         picked = jnp.concatenate(
             [
                 jnp.where(rank[e : e + 1, :] == slot, gain[e : e + 1, :], 0.0)
@@ -397,14 +406,14 @@
     lanes = weights[0].shape[1]
     for member in range(hidden.shape[0]):
         for q in range(4):
-            at = pl.multiple_of((member * 4 + (sub ^ q)) * lanes, lanes)
+            at = pl.multiple_of((member * 4 + (sub ^ q ^ flipped(member))) * lanes, lanes)
             whole[:, pl.ds(at, lanes)] = hidden[member, : whole.shape[0], q * lanes : (q + 1) * lanes]
     rows = whole[...]
     for q in (0, 2):
         both = jnp.concatenate([weights[q][...], weights[q + 1][...]], axis=1)
         got = jnp.dot(rows, both, preferred_element_type=F32).astype(BF16)
-        out_ref[sub ^ q] = got[:, :lanes]
-        out_ref[sub ^ (q + 1)] = got[:, lanes:]
+        out_ref[own_place() ^ q] = got[:, :lanes]
+        out_ref[own_place() ^ (q + 1)] = got[:, lanes:]
 
 
 def run_down(hidden, weights, rows):
@@ -439,11 +448,12 @@
         in_specs=vmem(4),
         out_specs=pl.BlockSpec(memory_space=VM),
         name="combine",
-    )(shared, *held(back), high, low)
+    )(shared, *held(back, high, low))
 
 
 TP = ("yh", "yl", "co")
 SWAP = [(0, 1), (1, 0)]
+LINES = [[0, 2, 5, 7], [1, 3, 4, 6]]
 
 
 def exchanged(piece):
@@ -453,8 +463,10 @@
     return (piece, core, over, both)
 
 
-def spread_out(pieces, axes):
-    return lax.all_to_all(pieces, axes, split_axis=0, concat_axis=0, tiled=True)
+def spread_out(pieces, axes, groups=None):
+    return lax.all_to_all(
+        pieces, axes, split_axis=0, concat_axis=0, axis_index_groups=groups, tiled=True
+    )
 
 
 def on_device(
@@ -511,7 +523,7 @@
         group_output_matrices.reshape(-1, frequency.shape[1]),
         lax.axis_size("yh"),
     )
-    hidden = spread_out(hidden, "yh")
+    hidden = spread_out(hidden, ("yh", "yl"), LINES)
     results, own = run_down(hidden, downs, blocks * 8)
     results = results.reshape(4 * blocks, 8, -1)
     back = spread_out(results, ("yl", "co", "ep")).reshape(blocks * 32, -1)

time: 143 us -> 135 us (0.944)
  waiting for transfers between devices: 51.4 us -> 44.4 us
    ppermute x3, waiting for transfers between devices: 45.8 us -> 38.8 us  [exchanged(): over = lax.ppermute(piece, 'yl', SWAP)]
where the time goes in v5:
time: 135 us
  starting transfers between devices  66.6 us (49%)
  waiting for transfers between devices  44.4 us (33%)
  Pallas kernels  21.8 us (16%)
    ppermute x3, waiting for transfers between devices, exchanged(): over = lax.ppermute(piece, 'yl', SWAP)  38.8 us
    all_to_all x3, starting transfers between devices, spread_out(): lax.all_to_all(pieces, axes, split_axis=0, concat_axis=0, axis_index_grou...  32 us
    ppermute x3, starting transfers between devices, exchanged(): both = lax.ppermute(over, 'co', SWAP)  11.6 us
    ppermute x3, starting transfers between devices, exchanged(): over = lax.ppermute(piece, 'yl', SWAP)  8.25 us
    ppermute x3, starting transfers between devices, exchanged(): core = lax.ppermute(piece, 'co', SWAP)  7.83 us
    pallas_call x1, Pallas kernels, run_second(): pl.pallas_call(second_kernel, out_shape=jax.ShapeDtypeStruct((copies, row...  5.27 us
    pallas_call x1, Pallas kernels, run_first(): pl.pallas_call(first_kernel, out_shape=[jax.ShapeDtypeStruct(tokens.shape...  4.72 us
    all_to_all x3, waiting for transfers between devices, spread_out(): lax.all_to_all(pieces, axes, split_axis=0, concat_axis=0, axis_index_grou...  4.11 us
  transfers between devices with their start and end apart: 15, of which 5 were waited for; matrix products, arithmetic and copies ran while one was open for 0% of the time, Pallas kernels for 5%

profile of v5, /device:TPU:1, one launch (start us, length us, event | category | flops | bytes accessed | tf_op | source)
XLA Modules:
  0.0 134.5 jit_solution(1911328269046434722)
XLA Ops:
  0.6 4.7 %first.1 = (bf16[128,2048]{1,0:T(8,128)(2,1)}, bf16[256,2304]{1,0:T(8,128)(2,1)}, f32[32,8,256]{2,1,0:T(8,128)}, f32[32,8,256]{2,1,0:T(8,128)}, f32[32,8,256]{2,...) custom-call(bf16[128,2048]{1,0:T(8,128)(2,1)} %tokens_ref.1, f32[1,2048]{1,0:T(1,128)} %bitcast.31, ...), custom_call_target="tpu_custom_call" | custom-call | tf_op jit(solution)/shard_map/first/pallas_call | solution.py:297
  5.4 13.9 %all-to-all-start = ((bf16[32,8,2304]{2,1,0:T(8,128)(2,1)}), bf16[32,8,2304]{2,1,0:T(8,128)(2,1)S(1)}, u32[]{:S(2)}, u32[]{:S(2)}) async-start(bf16[32,8,2304]{2,1,0:T(8,128)(2,1)} %bitcast.17), calls=%async_computation | async-start | bytes 2359296 | tf_op jit(solution)/shard_map/all_to_all | solution.py:467
  19.2 3.2 %collective-permute-start.1 = (bf16[2048,128]{1,0:T(8,128)(2,1)S(1)}, bf16[2048,128]{1,0:T(8,128)(2,1)S(1)}, u32[]{:S(2)}, u32[]{:S(2)}) collective-permute-start(bf16[2048,128]{1,0:T(8,128)(2,1)S(1)} %bitcast.22), channel_id=1, source_target_pairs={{0,2},{2,0},{1,3},{3,1},{4,6},{6,4},{5,7},{7,5},{8,10},{10,8},{9,1... | collective-permute-start | bytes 1572872 | tf_op jit(solution)/shard_map/ppermute | solution.py:460
  22.5 2.1 %collective-permute-start.4 = (bf16[2048,128]{1,0:T(8,128)(2,1)S(1)}, bf16[2048,128]{1,0:T(8,128)(2,1)S(1)}, u32[]{:S(2)}, u32[]{:S(2)}) collective-permute-start(bf16[2048,128]{1,0:T(8,128)(2,1)S(1)} %bitcast.25), channel_id=1, source_target_pairs={{0,2},{2,0},{1,3},{3,1},{4,6},{6,4},{5,7},{7,5},{8,10},{10,8},{9,1... | collective-permute-start | bytes 1572872 | tf_op jit(solution)/shard_map/ppermute | solution.py:460
  24.6 3.4 %collective-permute-start = (bf16[2048,128]{1,0:T(8,128)(2,1)S(1)}, bf16[2048,128]{1,0:T(8,128)(2,1)}, u32[]{:S(2)}, u32[]{:S(2)}) collective-permute-start(bf16[2048,128]{1,0:T(8,128)(2,1)S(1)} %bitcast.23), channel_id=1, source_target_pairs={{0,1},{1,0},{2,3},{3,2},{4,5},{5,4},{6,7},{7,6},{8,9},{9,8},{10,11... | collective-permute-start | bytes 1572872 | tf_op jit(solution)/shard_map/ppermute | solution.py:461
  28.0 1.9 %collective-permute-start.3 = (bf16[2048,128]{1,0:T(8,128)(2,1)S(1)}, bf16[2048,128]{1,0:T(8,128)(2,1)}, u32[]{:S(2)}, u32[]{:S(2)}) collective-permute-start(bf16[2048,128]{1,0:T(8,128)(2,1)S(1)} %bitcast.26), channel_id=1, source_target_pairs={{0,1},{1,0},{2,3},{3,2},{4,5},{5,4},{6,7},{7,6},{8,9},{9,8},{10,11... | collective-permute-start | bytes 1572872 | tf_op jit(solution)/shard_map/ppermute | solution.py:461
  29.9 3.8 %collective-permute-done.1.refs_2_ = bf16[2048,128]{1,0:T(8,128)(2,1)S(1)} collective-permute-done((bf16[2048,128]{1,0:T(8,128)(2,1)S(1)}, bf16[2048,128]{1,0:T(8,128)(2,1)S(1)}, u32[]{:S(2)}, u32[]{:S(2)}) %collective-permute-start.1) | collective-permute-done | bytes 524320 | tf_op jit(solution)/shard_map/ppermute | solution.py:460
  33.7 5.1 %collective-permute-start.2 = (bf16[2048,128]{1,0:T(8,128)(2,1)S(1)}, bf16[2048,128]{1,0:T(8,128)(2,1)}, u32[]{:S(2)}, u32[]{:S(2)}) collective-permute-start(bf16[2048,128]{1,0:T(8,128)(2,1)S(1)} %collective-permute-done.1.refs_2_), channel_id=1, source_target_pairs={{0,1},{1,0},{2,3},{3,2},{4,5},{5,4},{6,7},{7,6},{8,9},{9,8},{10,11... | collective-permute-start | bytes 1572872 | tf_op jit(solution)/shard_map/ppermute | solution.py:462
  38.8 6.1 %collective-permute-done.4.refs_6_ = bf16[2048,128]{1,0:T(8,128)(2,1)S(1)} collective-permute-done((bf16[2048,128]{1,0:T(8,128)(2,1)S(1)}, bf16[2048,128]{1,0:T(8,128)(2,1)S(1)}, u32[]{:S(2)}, u32[]{:S(2)}) %collective-permute-start.4) | collective-permute-done | bytes 524320 | tf_op jit(solution)/shard_map/ppermute | solution.py:460
  44.9 3.7 %collective-permute-start.5 = (bf16[2048,128]{1,0:T(8,128)(2,1)S(1)}, bf16[2048,128]{1,0:T(8,128)(2,1)}, u32[]{:S(2)}, u32[]{:S(2)}) collective-permute-start(bf16[2048,128]{1,0:T(8,128)(2,1)S(1)} %collective-permute-done.4.refs_6_), channel_id=1, source_target_pairs={{0,1},{1,0},{2,3},{3,2},{4,5},{5,4},{6,7},{7,6},{8,9},{9,8},{10,11... | collective-permute-start | bytes 1572872 | tf_op jit(solution)/shard_map/ppermute | solution.py:462
  48.6 2.3 %shared_hidden.1.extra_ref = bf16[128,128]{1,0:T(8,128)(2,1)} custom-call(bf16[128,2048]{1,0:T(8,128)(2,1)} %get-tuple-element.16.rows_ref, bf16[2048,128]{1,0:T(8,128)(2,1)} %gate_ref.1, bf16[2048,128]{1,0:T(8,128)(2,1)} %up_ref.1), custom_call_target="tpu_custom_call" | custom-call | tf_op jit(solution)/shard_map/shared_hidden/pallas_call | solution.py:393
  51.0 5.3 %second.1 = bf16[4,320,512]{2,1,0:T(8,128)(2,1)} custom-call(bf16[32,8,2304]{2,1,0:T(8,128)(2,1)S(1)} %all-to-all-done.arrived_ref, bf16[128,128]{1,0:T(8,128)(2,1)} %shared_hidden.1.extra_ref, bf16[2048,128]{1,0:T(8,128)(2,1)} %bitcast.21, bf16[2048,128]{1,0:T(8,128)(2,1)} %collective-permute-done.refs_1_, bf16[2048,128]{1,0:T(8,128)(2,1)} %copy-done.8, ...), custom_call_target="tpu_custom_call" | custom-call | tf_op jit(solution)/shard_map/second/pallas_call | solution.py:376
  56.2 6.2 %all-to-all-start.1 = ((bf16[4,320,512]{2,1,0:T(8,128)(2,1)}), bf16[4,320,512]{2,1,0:T(8,128)(2,1)S(1)}, u32[]{:S(2)}, u32[]{:S(2)}) async-start(bf16[4,320,512]{2,1,0:T(8,128)(2,1)} %second.1), calls=%async_computation.1 | async-start | bytes 2621440 | tf_op jit(solution)/shard_map/all_to_all | solution.py:467
  62.4 3.0 %collective-permute-start.7 = (bf16[2048,128]{1,0:T(8,128)(2,1)S(1)}, bf16[2048,128]{1,0:T(8,128)(2,1)S(1)}, u32[]{:S(2)}, u32[]{:S(2)}) collective-permute-start(bf16[2048,128]{1,0:T(8,128)(2,1)S(1)} %bitcast.19), channel_id=1, source_target_pairs={{0,2},{2,0},{1,3},{3,1},{4,6},{6,4},{5,7},{7,5},{8,10},{10,8},{9,1... | collective-permute-start | bytes 1572872 | tf_op jit(solution)/shard_map/ppermute | solution.py:460
  65.4 2.5 %collective-permute-start.6 = (bf16[2048,128]{1,0:T(8,128)(2,1)S(1)}, bf16[2048,128]{1,0:T(8,128)(2,1)S(1)}, u32[]{:S(2)}, u32[]{:S(2)}) collective-permute-start(bf16[2048,128]{1,0:T(8,128)(2,1)S(1)} %bitcast.20), channel_id=1, source_target_pairs={{0,1},{1,0},{2,3},{3,2},{4,5},{5,4},{6,7},{7,6},{8,9},{9,8},{10,11... | collective-permute-start | bytes 1572872 | tf_op jit(solution)/shard_map/ppermute | solution.py:461
  67.9 28.9 %collective-permute-done.7.refs_3_ = bf16[2048,128]{1,0:T(8,128)(2,1)S(1)} collective-permute-done((bf16[2048,128]{1,0:T(8,128)(2,1)S(1)}, bf16[2048,128]{1,0:T(8,128)(2,1)S(1)}, u32[]{:S(2)}, u32[]{:S(2)}) %collective-permute-start.7) | collective-permute-done | bytes 524320 | tf_op jit(solution)/shard_map/ppermute | solution.py:460
  96.8 2.8 %collective-permute-start.8 = (bf16[2048,128]{1,0:T(8,128)(2,1)S(1)}, bf16[2048,128]{1,0:T(8,128)(2,1)S(1)}, u32[]{:S(2)}, u32[]{:S(2)}) collective-permute-start(bf16[2048,128]{1,0:T(8,128)(2,1)S(1)} %collective-permute-done.7.refs_3_), channel_id=1, source_target_pairs={{0,1},{1,0},{2,3},{3,2},{4,5},{5,4},{6,7},{7,6},{8,9},{9,8},{10,11... | collective-permute-start | bytes 1572872 | tf_op jit(solution)/shard_map/ppermute | solution.py:462
  101.9 3.3 %down.1 = (bf16[4,256,128]{2,1,0:T(8,128)(2,1)}, bf16[4,64,512]{2,1,0:T(8,128)(2,1)}) custom-call(bf16[4,320,512]{2,1,0:T(8,128)(2,1)S(1)} %all-to-all-done.1.refs_0_, bf16[2048,128]{1,0:T(8,128)(2,1)} %bitcast.18, bf16[2048,128]{1,0:T(8,128)(2,1)} %copy-done.4, bf16[2048,128]{1,0:T(8,128)(2,1)} %copy-done.3, bf16[2048,128]{1,0:T(8,128)(2,1)} %copy-done.5), custom_call_target="tpu_custom_call" | custom-call | tf_op jit(solution)/shard_map/down/pallas_call | solution.py:421
  105.2 2.3 %collective-permute-start.10 = (bf16[4,64,512]{2,1,0:T(8,128)(2,1)}, bf16[4,64,512]{2,1,0:T(8,128)(2,1)S(1)}, u32[]{:S(2)}, u32[]{:S(2)}) collective-permute-start(bf16[4,64,512]{2,1,0:T(8,128)(2,1)} %get-tuple-element.22.refs_0_), channel_id=1, source_target_pairs={{0,2},{2,0},{1,3},{3,1},{4,6},{6,4},{5,7},{7,5},{8,10},{10,8},{9,1... | collective-permute-start | bytes 786440 | tf_op jit(solution)/shard_map/ppermute | solution.py:532
  107.5 12.0 %all-to-all-start.2 = ((bf16[128,8,128]{2,1,0:T(8,128)(2,1)}), bf16[128,8,128]{2,1,0:T(8,128)(2,1)S(1)}, u32[]{:S(2)}, u32[]{:S(2)}) async-start(bf16[128,8,128]{2,1,0:T(8,128)(2,1)} %bitcast.27), calls=%async_computation.2 | async-start | bytes 524288 | tf_op jit(solution)/shard_map/all_to_all | solution.py:467
  119.5 2.7 %collective-permute-start.9 = (bf16[4,64,512]{2,1,0:T(8,128)(2,1)}, bf16[4,64,512]{2,1,0:T(8,128)(2,1)S(1)}, u32[]{:S(2)}, u32[]{:S(2)}) collective-permute-start(bf16[4,64,512]{2,1,0:T(8,128)(2,1)} %get-tuple-element.22.refs_0_), channel_id=1, source_target_pairs={{0,1},{1,0},{2,3},{3,2},{4,5},{5,4},{6,7},{7,6},{8,9},{9,8},{10,11... | collective-permute-start | bytes 786440 | tf_op jit(solution)/shard_map/ppermute | solution.py:531
  122.2 1.9 %collective-permute-start.11 = (bf16[4,64,512]{2,1,0:T(8,128)(2,1)S(1)}, bf16[4,64,512]{2,1,0:T(8,128)(2,1)S(1)}, u32[]{:S(2)}, u32[]{:S(2)}) collective-permute-start(bf16[4,64,512]{2,1,0:T(8,128)(2,1)S(1)} %collective-permute-done.10.refs_2_), channel_id=1, source_target_pairs={{0,1},{1,0},{2,3},{3,2},{4,5},{5,4},{6,7},{7,6},{8,9},{9,8},{10,11... | collective-permute-start | bytes 786440 | tf_op jit(solution)/shard_map/ppermute | solution.py:533
  126.0 2.7 %third.1 = (bf16[256,128]{1,0:T(8,128)(2,1)}, f32[128,128]{1,0:T(8,128)}) custom-call(bf16[4,64,512]{2,1,0:T(8,128)(2,1)} %get-tuple-element.22.refs_0_, bf16[4,64,512]{2,1,0:T(8,128)(2,1)S(1)} %collective-permute-done.9.refs_1_, bf16[4,64,512]{2,1,0:T(8,128)(2,1)S(1)} %collective-permute-done.10.refs_2_, ...), custom_call_target="tpu_custom_call" | custom-call | tf_op jit(solution)/shard_map/third/pallas_call | solution.py:233
  128.7 4.1 %all-to-all-done.2 = bf16[128,8,128]{2,1,0:T(8,128)(2,1)S(1)} async-done(((bf16[128,8,128]{2,1,0:T(8,128)(2,1)}), bf16[128,8,128]{2,1,0:T(8,128)(2,1)S(1)}, u32[]{:S(2)}, u32[]{:S(2)}) %all-to-all-start.2) | async-done | bytes 262176 | tf_op jit(solution)/shard_map/all_to_all | solution.py:467
  (33 shorter events, 6.0 us)
Async XLA Ops:
  5.4 13.9 %copy-start.6 = (bf16[1,2048,128]{2,1,0:T(8,128)(2,1)S(1)}, bf16[1,2048,128]{2,1,0:T(8,128)(2,1)}, u32[]{:S(2)}) copy-start(bf16[1,2048,128]{2,1,0:T(8,128)(2,1)} %param.34) | copy-start | bytes 1572868
  5.4 17.1 %copy-start.7 = (bf16[1,2048,128]{2,1,0:T(8,128)(2,1)S(1)}, bf16[1,2048,128]{2,1,0:T(8,128)(2,1)}, u32[]{:S(2)}) copy-start(bf16[1,2048,128]{2,1,0:T(8,128)(2,1)} %param.35) | copy-start | bytes 1572868
  5.4 45.6 %all-to-all-start = ((bf16[32,8,2304]{2,1,0:T(8,128)(2,1)}), bf16[32,8,2304]{2,1,0:T(8,128)(2,1)S(1)}, u32[]{:S(2)}, u32[]{:S(2)}) async-start(bf16[32,8,2304]{2,1,0:T(8,128)(2,1)} %bitcast.17), calls=%async_computation | async-start | bytes 2359296 | tf_op jit(solution)/shard_map/all_to_all | solution.py:467
  19.2 14.4 %collective-permute-start.1 = (bf16[2048,128]{1,0:T(8,128)(2,1)S(1)}, bf16[2048,128]{1,0:T(8,128)(2,1)S(1)}, u32[]{:S(2)}, u32[]{:S(2)}) collective-permute-start(bf16[2048,128]{1,0:T(8,128)(2,1)S(1)} %bitcast.22), channel_id=1, source_target_pairs={{0,2},{2,0},{1,3},{3,1},{4,6},{6,4},{5,7},{7,5},{8,10},{10,8},{9,1... | collective-permute-start | bytes 1572872 | tf_op jit(solution)/shard_map/ppermute | solution.py:460
  22.5 22.4 %collective-permute-start.4 = (bf16[2048,128]{1,0:T(8,128)(2,1)S(1)}, bf16[2048,128]{1,0:T(8,128)(2,1)S(1)}, u32[]{:S(2)}, u32[]{:S(2)}) collective-permute-start(bf16[2048,128]{1,0:T(8,128)(2,1)S(1)} %bitcast.25), channel_id=1, source_target_pairs={{0,2},{2,0},{1,3},{3,1},{4,6},{6,4},{5,7},{7,5},{8,10},{10,8},{9,1... | collective-permute-start | bytes 1572872 | tf_op jit(solution)/shard_map/ppermute | solution.py:460
  24.6 26.4 %collective-permute-start = (bf16[2048,128]{1,0:T(8,128)(2,1)S(1)}, bf16[2048,128]{1,0:T(8,128)(2,1)}, u32[]{:S(2)}, u32[]{:S(2)}) collective-permute-start(bf16[2048,128]{1,0:T(8,128)(2,1)S(1)} %bitcast.23), channel_id=1, source_target_pairs={{0,1},{1,0},{2,3},{3,2},{4,5},{5,4},{6,7},{7,6},{8,9},{9,8},{10,11... | collective-permute-start | bytes 1572872 | tf_op jit(solution)/shard_map/ppermute | solution.py:461
  28.0 22.9 %collective-permute-start.3 = (bf16[2048,128]{1,0:T(8,128)(2,1)S(1)}, bf16[2048,128]{1,0:T(8,128)(2,1)}, u32[]{:S(2)}, u32[]{:S(2)}) collective-permute-start(bf16[2048,128]{1,0:T(8,128)(2,1)S(1)} %bitcast.26), channel_id=1, source_target_pairs={{0,1},{1,0},{2,3},{3,2},{4,5},{5,4},{6,7},{7,6},{8,9},{9,8},{10,11... | collective-permute-start | bytes 1572872 | tf_op jit(solution)/shard_map/ppermute | solution.py:461
  33.7 17.3 %copy-start.8 = (bf16[2048,128]{1,0:T(8,128)(2,1)}, bf16[2048,128]{1,0:T(8,128)(2,1)S(1)}, u32[]{:S(2)}) copy-start(bf16[2048,128]{1,0:T(8,128)(2,1)S(1)} %collective-permute-done.1.refs_2_) | copy-start | bytes 1572868
  33.7 17.3 %collective-permute-start.2 = (bf16[2048,128]{1,0:T(8,128)(2,1)S(1)}, bf16[2048,128]{1,0:T(8,128)(2,1)}, u32[]{:S(2)}, u32[]{:S(2)}) collective-permute-start(bf16[2048,128]{1,0:T(8,128)(2,1)S(1)} %collective-permute-done.1.refs_2_), channel_id=1, source_target_pairs={{0,1},{1,0},{2,3},{3,2},{4,5},{5,4},{6,7},{7,6},{8,9},{9,8},{10,11... | collective-permute-start | bytes 1572872 | tf_op jit(solution)/shard_map/ppermute | solution.py:462
  44.9 6.1 %copy-start.9 = (bf16[2048,128]{1,0:T(8,128)(2,1)}, bf16[2048,128]{1,0:T(8,128)(2,1)S(1)}, u32[]{:S(2)}) copy-start(bf16[2048,128]{1,0:T(8,128)(2,1)S(1)} %collective-permute-done.4.refs_6_) | copy-start | bytes 1572868
  44.9 6.0 %collective-permute-start.5 = (bf16[2048,128]{1,0:T(8,128)(2,1)S(1)}, bf16[2048,128]{1,0:T(8,128)(2,1)}, u32[]{:S(2)}, u32[]{:S(2)}) collective-permute-start(bf16[2048,128]{1,0:T(8,128)(2,1)S(1)} %collective-permute-done.4.refs_6_), channel_id=1, source_target_pairs={{0,1},{1,0},{2,3},{3,2},{4,5},{5,4},{6,7},{7,6},{8,9},{9,8},{10,11... | collective-permute-start | bytes 1572872 | tf_op jit(solution)/shard_map/ppermute | solution.py:462
  56.2 6.2 %copy-start.2 = (bf16[1,2048,128]{2,1,0:T(8,128)(2,1)S(1)}, bf16[1,2048,128]{2,1,0:T(8,128)(2,1)}, u32[]{:S(2)}) copy-start(bf16[1,2048,128]{2,1,0:T(8,128)(2,1)} %param.36) | copy-start | bytes 1572868
  56.2 44.8 %all-to-all-start.1 = ((bf16[4,320,512]{2,1,0:T(8,128)(2,1)}), bf16[4,320,512]{2,1,0:T(8,128)(2,1)S(1)}, u32[]{:S(2)}, u32[]{:S(2)}) async-start(bf16[4,320,512]{2,1,0:T(8,128)(2,1)} %second.1), calls=%async_computation.1 | async-start | bytes 2621440 | tf_op jit(solution)/shard_map/all_to_all | solution.py:467
  62.4 34.4 %collective-permute-start.7 = (bf16[2048,128]{1,0:T(8,128)(2,1)S(1)}, bf16[2048,128]{1,0:T(8,128)(2,1)S(1)}, u32[]{:S(2)}, u32[]{:S(2)}) collective-permute-start(bf16[2048,128]{1,0:T(8,128)(2,1)S(1)} %bitcast.19), channel_id=1, source_target_pairs={{0,2},{2,0},{1,3},{3,1},{4,6},{6,4},{5,7},{7,5},{8,10},{10,8},{9,1... | collective-permute-start | bytes 1572872 | tf_op jit(solution)/shard_map/ppermute | solution.py:460
  65.4 34.2 %collective-permute-start.6 = (bf16[2048,128]{1,0:T(8,128)(2,1)S(1)}, bf16[2048,128]{1,0:T(8,128)(2,1)S(1)}, u32[]{:S(2)}, u32[]{:S(2)}) collective-permute-start(bf16[2048,128]{1,0:T(8,128)(2,1)S(1)} %bitcast.20), channel_id=1, source_target_pairs={{0,1},{1,0},{2,3},{3,2},{4,5},{5,4},{6,7},{7,6},{8,9},{9,8},{10,11... | collective-permute-start | bytes 1572872 | tf_op jit(solution)/shard_map/ppermute | solution.py:461
  96.8 4.3 %copy-start.3 = (bf16[2048,128]{1,0:T(8,128)(2,1)}, bf16[2048,128]{1,0:T(8,128)(2,1)S(1)}, u32[]{:S(2)}) copy-start(bf16[2048,128]{1,0:T(8,128)(2,1)S(1)} %collective-permute-done.7.refs_3_) | copy-start | bytes 1572868
  96.8 4.3 %collective-permute-start.8 = (bf16[2048,128]{1,0:T(8,128)(2,1)S(1)}, bf16[2048,128]{1,0:T(8,128)(2,1)S(1)}, u32[]{:S(2)}, u32[]{:S(2)}) collective-permute-start(bf16[2048,128]{1,0:T(8,128)(2,1)S(1)} %collective-permute-done.7.refs_3_), channel_id=1, source_target_pairs={{0,1},{1,0},{2,3},{3,2},{4,5},{5,4},{6,7},{7,6},{8,9},{9,8},{10,11... | collective-permute-start | bytes 1572872 | tf_op jit(solution)/shard_map/ppermute | solution.py:462
  99.6 1.5 %copy-start.4 = (bf16[2048,128]{1,0:T(8,128)(2,1)}, bf16[2048,128]{1,0:T(8,128)(2,1)S(1)}, u32[]{:S(2)}) copy-start(bf16[2048,128]{1,0:T(8,128)(2,1)S(1)} %collective-permute-done.6.refs_2_) | copy-start | bytes 1572868
  105.2 17.0 %collective-permute-start.10 = (bf16[4,64,512]{2,1,0:T(8,128)(2,1)}, bf16[4,64,512]{2,1,0:T(8,128)(2,1)S(1)}, u32[]{:S(2)}, u32[]{:S(2)}) collective-permute-start(bf16[4,64,512]{2,1,0:T(8,128)(2,1)} %get-tuple-element.22.refs_0_), channel_id=1, source_target_pairs={{0,2},{2,0},{1,3},{3,1},{4,6},{6,4},{5,7},{7,5},{8,10},{10,8},{9,1... | collective-permute-start | bytes 786440 | tf_op jit(solution)/shard_map/ppermute | solution.py:532
  107.5 25.3 %all-to-all-start.2 = ((bf16[128,8,128]{2,1,0:T(8,128)(2,1)}), bf16[128,8,128]{2,1,0:T(8,128)(2,1)S(1)}, u32[]{:S(2)}, u32[]{:S(2)}) async-start(bf16[128,8,128]{2,1,0:T(8,128)(2,1)} %bitcast.27), calls=%async_computation.2 | async-start | bytes 524288 | tf_op jit(solution)/shard_map/all_to_all | solution.py:467
  119.5 6.5 %collective-permute-start.9 = (bf16[4,64,512]{2,1,0:T(8,128)(2,1)}, bf16[4,64,512]{2,1,0:T(8,128)(2,1)S(1)}, u32[]{:S(2)}, u32[]{:S(2)}) collective-permute-start(bf16[4,64,512]{2,1,0:T(8,128)(2,1)} %get-tuple-element.22.refs_0_), channel_id=1, source_target_pairs={{0,1},{1,0},{2,3},{3,2},{4,5},{5,4},{6,7},{7,6},{8,9},{9,8},{10,11... | collective-permute-start | bytes 786440 | tf_op jit(solution)/shard_map/ppermute | solution.py:531
  122.2 3.8 %collective-permute-start.11 = (bf16[4,64,512]{2,1,0:T(8,128)(2,1)S(1)}, bf16[4,64,512]{2,1,0:T(8,128)(2,1)S(1)}, u32[]{:S(2)}, u32[]{:S(2)}) collective-permute-start(bf16[4,64,512]{2,1,0:T(8,128)(2,1)S(1)} %collective-permute-done.10.refs_2_), channel_id=1, source_target_pairs={{0,1},{1,0},{2,3},{3,2},{4,5},{5,4},{6,7},{7,6},{8,9},{9,8},{10,11... | collective-permute-start | bytes 786440 | tf_op jit(solution)/shard_map/ppermute | solution.py:533
  126.0 6.8 %copy-start = (bf16[128,1024]{1,0:T(8,128)(2,1)S(1)}, bf16[128,1024]{1,0:T(8,128)(2,1)}, u32[]{:S(2)}) copy-start(bf16[128,1024]{1,0:T(8,128)(2,1)} %get-tuple-element.26.high_ref) | copy-start | bytes 786436
  126.0 6.8 %copy-start.1 = (bf16[128,1024]{1,0:T(8,128)(2,1)S(1)}, bf16[128,1024]{1,0:T(8,128)(2,1)}, u32[]{:S(2)}) copy-start(bf16[128,1024]{1,0:T(8,128)(2,1)} %get-tuple-element.27.low_ref) | copy-start | bytes 786436
  (1 other events, 0.8 us)

commit v6 on v5

--- a/solution.py
+++ b/solution.py
@@ -270,15 +270,17 @@
     return own_place() ^ flipped(lax.axis_index("yh"))
 
 
-def first_kernel(tokens_ref, gain_ref, routes_ref, *refs):
-    scan_in, (normed_ref, sent_ref), scan_out = refs[:7], refs[7:9], refs[9:]
-    ends = scan_part(*scan_in, *scan_out)
-    tokens, width = tokens_ref.shape
+def normed_rows(tokens_ref, gain_ref):
     v = tokens_ref[...].astype(F32)
     factor = lax.rsqrt(jnp.mean(v * v, axis=1, keepdims=True) + EPS)
-    normed = (v * factor * gain_ref[...]).astype(BF16)
-    normed_ref[...] = normed
-    share = ends.shape[0]
+    return (v * factor * gain_ref[...]).astype(BF16)
+
+
+def first_kernel(tokens_ref, gain_ref, routes_ref, *refs):
+    scan_in, sent_ref, scan_out = refs[:7], refs[7], refs[8:]
+    tokens, width = tokens_ref.shape
+    normed = normed_rows(tokens_ref, gain_ref)
+    share = 8
     experts = sent_ref.shape[0] // share
     rank, _ = expert_table(routes_ref, None, experts)
     slot = (iota((share, tokens), 0) + own_sub() * share).astype(F32)
@@ -286,6 +288,7 @@
         [jnp.where(rank[e : e + 1, :] == slot, 1.0, 0.0) for e in range(experts)], axis=0
     ).astype(BF16)
     sent_ref[:, :width] = jnp.dot(chosen, normed, preferred_element_type=F32).astype(BF16)
+    ends = scan_part(*scan_in, *scan_out)
     for e in range(experts):
         sent_ref[e * share : (e + 1) * share, width:] = ends
 
@@ -293,17 +296,16 @@
 def run_first(tokens, gain, routes, blocks, x, log_step, loss, eig, freq, win, feed):
     width, positions = x.shape
     half = eig.size
-    piece = jax.ShapeDtypeStruct((positions // CHUNKS, CHUNKS, half), F32)
+    piece = VM((positions // CHUNKS, CHUNKS, half), F32)
     return pl.pallas_call(
         first_kernel,
         out_shape=[
-            jax.ShapeDtypeStruct(tokens.shape, BF16),
             jax.ShapeDtypeStruct((blocks * half // 32, tokens.shape[1] + 256), BF16),
         ]
         + [piece] * 4
         + [jax.ShapeDtypeStruct((positions, width), F32)],
         in_specs=vmem(10),
-        out_specs=vmem(7),
+        out_specs=vmem(6),
         scratch_shapes=[VM((half // 128, positions, 128), F32)] * 4,
         name="first",
     )(tokens, gain.reshape(1, -1), routes, x, log_step, loss, eig, freq, win, feed)
@@ -380,23 +382,24 @@
         out_specs=pl.BlockSpec(memory_space=VM),
         scratch_shapes=[VM((through.shape[0], 128), F32)],
         name="second",
-    )(*held(arrived), extra, *gates, *ups, *pieces, through, wout)
-
-
-def shared_hidden_kernel(rows_ref, gate_ref, up_ref, out_ref):
+    )(*held(arrived), extra, *gates, *ups, *held(*pieces), through, wout)
+
+
+def shared_hidden_kernel(tokens_ref, gain_ref, gate_ref, up_ref, out_ref):
+    rows = normed_rows(tokens_ref, gain_ref)
     both = jnp.concatenate([gate_ref[...], up_ref[...]], axis=1)
-    got = gated(jnp.dot(rows_ref[...], both, preferred_element_type=F32))
+    got = gated(jnp.dot(rows, both, preferred_element_type=F32))
     out_ref[...] = got
 
 
-def run_shared_hidden(rows, gate, up):
+def run_shared_hidden(tokens, gain, gate, up):
     return pl.pallas_call(
         shared_hidden_kernel,
-        out_shape=jax.ShapeDtypeStruct((rows.shape[0], gate.shape[1]), BF16),
-        in_specs=vmem(3),
+        out_shape=jax.ShapeDtypeStruct((tokens.shape[0], gate.shape[1]), BF16),
+        in_specs=vmem(4),
         out_specs=pl.BlockSpec(memory_space=VM),
         name="shared_hidden",
-    )(rows, gate, up)
+    )(tokens, gain.reshape(1, -1), gate, up)
 
 
 def down_kernel(*refs):
@@ -493,7 +496,7 @@
 ):
     blocks = lax.axis_size("ep")
     routes = routes.T
-    normed, sent, *pieces, through = run_first(
+    sent, *pieces, through = run_first(
         second_micro_input,
         expert_norm_scale,
         routes,
@@ -510,7 +513,9 @@
     gates = exchanged(expert_gate_weight[0])
     ups = exchanged(expert_up_weight[0])
     downs = exchanged(expert_down_weight[0])
-    shared_hidden = run_shared_hidden(normed, shared_gate_weight, shared_up_weight)
+    shared_hidden = run_shared_hidden(
+        second_micro_input, expert_norm_scale, shared_gate_weight, shared_up_weight
+    )
     high, low = run_choice(routes, chosen_expert_weight.T, blocks * 32)
 
     hidden = run_second(

time: 135 us -> 135 us (level)
  no operation moved by 1% of the time
where the time goes in v6:
time: 135 us; the launch traced here: 134 us
  starting transfers between devices  66.6 us (49%)
  waiting for transfers between devices  44.5 us (33%)
  Pallas kernels  21.2 us (16%)
    ppermute x3, waiting for transfers between devices, exchanged(): over = lax.ppermute(piece, 'yl', SWAP)  38.9 us
    all_to_all x3, starting transfers between devices, spread_out(): lax.all_to_all(pieces, axes, split_axis=0, concat_axis=0, axis_index_grou...  32 us
    ppermute x3, starting transfers between devices, exchanged(): both = lax.ppermute(over, 'co', SWAP)  11.6 us
    ppermute x3, starting transfers between devices, exchanged(): over = lax.ppermute(piece, 'yl', SWAP)  8.25 us
    ppermute x3, starting transfers between devices, exchanged(): core = lax.ppermute(piece, 'co', SWAP)  7.83 us
    pallas_call x1, Pallas kernels, run_second(): pl.pallas_call(second_kernel, out_shape=jax.ShapeDtypeStruct((copies, row...  4.96 us
    pallas_call x1, Pallas kernels, run_first(): pl.pallas_call(first_kernel, out_shape=[jax.ShapeDtypeStruct((blocks * ha...  4.3 us
    all_to_all x3, waiting for transfers between devices, spread_out(): lax.all_to_all(pieces, axes, split_axis=0, concat_axis=0, axis_index_grou...  4.11 us
  transfers between devices with their start and end apart: 15, of which 5 were waited for; matrix products, arithmetic and copies ran while one was open for 0% of the time, Pallas kernels for 5%

profile of v6, /device:TPU:1, one launch (start us, length us, event | category | flops | bytes accessed | tf_op | source)
XLA Modules:
  0.0 134.0 jit_solution(3020072537277858619)
XLA Ops:
  0.6 4.3 %first.1 = (bf16[256,2304]{1,0:T(8,128)(2,1)}, f32[32,8,256]{2,1,0:T(8,128)S(1)}, f32[32,8,256]{2,1,0:T(8,128)S(1)}, f32[32,8,256]{2,1,0:T(8,128)S(1)}, f32[32,8,256]{2,1,0:T(8,128)S(1)}, /*index=5*/f32[256,64]{1,0:T(8,128)}) custom-call(bf16[128,2048]{1,0:T(8,128)(2,1)} %tokens_ref.3, f32[1,2048]{1,0:T(1,128)} %bitcast.29, s32[4,128]{1,0:T(4,128)} %bitcast.33, ...), custom_call_target="tpu_custom_call" | custom-call | tf_op jit(solution)/shard_map/first/pallas_call | solution.py:300
  4.9 13.8 %all-to-all-start = ((bf16[32,8,2304]{2,1,0:T(8,128)(2,1)}), bf16[32,8,2304]{2,1,0:T(8,128)(2,1)S(1)}, u32[]{:S(2)}, u32[]{:S(2)}) async-start(bf16[32,8,2304]{2,1,0:T(8,128)(2,1)} %bitcast.17), calls=%async_computation | async-start | bytes 2359296 | tf_op jit(solution)/shard_map/all_to_all | solution.py:470
  18.8 3.2 %collective-permute-start.1 = (bf16[2048,128]{1,0:T(8,128)(2,1)S(1)}, bf16[2048,128]{1,0:T(8,128)(2,1)}, u32[]{:S(2)}, u32[]{:S(2)}) collective-permute-start(bf16[2048,128]{1,0:T(8,128)(2,1)S(1)} %bitcast.22), channel_id=1, source_target_pairs={{0,2},{2,0},{1,3},{3,1},{4,6},{6,4},{5,7},{7,5},{8,10},{10,8},{9,1... | collective-permute-start | bytes 1572872 | tf_op jit(solution)/shard_map/ppermute | solution.py:463
  22.0 2.1 %collective-permute-start.4 = (bf16[2048,128]{1,0:T(8,128)(2,1)S(1)}, bf16[2048,128]{1,0:T(8,128)(2,1)}, u32[]{:S(2)}, u32[]{:S(2)}) collective-permute-start(bf16[2048,128]{1,0:T(8,128)(2,1)S(1)} %bitcast.25), channel_id=1, source_target_pairs={{0,2},{2,0},{1,3},{3,1},{4,6},{6,4},{5,7},{7,5},{8,10},{10,8},{9,1... | collective-permute-start | bytes 1572872 | tf_op jit(solution)/shard_map/ppermute | solution.py:463
  24.1 3.4 %collective-permute-start = (bf16[2048,128]{1,0:T(8,128)(2,1)S(1)}, bf16[2048,128]{1,0:T(8,128)(2,1)}, u32[]{:S(2)}, u32[]{:S(2)}) collective-permute-start(bf16[2048,128]{1,0:T(8,128)(2,1)S(1)} %bitcast.23), channel_id=1, source_target_pairs={{0,1},{1,0},{2,3},{3,2},{4,5},{5,4},{6,7},{7,6},{8,9},{9,8},{10,11... | collective-permute-start | bytes 1572872 | tf_op jit(solution)/shard_map/ppermute | solution.py:464
  27.6 1.9 %collective-permute-start.3 = (bf16[2048,128]{1,0:T(8,128)(2,1)S(1)}, bf16[2048,128]{1,0:T(8,128)(2,1)}, u32[]{:S(2)}, u32[]{:S(2)}) collective-permute-start(bf16[2048,128]{1,0:T(8,128)(2,1)S(1)} %bitcast.26), channel_id=1, source_target_pairs={{0,1},{1,0},{2,3},{3,2},{4,5},{5,4},{6,7},{7,6},{8,9},{9,8},{10,11... | collective-permute-start | bytes 1572872 | tf_op jit(solution)/shard_map/ppermute | solution.py:464
  29.5 3.8 %collective-permute-done.1.refs_2_ = bf16[2048,128]{1,0:T(8,128)(2,1)} collective-permute-done((bf16[2048,128]{1,0:T(8,128)(2,1)S(1)}, bf16[2048,128]{1,0:T(8,128)(2,1)}, u32[]{:S(2)}, u32[]{:S(2)}) %collective-permute-start.1) | collective-permute-done | bytes 524320 | tf_op jit(solution)/shard_map/ppermute | solution.py:463
  33.3 5.1 %collective-permute-start.2 = (bf16[2048,128]{1,0:T(8,128)(2,1)}, bf16[2048,128]{1,0:T(8,128)(2,1)}, u32[]{:S(2)}, u32[]{:S(2)}) collective-permute-start(bf16[2048,128]{1,0:T(8,128)(2,1)} %collective-permute-done.1.refs_2_), channel_id=1, source_target_pairs={{0,1},{1,0},{2,3},{3,2},{4,5},{5,4},{6,7},{7,6},{8,9},{9,8},{10,11... | collective-permute-start | bytes 1572872 | tf_op jit(solution)/shard_map/ppermute | solution.py:465
  38.5 6.1 %collective-permute-done.4.refs_6_ = bf16[2048,128]{1,0:T(8,128)(2,1)} collective-permute-done((bf16[2048,128]{1,0:T(8,128)(2,1)S(1)}, bf16[2048,128]{1,0:T(8,128)(2,1)}, u32[]{:S(2)}, u32[]{:S(2)}) %collective-permute-start.4) | collective-permute-done | bytes 524320 | tf_op jit(solution)/shard_map/ppermute | solution.py:463
  44.6 3.7 %collective-permute-start.5 = (bf16[2048,128]{1,0:T(8,128)(2,1)}, bf16[2048,128]{1,0:T(8,128)(2,1)}, u32[]{:S(2)}, u32[]{:S(2)}) collective-permute-start(bf16[2048,128]{1,0:T(8,128)(2,1)} %collective-permute-done.4.refs_6_), channel_id=1, source_target_pairs={{0,1},{1,0},{2,3},{3,2},{4,5},{5,4},{6,7},{7,6},{8,9},{9,8},{10,11... | collective-permute-start | bytes 1572872 | tf_op jit(solution)/shard_map/ppermute | solution.py:465
  48.3 2.5 %shared_hidden.1.extra_ref = bf16[128,128]{1,0:T(8,128)(2,1)} custom-call(bf16[128,2048]{1,0:T(8,128)(2,1)} %tokens_ref.3, f32[1,2048]{1,0:T(1,128)} %bitcast.30, bf16[2048,128]{1,0:T(8,128)(2,1)} %gate_ref.1, bf16[2048,128]{1,0:T(8,128)(2,1)} %up_ref.1), custom_call_target="tpu_custom_call" | custom-call | tf_op jit(solution)/shard_map/shared_hidden/pallas_call | solution.py:396
  50.8 5.0 %second.1 = bf16[4,320,512]{2,1,0:T(8,128)(2,1)} custom-call(bf16[32,8,2304]{2,1,0:T(8,128)(2,1)S(1)} %all-to-all-done.arrived_ref, bf16[128,128]{1,0:T(8,128)(2,1)} %shared_hidden.1.extra_ref, bf16[2048,128]{1,0:T(8,128)(2,1)} %bitcast.21, bf16[2048,128]{1,0:T(8,128)(2,1)} %collective-permute-done.refs_1_, ...), custom_call_target="tpu_custom_call" | custom-call | tf_op jit(solution)/shard_map/second/pallas_call | solution.py:378
  55.7 6.2 %all-to-all-start.1 = ((bf16[4,320,512]{2,1,0:T(8,128)(2,1)}), bf16[4,320,512]{2,1,0:T(8,128)(2,1)S(1)}, u32[]{:S(2)}, u32[]{:S(2)}) async-start(bf16[4,320,512]{2,1,0:T(8,128)(2,1)} %second.1), calls=%async_computation.1 | async-start | bytes 2621440 | tf_op jit(solution)/shard_map/all_to_all | solution.py:470
  61.9 3.0 %collective-permute-start.7 = (bf16[2048,128]{1,0:T(8,128)(2,1)S(1)}, bf16[2048,128]{1,0:T(8,128)(2,1)S(1)}, u32[]{:S(2)}, u32[]{:S(2)}) collective-permute-start(bf16[2048,128]{1,0:T(8,128)(2,1)S(1)} %bitcast.19), channel_id=1, source_target_pairs={{0,2},{2,0},{1,3},{3,1},{4,6},{6,4},{5,7},{7,5},{8,10},{10,8},{9,1... | collective-permute-start | bytes 1572872 | tf_op jit(solution)/shard_map/ppermute | solution.py:463
  64.9 2.5 %collective-permute-start.6 = (bf16[2048,128]{1,0:T(8,128)(2,1)S(1)}, bf16[2048,128]{1,0:T(8,128)(2,1)S(1)}, u32[]{:S(2)}, u32[]{:S(2)}) collective-permute-start(bf16[2048,128]{1,0:T(8,128)(2,1)S(1)} %bitcast.20), channel_id=1, source_target_pairs={{0,1},{1,0},{2,3},{3,2},{4,5},{5,4},{6,7},{7,6},{8,9},{9,8},{10,11... | collective-permute-start | bytes 1572872 | tf_op jit(solution)/shard_map/ppermute | solution.py:464
  67.4 28.9 %collective-permute-done.7.refs_3_ = bf16[2048,128]{1,0:T(8,128)(2,1)S(1)} collective-permute-done((bf16[2048,128]{1,0:T(8,128)(2,1)S(1)}, bf16[2048,128]{1,0:T(8,128)(2,1)S(1)}, u32[]{:S(2)}, u32[]{:S(2)}) %collective-permute-start.7) | collective-permute-done | bytes 524320 | tf_op jit(solution)/shard_map/ppermute | solution.py:463
  96.3 2.8 %collective-permute-start.8 = (bf16[2048,128]{1,0:T(8,128)(2,1)S(1)}, bf16[2048,128]{1,0:T(8,128)(2,1)S(1)}, u32[]{:S(2)}, u32[]{:S(2)}) collective-permute-start(bf16[2048,128]{1,0:T(8,128)(2,1)S(1)} %collective-permute-done.7.refs_3_), channel_id=1, source_target_pairs={{0,1},{1,0},{2,3},{3,2},{4,5},{5,4},{6,7},{7,6},{8,9},{9,8},{10,11... | collective-permute-start | bytes 1572872 | tf_op jit(solution)/shard_map/ppermute | solution.py:465
  101.4 3.3 %down.1 = (bf16[4,256,128]{2,1,0:T(8,128)(2,1)}, bf16[4,64,512]{2,1,0:T(8,128)(2,1)}) custom-call(bf16[4,320,512]{2,1,0:T(8,128)(2,1)S(1)} %all-to-all-done.1.refs_0_, bf16[2048,128]{1,0:T(8,128)(2,1)} %bitcast.18, bf16[2048,128]{1,0:T(8,128)(2,1)} %copy-done.4, bf16[2048,128]{1,0:T(8,128)(2,1)} %copy-done.3, bf16[2048,128]{1,0:T(8,128)(2,1)} %copy-done.5), custom_call_target="tpu_custom_call" | custom-call | tf_op jit(solution)/shard_map/down/pallas_call | solution.py:424
  104.6 2.3 %collective-permute-start.10 = (bf16[4,64,512]{2,1,0:T(8,128)(2,1)}, bf16[4,64,512]{2,1,0:T(8,128)(2,1)S(1)}, u32[]{:S(2)}, u32[]{:S(2)}) collective-permute-start(bf16[4,64,512]{2,1,0:T(8,128)(2,1)} %get-tuple-element.20.refs_0_), channel_id=1, source_target_pairs={{0,2},{2,0},{1,3},{3,1},{4,6},{6,4},{5,7},{7,5},{8,10},{10,8},{9,1... | collective-permute-start | bytes 786440 | tf_op jit(solution)/shard_map/ppermute | solution.py:537
  106.9 12.0 %all-to-all-start.2 = ((bf16[128,8,128]{2,1,0:T(8,128)(2,1)}), bf16[128,8,128]{2,1,0:T(8,128)(2,1)S(1)}, u32[]{:S(2)}, u32[]{:S(2)}) async-start(bf16[128,8,128]{2,1,0:T(8,128)(2,1)} %bitcast.27), calls=%async_computation.2 | async-start | bytes 524288 | tf_op jit(solution)/shard_map/all_to_all | solution.py:470
  118.9 2.7 %collective-permute-start.9 = (bf16[4,64,512]{2,1,0:T(8,128)(2,1)}, bf16[4,64,512]{2,1,0:T(8,128)(2,1)S(1)}, u32[]{:S(2)}, u32[]{:S(2)}) collective-permute-start(bf16[4,64,512]{2,1,0:T(8,128)(2,1)} %get-tuple-element.20.refs_0_), channel_id=1, source_target_pairs={{0,1},{1,0},{2,3},{3,2},{4,5},{5,4},{6,7},{7,6},{8,9},{9,8},{10,11... | collective-permute-start | bytes 786440 | tf_op jit(solution)/shard_map/ppermute | solution.py:536
  121.7 1.9 %collective-permute-start.11 = (bf16[4,64,512]{2,1,0:T(8,128)(2,1)S(1)}, bf16[4,64,512]{2,1,0:T(8,128)(2,1)S(1)}, u32[]{:S(2)}, u32[]{:S(2)}) collective-permute-start(bf16[4,64,512]{2,1,0:T(8,128)(2,1)S(1)} %collective-permute-done.10.refs_2_), channel_id=1, source_target_pairs={{0,1},{1,0},{2,3},{3,2},{4,5},{5,4},{6,7},{7,6},{8,9},{9,8},{10,11... | collective-permute-start | bytes 786440 | tf_op jit(solution)/shard_map/ppermute | solution.py:538
  125.5 2.7 %third.1 = (bf16[256,128]{1,0:T(8,128)(2,1)}, f32[128,128]{1,0:T(8,128)}) custom-call(bf16[4,64,512]{2,1,0:T(8,128)(2,1)} %get-tuple-element.20.refs_0_, bf16[4,64,512]{2,1,0:T(8,128)(2,1)S(1)} %collective-permute-done.9.refs_1_, bf16[4,64,512]{2,1,0:T(8,128)(2,1)S(1)} %collective-permute-done.10.refs_2_, ...), custom_call_target="tpu_custom_call" | custom-call | tf_op jit(solution)/shard_map/third/pallas_call | solution.py:233
  128.1 4.1 %all-to-all-done.2 = bf16[128,8,128]{2,1,0:T(8,128)(2,1)S(1)} async-done(((bf16[128,8,128]{2,1,0:T(8,128)(2,1)}), bf16[128,8,128]{2,1,0:T(8,128)(2,1)S(1)}, u32[]{:S(2)}, u32[]{:S(2)}) %all-to-all-start.2) | async-done | bytes 262176 | tf_op jit(solution)/shard_map/all_to_all | solution.py:470
  (29 shorter events, 5.9 us)
Async XLA Ops:
  4.9 13.9 %copy-start.6 = (bf16[1,2048,128]{2,1,0:T(8,128)(2,1)S(1)}, bf16[1,2048,128]{2,1,0:T(8,128)(2,1)}, u32[]{:S(2)}) copy-start(bf16[1,2048,128]{2,1,0:T(8,128)(2,1)} %param.34) | copy-start | bytes 1572868
  4.9 17.1 %copy-start.7 = (bf16[1,2048,128]{2,1,0:T(8,128)(2,1)S(1)}, bf16[1,2048,128]{2,1,0:T(8,128)(2,1)}, u32[]{:S(2)}) copy-start(bf16[1,2048,128]{2,1,0:T(8,128)(2,1)} %param.35) | copy-start | bytes 1572868
  4.9 45.8 %all-to-all-start = ((bf16[32,8,2304]{2,1,0:T(8,128)(2,1)}), bf16[32,8,2304]{2,1,0:T(8,128)(2,1)S(1)}, u32[]{:S(2)}, u32[]{:S(2)}) async-start(bf16[32,8,2304]{2,1,0:T(8,128)(2,1)} %bitcast.17), calls=%async_computation | async-start | bytes 2359296 | tf_op jit(solution)/shard_map/all_to_all | solution.py:470
  18.8 14.5 %collective-permute-start.1 = (bf16[2048,128]{1,0:T(8,128)(2,1)S(1)}, bf16[2048,128]{1,0:T(8,128)(2,1)}, u32[]{:S(2)}, u32[]{:S(2)}) collective-permute-start(bf16[2048,128]{1,0:T(8,128)(2,1)S(1)} %bitcast.22), channel_id=1, source_target_pairs={{0,2},{2,0},{1,3},{3,1},{4,6},{6,4},{5,7},{7,5},{8,10},{10,8},{9,1... | collective-permute-start | bytes 1572872 | tf_op jit(solution)/shard_map/ppermute | solution.py:463
  22.0 22.5 %collective-permute-start.4 = (bf16[2048,128]{1,0:T(8,128)(2,1)S(1)}, bf16[2048,128]{1,0:T(8,128)(2,1)}, u32[]{:S(2)}, u32[]{:S(2)}) collective-permute-start(bf16[2048,128]{1,0:T(8,128)(2,1)S(1)} %bitcast.25), channel_id=1, source_target_pairs={{0,2},{2,0},{1,3},{3,1},{4,6},{6,4},{5,7},{7,5},{8,10},{10,8},{9,1... | collective-permute-start | bytes 1572872 | tf_op jit(solution)/shard_map/ppermute | solution.py:463
  24.1 26.6 %collective-permute-start = (bf16[2048,128]{1,0:T(8,128)(2,1)S(1)}, bf16[2048,128]{1,0:T(8,128)(2,1)}, u32[]{:S(2)}, u32[]{:S(2)}) collective-permute-start(bf16[2048,128]{1,0:T(8,128)(2,1)S(1)} %bitcast.23), channel_id=1, source_target_pairs={{0,1},{1,0},{2,3},{3,2},{4,5},{5,4},{6,7},{7,6},{8,9},{9,8},{10,11... | collective-permute-start | bytes 1572872 | tf_op jit(solution)/shard_map/ppermute | solution.py:464
  27.6 23.2 %collective-permute-start.3 = (bf16[2048,128]{1,0:T(8,128)(2,1)S(1)}, bf16[2048,128]{1,0:T(8,128)(2,1)}, u32[]{:S(2)}, u32[]{:S(2)}) collective-permute-start(bf16[2048,128]{1,0:T(8,128)(2,1)S(1)} %bitcast.26), channel_id=1, source_target_pairs={{0,1},{1,0},{2,3},{3,2},{4,5},{5,4},{6,7},{7,6},{8,9},{9,8},{10,11... | collective-permute-start | bytes 1572872 | tf_op jit(solution)/shard_map/ppermute | solution.py:464
  33.3 17.4 %collective-permute-start.2 = (bf16[2048,128]{1,0:T(8,128)(2,1)}, bf16[2048,128]{1,0:T(8,128)(2,1)}, u32[]{:S(2)}, u32[]{:S(2)}) collective-permute-start(bf16[2048,128]{1,0:T(8,128)(2,1)} %collective-permute-done.1.refs_2_), channel_id=1, source_target_pairs={{0,1},{1,0},{2,3},{3,2},{4,5},{5,4},{6,7},{7,6},{8,9},{9,8},{10,11... | collective-permute-start | bytes 1572872 | tf_op jit(solution)/shard_map/ppermute | solution.py:465
  44.6 6.2 %collective-permute-start.5 = (bf16[2048,128]{1,0:T(8,128)(2,1)}, bf16[2048,128]{1,0:T(8,128)(2,1)}, u32[]{:S(2)}, u32[]{:S(2)}) collective-permute-start(bf16[2048,128]{1,0:T(8,128)(2,1)} %collective-permute-done.4.refs_6_), channel_id=1, source_target_pairs={{0,1},{1,0},{2,3},{3,2},{4,5},{5,4},{6,7},{7,6},{8,9},{9,8},{10,11... | collective-permute-start | bytes 1572872 | tf_op jit(solution)/shard_map/ppermute | solution.py:465
  55.7 6.2 %copy-start.2 = (bf16[1,2048,128]{2,1,0:T(8,128)(2,1)S(1)}, bf16[1,2048,128]{2,1,0:T(8,128)(2,1)}, u32[]{:S(2)}) copy-start(bf16[1,2048,128]{2,1,0:T(8,128)(2,1)} %param.36) | copy-start | bytes 1572868
  55.7 44.9 %all-to-all-start.1 = ((bf16[4,320,512]{2,1,0:T(8,128)(2,1)}), bf16[4,320,512]{2,1,0:T(8,128)(2,1)S(1)}, u32[]{:S(2)}, u32[]{:S(2)}) async-start(bf16[4,320,512]{2,1,0:T(8,128)(2,1)} %second.1), calls=%async_computation.1 | async-start | bytes 2621440 | tf_op jit(solution)/shard_map/all_to_all | solution.py:470
  61.9 34.4 %collective-permute-start.7 = (bf16[2048,128]{1,0:T(8,128)(2,1)S(1)}, bf16[2048,128]{1,0:T(8,128)(2,1)S(1)}, u32[]{:S(2)}, u32[]{:S(2)}) collective-permute-start(bf16[2048,128]{1,0:T(8,128)(2,1)S(1)} %bitcast.19), channel_id=1, source_target_pairs={{0,2},{2,0},{1,3},{3,1},{4,6},{6,4},{5,7},{7,5},{8,10},{10,8},{9,1... | collective-permute-start | bytes 1572872 | tf_op jit(solution)/shard_map/ppermute | solution.py:463
  64.9 34.2 %collective-permute-start.6 = (bf16[2048,128]{1,0:T(8,128)(2,1)S(1)}, bf16[2048,128]{1,0:T(8,128)(2,1)S(1)}, u32[]{:S(2)}, u32[]{:S(2)}) collective-permute-start(bf16[2048,128]{1,0:T(8,128)(2,1)S(1)} %bitcast.20), channel_id=1, source_target_pairs={{0,1},{1,0},{2,3},{3,2},{4,5},{5,4},{6,7},{7,6},{8,9},{9,8},{10,11... | collective-permute-start | bytes 1572872 | tf_op jit(solution)/shard_map/ppermute | solution.py:464
  96.3 4.3 %copy-start.3 = (bf16[2048,128]{1,0:T(8,128)(2,1)}, bf16[2048,128]{1,0:T(8,128)(2,1)S(1)}, u32[]{:S(2)}) copy-start(bf16[2048,128]{1,0:T(8,128)(2,1)S(1)} %collective-permute-done.7.refs_3_) | copy-start | bytes 1572868
  96.3 4.3 %collective-permute-start.8 = (bf16[2048,128]{1,0:T(8,128)(2,1)S(1)}, bf16[2048,128]{1,0:T(8,128)(2,1)S(1)}, u32[]{:S(2)}, u32[]{:S(2)}) collective-permute-start(bf16[2048,128]{1,0:T(8,128)(2,1)S(1)} %collective-permute-done.7.refs_3_), channel_id=1, source_target_pairs={{0,1},{1,0},{2,3},{3,2},{4,5},{5,4},{6,7},{7,6},{8,9},{9,8},{10,11... | collective-permute-start | bytes 1572872 | tf_op jit(solution)/shard_map/ppermute | solution.py:465
  99.1 1.5 %copy-start.4 = (bf16[2048,128]{1,0:T(8,128)(2,1)}, bf16[2048,128]{1,0:T(8,128)(2,1)S(1)}, u32[]{:S(2)}) copy-start(bf16[2048,128]{1,0:T(8,128)(2,1)S(1)} %collective-permute-done.6.refs_2_) | copy-start | bytes 1572868
  100.6 0.8 copy-start.5
  104.6 17.0 %collective-permute-start.10 = (bf16[4,64,512]{2,1,0:T(8,128)(2,1)}, bf16[4,64,512]{2,1,0:T(8,128)(2,1)S(1)}, u32[]{:S(2)}, u32[]{:S(2)}) collective-permute-start(bf16[4,64,512]{2,1,0:T(8,128)(2,1)} %get-tuple-element.20.refs_0_), channel_id=1, source_target_pairs={{0,2},{2,0},{1,3},{3,1},{4,6},{6,4},{5,7},{7,5},{8,10},{10,8},{9,1... | collective-permute-start | bytes 786440 | tf_op jit(solution)/shard_map/ppermute | solution.py:537
  106.9 25.3 %all-to-all-start.2 = ((bf16[128,8,128]{2,1,0:T(8,128)(2,1)}), bf16[128,8,128]{2,1,0:T(8,128)(2,1)S(1)}, u32[]{:S(2)}, u32[]{:S(2)}) async-start(bf16[128,8,128]{2,1,0:T(8,128)(2,1)} %bitcast.27), calls=%async_computation.2 | async-start | bytes 524288 | tf_op jit(solution)/shard_map/all_to_all | solution.py:470
  118.9 6.5 %collective-permute-start.9 = (bf16[4,64,512]{2,1,0:T(8,128)(2,1)}, bf16[4,64,512]{2,1,0:T(8,128)(2,1)S(1)}, u32[]{:S(2)}, u32[]{:S(2)}) collective-permute-start(bf16[4,64,512]{2,1,0:T(8,128)(2,1)} %get-tuple-element.20.refs_0_), channel_id=1, source_target_pairs={{0,1},{1,0},{2,3},{3,2},{4,5},{5,4},{6,7},{7,6},{8,9},{9,8},{10,11... | collective-permute-start | bytes 786440 | tf_op jit(solution)/shard_map/ppermute | solution.py:536
  121.7 3.8 %collective-permute-start.11 = (bf16[4,64,512]{2,1,0:T(8,128)(2,1)S(1)}, bf16[4,64,512]{2,1,0:T(8,128)(2,1)S(1)}, u32[]{:S(2)}, u32[]{:S(2)}) collective-permute-start(bf16[4,64,512]{2,1,0:T(8,128)(2,1)S(1)} %collective-permute-done.10.refs_2_), channel_id=1, source_target_pairs={{0,1},{1,0},{2,3},{3,2},{4,5},{5,4},{6,7},{7,6},{8,9},{9,8},{10,11... | collective-permute-start | bytes 786440 | tf_op jit(solution)/shard_map/ppermute | solution.py:538
  125.5 6.8 %copy-start = (bf16[128,1024]{1,0:T(8,128)(2,1)S(1)}, bf16[128,1024]{1,0:T(8,128)(2,1)}, u32[]{:S(2)}) copy-start(bf16[128,1024]{1,0:T(8,128)(2,1)} %get-tuple-element.24.high_ref) | copy-start | bytes 786436
  125.5 6.8 %copy-start.1 = (bf16[128,1024]{1,0:T(8,128)(2,1)S(1)}, bf16[128,1024]{1,0:T(8,128)(2,1)}, u32[]{:S(2)}) copy-start(bf16[128,1024]{1,0:T(8,128)(2,1)} %get-tuple-element.25.low_ref) | copy-start | bytes 786436
